TPU v7x, 32 devices: a whole 2x2x4 slice. The times are simulated.
32 devices in a mesh: sp: 8 (over z, y), tp: 4 (over x, core).
Axes of the slice: x: 2, y: 2, z: 4, core: 2. Of those that a mesh axis runs over, the one named last changes fastest.
Arguments:
- latent: bfloat16 [2048, 2048], P('sp'), may hold values from -6 to 6
- context: bfloat16 [512, 2048], P('sp'), may hold values from -6 to 6
- condition: float32 [2048], P('sp'), may hold values from -6 to 6
- ctx_condition: float32 [2048], P('sp'), may hold values from -6 to 6
- shift_weight: bfloat16 [2048, 2048], P('sp', 'tp'), may hold values from -0.125 to 0.125
- scale_weight: bfloat16 [2048, 2048], P('sp', 'tp'), may hold values from -0.125 to 0.125
- gate_weight: bfloat16 [2048, 2048], P('sp', 'tp'), may hold values from -0.125 to 0.125
- norm_gain: float32 [2048], replicated, may hold values from 0.1 to 1.9
- query_weight: bfloat16 [2048, 1024], P(None, 'tp'), may hold values from -0.125 to 0.125
- key_weight: bfloat16 [2048, 1024], P(None, 'tp'), may hold values from -0.125 to 0.125
- value_weight: bfloat16 [2048, 1024], P(None, 'tp'), may hold values from -0.125 to 0.125
- query_gain: float32 [64], replicated, may hold values from 0.6 to 6.5
- key_gain: float32 [64], replicated, may hold values from 0.6 to 6.5
- offset_bias: float32 [16, 15, 31], P('tp'), may hold values from 1 to 3
- out_weight: bfloat16 [1024, 2048], P('tp'), may hold values from -0.75 to 0.75
Outputs:
- mixed_rows: bfloat16 [2048, 2048], P('sp')
All inputs are finite; a program needn't handle non-finite values.
Results may differ from a plain program's by a relative error of at most 0.01405.
The roundings to bfloat16 on the way count: a program that leaves them out, or rounds other values in their place, can miss the bound.
Values may be sent and summed in bfloat16 or wider, within the bound.
No kernel may reach another device: no remote copies, remote signals or barrier semaphores. Data moves between devices by JAX's collectives and lax.ppermute only.
A program may use at most 64 MiB of HBM per device.

v0:
```python
import functools

import jax
import jax.numpy as jnp
from jax import lax
from jax.experimental import pallas as pl
from jax.experimental.pallas import tpu as pltpu
from jax.sharding import PartitionSpec as P


HEAD_DIM = 64
GRID_W = 64
WIN_ROWS = 8
WIN_COLS = 16
LANES = 128
EPS = 1e-06
MASKED = -1e30

F32 = jnp.float32
BF16 = jnp.bfloat16


def vmem(count):
    return [pl.BlockSpec(memory_space=pltpu.VMEM) for _ in range(count)]


def params(mib):
    return pltpu.CompilerParams(vmem_limit_bytes=mib << 20)


def swap(x, axis, code):
    return lax.ppermute(x, axis, [(i, i ^ code) for i in range(lax.axis_size(axis))])


def call(*args, **kwargs):
    def run(*operands):
        return pl.pallas_call(*args, **kwargs)(*operands)

    return run


def in_hbm(x):
    return pltpu.with_memory_space_constraint(x, pltpu.HBM)


def raw(count):
    return [pl.BlockSpec(memory_space=pltpu.HBM) for _ in range(count)]


def bits_of(axis):
    count = lax.axis_size(axis)
    return [1 << b for b in range(count.bit_length() - 1)]


def bt_dot(a, b):
    return lax.dot_general(a, b, (((1,), (1,)), ((), ())), preferred_element_type=F32)


def partials_body(
    cond_ref, ctx_cond_ref, shift_ref, scale_ref, gate_ref, out_ref, rows_ref, *scratch
):
    weights, sems = scratch[:3], scratch[3]
    copies = [
        pltpu.make_async_copy(cond_ref, rows_ref.at[0:1], sems.at[3]),
        pltpu.make_async_copy(ctx_cond_ref, rows_ref.at[1:2], sems.at[4]),
    ] + [
        pltpu.make_async_copy(src, dst, sems.at[n])
        for n, (src, dst) in enumerate(zip((shift_ref, scale_ref, gate_ref), weights))
    ]
    for copy in copies:
        copy.start()
    copies[0].wait()
    copies[1].wait()
    rows = rows_ref[...]
    act = (rows / (1.0 + jnp.exp(-rows))).astype(BF16)
    for n in range(3):
        copies[2 + n].wait()
        out_ref[2 * n : 2 * n + 2, :] = jnp.dot(
            act, weights[n][...], preferred_element_type=F32
        )
    out_ref[6:8, :] = jnp.zeros((2, out_ref.shape[1]), F32)


def table_body(bias_ref, out_ref):
    heads, pairs = out_ref.shape[:2]
    q = lax.broadcasted_iota(jnp.int32, (GRID_W, 2 * GRID_W), 0)
    lane = lax.broadcasted_iota(jnp.int32, (GRID_W, 2 * GRID_W), 1)
    k = lane & (GRID_W - 1)
    start = jnp.clip(q - WIN_COLS // 2, 0, GRID_W - WIN_COLS)
    is_open = (k >= start) & (k < start + WIN_COLS)
    low = lane < GRID_W
    width = 2 * GRID_W
    for h in range(heads):
        rolled = []
        for a in range(pairs + 1):
            row = jnp.broadcast_to(bias_ref[h, a : a + 1, :], (GRID_W, width))
            rolled.append(row)
        for a in range(pairs):
            first = pltpu.roll(rolled[a], (1 - WIN_COLS) % width, 1, stride=1, stride_axis=0)
            second = pltpu.roll(
                rolled[a + 1], (1 - WIN_COLS + GRID_W) % width, 1, stride=1, stride_axis=0
            )
            out_ref[h, a] = jnp.where(is_open, jnp.where(low, first, second), MASKED)


def head_norm(x, gain_row):
    cols = x.shape[1]
    r = lax.broadcasted_iota(jnp.int32, (cols, cols), 0) // HEAD_DIM
    c = lax.broadcasted_iota(jnp.int32, (cols, cols), 1) // HEAD_DIM
    same = jnp.where(r == c, 1.0 / HEAD_DIM, 0.0).astype(BF16)
    head_gain = jnp.concatenate([gain_row[...]] * (cols // HEAD_DIM), axis=1)
    square = x * x
    high = square.astype(BF16)
    rest = (square - high.astype(F32)).astype(BF16)
    mean = jnp.dot(high, same, preferred_element_type=F32) + jnp.dot(
        rest, same, preferred_element_type=F32
    )
    return x * lax.rsqrt(mean + EPS) * head_gain


def project_body(codes, n_ctx, lat_ref, *refs):
    count = len(codes)
    ctx_refs, refs = refs[:n_ctx], refs[n_ctx:]
    blocks, refs = refs[:count], refs[count:]
    gain_ref, kg_ref, wk, wv = refs[:4]
    kv_ref, ckv_ref, lat_hid_ref, gate_ref = refs[4:8]
    vec_ref, hid_ref = refs[8:]
    width = blocks[0].shape[1]
    me = lax.axis_index("tp")
    for code, block in zip(codes, blocks):
        at = pl.multiple_of((me ^ code) * width, width)
        vec_ref[:, pl.ds(at, width)] = block[...]
    gate_ref[...] = vec_ref[4:5, :]
    lat_count = lat_ref.shape[0]
    gain = gain_ref[...]

    def modulated(values, row):
        mult = gain * (1.0 + vec_ref[2 + row : 3 + row, :])
        shift = vec_ref[row : row + 1, :]
        mean = jnp.mean(values * values, axis=-1, keepdims=True)
        return (values * lax.rsqrt(mean + EPS) * mult + shift).astype(BF16)

    step = 32
    for at in range(0, lat_count, step):
        hid_ref[at : at + step, :] = modulated(lat_ref[at : at + step, :].astype(F32), 0)
    if ctx_refs[0].shape[0] % step:
        both = jnp.concatenate([c[...].astype(F32) for c in ctx_refs], axis=0)
        hid_ref[lat_count:, :] = modulated(both, 1)
    else:
        base = lat_count
        for c in ctx_refs:
            for at in range(0, c.shape[0], step):
                hid_ref[base : base + step, :] = modulated(c[at : at + step, :].astype(F32), 1)
                base += step
    cols = wk.shape[1]
    hidden = hid_ref[...]
    keys = head_norm(jnp.dot(hidden, wk[...], preferred_element_type=F32), kg_ref).astype(BF16)
    kv_ref[:, :cols] = keys[:lat_count]
    ckv_ref[:, :cols] = keys[lat_count:]
    values = jnp.dot(hidden, wv[...], preferred_element_type=F32).astype(BF16)
    kv_ref[:, cols:] = values[:lat_count]
    ckv_ref[:, cols:] = values[lat_count:]
    lat_hid_ref[...] = hidden[:lat_count]


def query_body(hid_ref, wq_ref, qg_ref, q_ref):
    queries = head_norm(
        jnp.dot(hid_ref[...], wq_ref[...], preferred_element_type=F32), qg_ref
    ).astype(BF16)
    q_ref[...] = (queries.astype(F32) * HEAD_DIM ** (-0.5)).astype(BF16)


OWN, NEAR, OTHER = range(3)


def attend_body(heads, lat_kinds, n_ctx, has_prev, is_last, q_ref, *refs):
    n_lat = len(lat_kinds)
    lat_refs, refs = refs[:n_lat], refs[n_lat:]
    ctx_refs, refs = refs[:n_ctx], refs[n_ctx:]
    if n_lat:
        table_ref, refs = refs[0], refs[1:]
    if has_prev:
        prev, refs = refs[:3], refs[3:]
    tokens, cols = q_ref.shape
    rows = tokens // GRID_W
    halo = WIN_ROWS // 2
    lane_head = lax.broadcasted_iota(jnp.int32, (1, cols), 1) // HEAD_DIM
    lane_row = lax.broadcasted_iota(jnp.int32, (1, 2 * GRID_W), 1) // GRID_W
    q_all = q_ref[...]
    parts = list(lat_refs) + list(ctx_refs)
    keys = [p[:, :cols] for p in parts]
    values = [p[:, cols:] for p in parts]
    sp_index = lax.axis_index("sp")
    first_row = sp_index * rows
    total_rows = rows * lax.axis_size("sp")
    starts = [
        jnp.clip(first_row + i - halo, 0, total_rows - WIN_ROWS) - first_row + halo
        for i in range(rows)
    ]
    is_odd = lax.rem(sp_index, 2)
    base_of = {
        OWN: halo,
        NEAR: (1 - is_odd) * (halo + rows),
        OTHER: is_odd * (halo + rows),
    }
    bases = [base_of[kind] for kind in lat_kinds]
    opens = {}
    for n in range(n_lat):
        for i in range(rows):
            for p in range(lat_refs[n].shape[0] // (2 * GRID_W)):
                row = lane_row + (bases[n] + 2 * p)
                start = starts[i]
                opens[n, i, p] = jnp.where(
                    (row >= start) & (row < start + WIN_ROWS), 0.0, MASKED
                )
    tops = jnp.zeros((tokens, cols), F32)
    sums = jnp.zeros((tokens, cols), F32)
    total = jnp.zeros((tokens, cols), F32)
    for h in range(heads):
        mine = lane_head == h
        q_h = jnp.where(mine, q_all, jnp.zeros_like(q_all))
        scores = [bt_dot(q_h, k) for k in keys]
        for n in range(n_lat):
            lines = []
            for i in range(rows):
                line = []
                for p in range(lat_refs[n].shape[0] // (2 * GRID_W)):
                    at = bases[n] + 2 * p - i + WIN_ROWS - 1 - halo
                    piece = scores[n][
                        i * GRID_W : (i + 1) * GRID_W, 2 * p * GRID_W : (2 * p + 2) * GRID_W
                    ]
                    line.append(piece + (table_ref[h, at] + opens[n, i, p]))
                lines.append(jnp.concatenate(line, axis=1))
            scores[n] = jnp.concatenate(lines, axis=0)
        top = functools.reduce(jnp.maximum, [jnp.max(s, axis=1, keepdims=True) for s in scores])
        powers = [jnp.exp(s - top) for s in scores]
        denom = functools.reduce(jnp.add, [jnp.sum(e, axis=1, keepdims=True) for e in powers])
        acc = functools.reduce(
            jnp.add,
            [
                jnp.dot(e.astype(BF16), v, preferred_element_type=F32)
                for e, v in zip(powers, values)
            ],
        )
        tops = jnp.where(mine, top, tops)
        sums = jnp.where(mine, denom, sums)
        total = jnp.where(mine, acc, total)
    if has_prev:
        before = prev[0][...]
        both = jnp.maximum(before, tops)
        old = jnp.exp(before - both)
        new = jnp.exp(tops - both)
        tops = both
        sums = prev[1][...] * old + sums * new
        total = prev[2][...] * old + total * new
    if is_last:
        refs[0][...] = (total / sums).astype(BF16)
    else:
        for ref, value in zip(refs, (tops, sums, total)):
            ref[...] = value


def first_body(count, *refs):
    att, weights, sum_ref = refs[:count], refs[count : 2 * count], refs[2 * count]
    branch = None
    for a, w in zip(att, weights):
        part = jnp.dot(a[...], w[...], preferred_element_type=F32).astype(BF16).astype(F32)
        branch = part if branch is None else branch + part
    sum_ref[...] = branch


def output_body(count, lat_ref, gate_ref, sum_ref, *refs):
    att = refs[:count]
    weights = refs[count : 2 * count]
    out_ref = refs[2 * count]
    branch = sum_ref[...]
    for a, w in zip(att, weights):
        branch = branch + jnp.dot(a[...], w[...], preferred_element_type=F32).astype(
            BF16
        ).astype(F32)
    out_ref[...] = (lat_ref[...].astype(F32) + gate_ref[...] * branch).astype(BF16)


def gather_pieces(x, axis, codes):
    pieces = [x]
    for code in codes:
        if len(pieces) > 2:
            pieces = [jnp.concatenate(pieces, axis=0)]
        pieces = pieces + [swap(p, axis, code) for p in pieces]
    return pieces


def gather_tp(x, codes):
    held = [(0, x)]
    for code in codes:
        held = held + [(had ^ code, swap(p, "tp", code)) for had, p in held]
    return held


def per_device(
    latent,
    context,
    condition,
    ctx_condition,
    shift_weight,
    scale_weight,
    gate_weight,
    norm_gain,
    query_weight,
    key_weight,
    value_weight,
    query_gain,
    key_gain,
    offset_bias,
    out_weight,
):
    sp_bits = bits_of("sp")
    tp_bits = bits_of("tp")[::-1]
    tokens, width = latent.shape
    cols = query_weight.shape[1]
    heads = cols // HEAD_DIM
    block_cols = shift_weight.shape[1]

    raw_codes = [code for code in RAW_CODES if code in sp_bits]
    ctx_parts = gather_pieces(context, "sp", raw_codes)
    part = call(
        partials_body,
        out_shape=jax.ShapeDtypeStruct((8, block_cols), F32),
        in_specs=raw(5),
        out_specs=vmem(1)[0],
        scratch_shapes=[pltpu.VMEM((2, condition.shape[0]), F32)]
        + [pltpu.VMEM(shift_weight.shape, BF16)] * 3
        + [pltpu.SemaphoreType.DMA((5,))],
        compiler_params=params(16),
        cost_estimate=pl.CostEstimate(flops=1 << 37, bytes_accessed=1 << 20, transcendentals=0),
    )(*[in_hbm(x) for x in (condition[None], ctx_condition[None], shift_weight, scale_weight, gate_weight)])
    for code in sp_bits[1:] + sp_bits[:1]:
        part = part + swap(part, "sp", code)
    vec_blocks = gather_tp(part, tp_bits)
    ow_blocks = gather_tp(out_weight, tp_bits)

    padded_bias = jnp.pad(offset_bias, ((0, 0), (0, 0), (0, LANES - offset_bias.shape[2])))
    tables = call(
        table_body,
        out_shape=jax.ShapeDtypeStruct((heads, 2 * WIN_ROWS - 2, GRID_W, 2 * GRID_W), F32),
        in_specs=vmem(1),
        out_specs=vmem(1)[0],
        compiler_params=params(16),
    )(padded_bias)

    codes = tuple(code for code, _ in vec_blocks)
    ctx_count = len(ctx_parts) * ctx_parts[0].shape[0]
    kv, ctx_kv, hidden, gate = call(
        functools.partial(project_body, codes, len(ctx_parts)),
        out_shape=(
            jax.ShapeDtypeStruct((tokens, 2 * cols), BF16),
            jax.ShapeDtypeStruct((ctx_count, 2 * cols), BF16),
            jax.ShapeDtypeStruct((tokens, width), BF16),
            jax.ShapeDtypeStruct((1, width), F32),
        ),
        in_specs=vmem(1 + len(ctx_parts) + len(codes) + 4),
        out_specs=vmem(4),
        scratch_shapes=[
            pltpu.VMEM((8, width), F32),
            pltpu.VMEM((tokens + ctx_count, width), BF16),
        ],
        compiler_params=params(20),
        cost_estimate=pl.CostEstimate(flops=1 << 37, bytes_accessed=1 << 20, transcendentals=0),
    )(
        latent,
        *ctx_parts,
        *[block for _, block in vec_blocks],
        norm_gain[None],
        key_gain[None],
        key_weight,
        value_weight,
    )
    queries = call(
        query_body,
        out_shape=jax.ShapeDtypeStruct((tokens, cols), BF16),
        in_specs=vmem(3),
        out_specs=vmem(1)[0],
        compiler_params=params(8),
    )(hidden, query_weight, query_gain[None])

    sp_count = lax.axis_size("sp")
    other_pairs = [(i, i + 1) for i in range(1, sp_count - 1, 2)]
    other_pairs += [(j, i) for i, j in other_pairs]
    near_kv = swap(kv, "sp", 1)
    other_kv = lax.ppermute(kv, "sp", other_pairs)
    ctx_pieces = gather_pieces(
        ctx_kv, "sp", [code for code in sp_bits[::-1] if code not in raw_codes]
    )

    def attend(lat, lat_kinds, ctx, prev, is_last):
        shape = (tokens, cols)
        one = jax.ShapeDtypeStruct(shape, BF16)
        three = (jax.ShapeDtypeStruct(shape, F32),) * 3
        operands = [queries, *lat, *ctx] + ([tables] if lat else []) + list(prev)
        return call(
            functools.partial(
                attend_body, heads, lat_kinds, len(ctx), bool(prev), is_last
            ),
            out_shape=one if is_last else three,
            in_specs=vmem(len(operands)),
            out_specs=vmem(1)[0] if is_last else tuple(vmem(3)),
            compiler_params=params(24),
            cost_estimate=pl.CostEstimate(
                flops=1 << 37, bytes_accessed=1 << 20, transcendentals=0
            ),
        )(*operands)

    state = attend([kv], (OWN,), ctx_pieces[:1], (), False)
    attended = attend([near_kv, other_kv], (NEAR, OTHER), ctx_pieces[1:], state, True)

    att_blocks = gather_tp(attended, tp_bits)
    near = [n for n, (code, _) in enumerate(att_blocks) if code < 2]
    far = [n for n in range(len(att_blocks)) if n not in near]
    tile = min(512, width)
    att_spec = pl.BlockSpec((tokens, cols), lambda n: (0, 0))
    weight_spec = pl.BlockSpec((cols, tile), lambda n: (0, n))
    wide_spec = pl.BlockSpec((tokens, tile), lambda n: (0, n))
    partial_sum = call(
        functools.partial(first_body, len(near)),
        grid=(width // tile,),
        out_shape=jax.ShapeDtypeStruct((tokens, width), F32),
        in_specs=[att_spec] * len(near) + [weight_spec] * len(near),
        out_specs=wide_spec,
        compiler_params=params(24),
    )(*[att_blocks[n][1] for n in near], *[ow_blocks[n][1] for n in near])
    return call(
        functools.partial(output_body, len(far)),
        grid=(width // tile,),
        out_shape=jax.ShapeDtypeStruct((tokens, width), BF16),
        in_specs=[wide_spec, pl.BlockSpec((1, tile), lambda n: (0, n)), wide_spec]
        + [att_spec] * len(far)
        + [weight_spec] * len(far),
        out_specs=wide_spec,
        compiler_params=params(24),
    )(
        latent,
        gate,
        partial_sum,
        *[att_blocks[n][1] for n in far],
        *[ow_blocks[n][1] for n in far],
    )


RAW_CODES = (1,)


def solution(mesh):
    in_specs = (
        P("sp", None),
        P("sp", None),
        P("sp"),
        P("sp"),
        P("sp", "tp"),
        P("sp", "tp"),
        P("sp", "tp"),
        P(),
        P(None, "tp"),
        P(None, "tp"),
        P(None, "tp"),
        P(),
        P(),
        P("tp", None, None),
        P("tp", None),
    )
    out_specs = P("sp", None)
    return jax.shard_map(
        per_device, mesh=mesh, in_specs=in_specs, out_specs=out_specs, check_vma=False
    )
```

profile of v0, /device:TPU:0, one launch (start us, length us, event | category | flops | bytes accessed | tf_op | source)
XLA Modules:
  0.0 64.3 jit_solution(11331410556523546040)
XLA Ops:
  0.0 3.0 %collective-permute-start = (bf16[64,2048]{1,0:T(8,128)(2,1)}, bf16[64,2048]{1,0:T(8,128)(2,1)S(1)}, u32[]{:S(2)}, u32[]{:S(2)}) collective-permute-start(bf16[64,2048]{1,0:T(8,128)(2,1)} %refs_0_.1), channel_id=1, source_target_pairs={{0,4},{4,0},{8,12},{12,8},{16,20},{20,16},{24,28},{28,24},{1,5},{5... | collective-permute-start | bytes 786440 | tf_op jit(solution)/shard_map/ppermute | solution.py:32
  3.0 1.6 %shard_map.145 = f32[8,512]{1,0:T(8,128)S(1)} custom-call(f32[1,256]{1,0:T(1,128)} %bitcast.8, f32[1,256]{1,0:T(1,128)} %bitcast.9, bf16[256,512]{1,0:T(8,128)(2,1)} %shift_ref.1, bf16[256,512]{1,0:T(8,128)(2,1)} %scale_ref.1, bf16[256,512]{1,0:T(8,128)(2,1)} %gate_ref.1), custom_call_target="tpu_custom_call" | custom-call | flops 137438953472 | bytes 1048576 | tf_op jit(solution)/shard_map/pallas_call | solution.py:37
  4.7 1.6 %collective-permute-start.1 = (f32[8,512]{1,0:T(8,128)S(1)}, f32[8,512]{1,0:T(8,128)S(1)}, u32[]{:S(2)}, u32[]{:S(2)}) collective-permute-start(f32[8,512]{1,0:T(8,128)S(1)} %shard_map.145), channel_id=1, source_target_pairs={{0,8},{4,12},{8,0},{12,4},{16,24},{20,28},{24,16},{28,20},{1,9},{5... | collective-permute-start | bytes 49160 | tf_op jit(solution)/shard_map/ppermute | solution.py:32
  6.3 2.2 %collective-permute-done.1 = f32[8,512]{1,0:T(8,128)S(1)} collective-permute-done((f32[8,512]{1,0:T(8,128)S(1)}, f32[8,512]{1,0:T(8,128)S(1)}, u32[]{:S(2)}, u32[]{:S(2)}) %collective-permute-start.1) | collective-permute-done | bytes 16416 | tf_op jit(solution)/shard_map/ppermute | solution.py:32
  8.5 2.6 %collective-permute-start.2 = (f32[8,512]{1,0:T(8,128)S(1)}, f32[8,512]{1,0:T(8,128)S(1)}, u32[]{:S(2)}, u32[]{:S(2)}) collective-permute-start(f32[8,512]{1,0:T(8,128)S(1)} %add.11), channel_id=1, source_target_pairs={{0,16},{4,20},{8,24},{12,28},{16,0},{20,4},{24,8},{28,12},{1,17},{... | collective-permute-start | bytes 49160 | tf_op jit(solution)/shard_map/ppermute | solution.py:32
  11.1 2.0 %collective-permute-done.2 = f32[8,512]{1,0:T(8,128)S(1)} collective-permute-done((f32[8,512]{1,0:T(8,128)S(1)}, f32[8,512]{1,0:T(8,128)S(1)}, u32[]{:S(2)}, u32[]{:S(2)}) %collective-permute-start.2) | collective-permute-done | bytes 16416 | tf_op jit(solution)/shard_map/ppermute | solution.py:32
  13.1 0.2 collective-permute-start.3
  13.3 3.6 %collective-permute-done.3 = f32[8,512]{1,0:T(8,128)S(1)} collective-permute-done((f32[8,512]{1,0:T(8,128)S(1)}, f32[8,512]{1,0:T(8,128)S(1)}, u32[]{:S(2)}, u32[]{:S(2)}) %collective-permute-start.3) | collective-permute-done | bytes 16416 | tf_op jit(solution)/shard_map/ppermute | solution.py:32
  16.9 1.5 %collective-permute-start.4 = (f32[8,512]{1,0:T(8,128)S(1)}, f32[8,512]{1,0:T(8,128)S(1)}, u32[]{:S(2)}, u32[]{:S(2)}) collective-permute-start(f32[8,512]{1,0:T(8,128)S(1)} %add.13.refs_2_), channel_id=1, source_target_pairs={{0,2},{1,3},{2,0},{3,1},{4,6},{5,7},{6,4},{7,5},{8,10},{9,11},{10,... | collective-permute-start | bytes 49160 | tf_op jit(solution)/shard_map/ppermute | solution.py:32
  18.4 2.2 %collective-permute-done.4.refs_3_ = f32[8,512]{1,0:T(8,128)S(1)} collective-permute-done((f32[8,512]{1,0:T(8,128)S(1)}, f32[8,512]{1,0:T(8,128)S(1)}, u32[]{:S(2)}, u32[]{:S(2)}) %collective-permute-start.4) | collective-permute-done | bytes 16416 | tf_op jit(solution)/shard_map/ppermute | solution.py:32
  20.6 1.2 %collective-permute-done.6.refs_5_ = f32[8,512]{1,0:T(8,128)S(1)} collective-permute-done((f32[8,512]{1,0:T(8,128)S(1)}, f32[8,512]{1,0:T(8,128)S(1)}, u32[]{:S(2)}, u32[]{:S(2)}) %collective-permute-start.6) | collective-permute-done | bytes 16416 | tf_op jit(solution)/shard_map/ppermute | solution.py:32
  21.8 0.0 copy-start
  21.8 0.0 copy-start.10
  21.9 2.2 %shard_map.146 = (bf16[256,512]{1,0:T(8,128)(2,1)S(1)}, bf16[128,512]{1,0:T(8,128)(2,1)S(1)}, bf16[256,2048]{1,0:T(8,128)(2,1)S(1)}, f32[1,2048]{1,0:T(1,128)S(1)}) custom-call(bf16[256,2048]{1,0:T(8,128)(2,1)S(1)} %copy-done.1, bf16[64,2048]{1,0:T(8,128)(2,1)S(1)} %copy-done.7, bf16[64,2048]{1,0:T(8,128)(2,1)S(1)} %collective-permute-done.refs_1_, ...), custom_call_target="tpu_custom_call" | custom-call | flops 137438953472 | bytes 1048576 | tf_op jit(solution)/shard_map/pallas_call | solution.py:37
  24.1 2.7 %collective-permute-start.9 = (bf16[128,512]{1,0:T(8,128)(2,1)S(1)}, bf16[128,512]{1,0:T(8,128)(2,1)S(1)}, u32[]{:S(2)}, u32[]{:S(2)}) collective-permute-start(bf16[128,512]{1,0:T(8,128)(2,1)S(1)} %get-tuple-element.15.refs_1_), channel_id=1, source_target_pairs={{0,16},{4,20},{8,24},{12,28},{16,0},{20,4},{24,8},{28,12},{1,17},{... | collective-permute-start | bytes 393224 | tf_op jit(solution)/shard_map/ppermute | solution.py:32
  26.8 1.5 %collective-permute-start.16 = (bf16[256,2048]{1,0:T(8,128)(2,1)S(1)}, bf16[256,2048]{1,0:T(8,128)(2,1)S(1)}, u32[]{:S(2)}, u32[]{:S(2)}) collective-permute-start(bf16[256,2048]{1,0:T(8,128)(2,1)S(1)} %copy-done), channel_id=1, source_target_pairs={{0,2},{1,3},{2,0},{3,1},{4,6},{5,7},{6,4},{7,5},{8,10},{9,11},{10,... | collective-permute-start | bytes 3145736 | tf_op jit(solution)/shard_map/ppermute | solution.py:32
  28.3 1.0 %shard_map.148.refs_2_.refs_5_ = f32[4,14,64,128]{3,2,1,0:T(8,128)S(1)} custom-call(f32[4,15,128]{2,1,0:T(8,128)S(1)} %pad.4.bias_ref), custom_call_target="tpu_custom_call" | custom-call | tf_op jit(solution)/shard_map/pallas_call | solution.py:37
  29.3 0.6 collective-permute-start.7
  29.9 0.7 %collective-permute-start.8 = (bf16[256,512]{1,0:T(8,128)(2,1)S(1)}, bf16[256,512]{1,0:T(8,128)(2,1)S(1)}, u32[]{:S(2)}, u32[]{:S(2)}) collective-permute-start(bf16[256,512]{1,0:T(8,128)(2,1)S(1)} %get-tuple-element.14.refs_0_), channel_id=1, source_target_pairs={{4,8},{12,16},{20,24},{8,4},{16,12},{24,20},{5,9},{13,17},{21,25},... | collective-permute-start | bytes 786440 | tf_op jit(solution)/shard_map/ppermute | solution.py:390
  30.6 4.3 %collective-permute-start.10 = (bf16[128,512]{1,0:T(8,128)(2,1)S(1)}, bf16[128,512]{1,0:T(8,128)(2,1)S(1)}, u32[]{:S(2)}, u32[]{:S(2)}) collective-permute-start(bf16[128,512]{1,0:T(8,128)(2,1)S(1)} %get-tuple-element.15.refs_1_), channel_id=1, source_target_pairs={{0,8},{4,12},{8,0},{12,4},{16,24},{20,28},{24,16},{28,20},{1,9},{5... | collective-permute-start | bytes 393224 | tf_op jit(solution)/shard_map/ppermute | solution.py:32
  34.9 0.7 %shard_map.147.q_ref = bf16[256,256]{1,0:T(8,128)(2,1)S(1)} custom-call(bf16[256,2048]{1,0:T(8,128)(2,1)S(1)} %get-tuple-element.13.hid_ref, bf16[2048,256]{1,0:T(8,128)(2,1)S(1)} %copy-done.3, f32[1,64]{1,0:T(1,128)S(1)} %bitcast.5), custom_call_target="tpu_custom_call" | custom-call | tf_op jit(solution)/shard_map/pallas_call | solution.py:37
  35.6 0.1 collective-permute-start.11
  35.7 1.0 %shard_map.149 = (f32[256,256]{1,0:T(8,128)S(1)}, f32[256,256]{1,0:T(8,128)S(1)}, f32[256,256]{1,0:T(8,128)S(1)}) custom-call(bf16[256,256]{1,0:T(8,128)(2,1)S(1)} %shard_map.147.q_ref, bf16[256,512]{1,0:T(8,128)(2,1)S(1)} %get-tuple-element.14.refs_0_, bf16[128,512]{1,0:T(8,128)(2,1)S(1)} %get-tuple-element.15.refs_1_, ...), custom_call_target="tpu_custom_call" | custom-call | flops 137438953472 | bytes 1048576 | tf_op jit(solution)/shard_map/pallas_call | solution.py:37
  36.7 7.9 %collective-permute-done.10.refs_3_ = bf16[128,512]{1,0:T(8,128)(2,1)S(1)} collective-permute-done((bf16[128,512]{1,0:T(8,128)(2,1)S(1)}, bf16[128,512]{1,0:T(8,128)(2,1)S(1)}, u32[]{:S(2)}, u32[]{:S(2)}) %collective-permute-start.10) | collective-permute-done | bytes 131104 | tf_op jit(solution)/shard_map/ppermute | solution.py:32
  44.5 7.2 %collective-permute-done.16.refs_2_ = bf16[256,2048]{1,0:T(8,128)(2,1)S(1)} collective-permute-done((bf16[256,2048]{1,0:T(8,128)(2,1)S(1)}, bf16[256,2048]{1,0:T(8,128)(2,1)S(1)}, u32[]{:S(2)}, u32[]{:S(2)}) %collective-permute-start.16) | collective-permute-done | bytes 1048608 | tf_op jit(solution)/shard_map/ppermute | solution.py:32
  51.8 2.1 %shard_map.150.refs_0_ = bf16[256,256]{1,0:T(8,128)(2,1)S(1)} custom-call(bf16[256,256]{1,0:T(8,128)(2,1)S(1)} %shard_map.147.q_ref, bf16[256,512]{1,0:T(8,128)(2,1)S(1)} %collective-permute-done.7.refs_0_, bf16[256,512]{1,0:T(8,128)(2,1)S(1)} %collective-permute-done.8.refs_1_, bf16[128,512]{1,0:T(8,128)(2,1)S(1)} %collective-permute-done.9.refs_2_, ...), custom_call_target="tpu_custom_call" | custom-call | flops 137438953472 | bytes 1048576 | tf_op jit(solution)/shard_map/pallas_call | solution.py:37
  53.9 0.0 copy-start.2
  53.9 1.6 %collective-permute-start.14 = (bf16[256,256]{1,0:T(8,128)(2,1)S(1)}, bf16[256,256]{1,0:T(8,128)(2,1)S(1)}, u32[]{:S(2)}, u32[]{:S(2)}) collective-permute-start(bf16[256,256]{1,0:T(8,128)(2,1)S(1)} %shard_map.150.refs_0_), channel_id=1, source_target_pairs={{0,2},{1,3},{2,0},{3,1},{4,6},{5,7},{6,4},{7,5},{8,10},{9,11},{10,... | collective-permute-start | bytes 393224 | tf_op jit(solution)/shard_map/ppermute | solution.py:32
  55.5 0.2 collective-permute-start.12
  55.7 4.2 %collective-permute-done.14.refs_0_ = bf16[256,256]{1,0:T(8,128)(2,1)S(1)} collective-permute-done((bf16[256,256]{1,0:T(8,128)(2,1)S(1)}, bf16[256,256]{1,0:T(8,128)(2,1)S(1)}, u32[]{:S(2)}, u32[]{:S(2)}) %collective-permute-start.14) | collective-permute-done | bytes 131104 | tf_op jit(solution)/shard_map/ppermute | solution.py:32
  59.9 1.6 %shard_map.151.sum_ref = f32[256,2048]{1,0:T(8,128)S(1)} custom-call(bf16[256,256]{1,0:T(8,128)(2,1)S(1)} %shard_map.150.refs_0_, bf16[256,256]{1,0:T(8,128)(2,1)S(1)} %collective-permute-done.12.refs_1_, bf16[256,2048]{1,0:T(8,128)(2,1)S(1)} %copy-done, bf16[256,2048]{1,0:T(8,128)(2,1)S(1)} %collective-permute-done.13.refs_3_), custom_call_target="tpu_custom_call" | custom-call | tf_op jit(solution)/shard_map/pallas_call | solution.py:37
  61.5 2.8 %shard_map.152 = bf16[256,2048]{1,0:T(8,128)(2,1)} custom-call(bf16[256,2048]{1,0:T(8,128)(2,1)S(1)} %copy-done.2, f32[1,2048]{1,0:T(1,128)S(1)} %get-tuple-element.12.gate_ref, f32[256,2048]{1,0:T(8,128)S(1)} %shard_map.151.sum_ref, bf16[256,256]{1,0:T(8,128)(2,1)S(1)} %collective-permute-done.14.refs_0_, ...), custom_call_target="tpu_custom_call" | custom-call | tf_op jit(solution)/shard_map/pallas_call | solution.py:37
  (39 shorter events, 0.1 us)
Async XLA Ops:
  0.0 21.8 %collective-permute-start = (bf16[64,2048]{1,0:T(8,128)(2,1)}, bf16[64,2048]{1,0:T(8,128)(2,1)S(1)}, u32[]{:S(2)}, u32[]{:S(2)}) collective-permute-start(bf16[64,2048]{1,0:T(8,128)(2,1)} %refs_0_.1), channel_id=1, source_target_pairs={{0,4},{4,0},{8,12},{12,8},{16,20},{20,16},{24,28},{28,24},{1,5},{5... | collective-permute-start | bytes 786440 | tf_op jit(solution)/shard_map/ppermute | solution.py:32
  3.0 18.8 %copy-start.1 = (bf16[256,2048]{1,0:T(8,128)(2,1)S(1)}, bf16[256,2048]{1,0:T(8,128)(2,1)}, u32[]{:S(2)}) copy-start(bf16[256,2048]{1,0:T(8,128)(2,1)} %lat_ref.3) | copy-start | bytes 3145732
  3.0 18.8 %copy-start.5 = (bf16[2048,256]{1,0:T(8,128)(2,1)S(1)}, bf16[2048,256]{1,0:T(8,128)(2,1)}, u32[]{:S(2)}) copy-start(bf16[2048,256]{1,0:T(8,128)(2,1)} %refs_8_.1) | copy-start | bytes 3145732
  3.0 18.8 %copy-start.6 = (bf16[2048,256]{1,0:T(8,128)(2,1)S(1)}, bf16[2048,256]{1,0:T(8,128)(2,1)}, u32[]{:S(2)}) copy-start(bf16[2048,256]{1,0:T(8,128)(2,1)} %refs_9_.1) | copy-start | bytes 3145732
  3.0 18.8 %copy-start.7 = (bf16[64,2048]{1,0:T(8,128)(2,1)S(1)}, bf16[64,2048]{1,0:T(8,128)(2,1)}, u32[]{:S(2)}) copy-start(bf16[64,2048]{1,0:T(8,128)(2,1)} %refs_0_.1) | copy-start | bytes 786436
  3.0 18.8 %copy-start.8 = (f32[2048]{0:T(1024)S(1)}, f32[2048]{0:T(1024)}, u32[]{:S(2)}) copy-start(f32[2048]{0:T(1024)} %param.22) | copy-start | bytes 24580
  3.0 18.8 %copy-start.9 = (f32[64]{0:T(128)S(1)}, f32[64]{0:T(128)}, u32[]{:S(2)}) copy-start(f32[64]{0:T(128)} %param.27) | copy-start | bytes 772
  4.7 3.8 %collective-permute-start.1 = (f32[8,512]{1,0:T(8,128)S(1)}, f32[8,512]{1,0:T(8,128)S(1)}, u32[]{:S(2)}, u32[]{:S(2)}) collective-permute-start(f32[8,512]{1,0:T(8,128)S(1)} %shard_map.145), channel_id=1, source_target_pairs={{0,8},{4,12},{8,0},{12,4},{16,24},{20,28},{24,16},{28,20},{1,9},{5... | collective-permute-start | bytes 49160 | tf_op jit(solution)/shard_map/ppermute | solution.py:32
  8.5 4.6 %collective-permute-start.2 = (f32[8,512]{1,0:T(8,128)S(1)}, f32[8,512]{1,0:T(8,128)S(1)}, u32[]{:S(2)}, u32[]{:S(2)}) collective-permute-start(f32[8,512]{1,0:T(8,128)S(1)} %add.11), channel_id=1, source_target_pairs={{0,16},{4,20},{8,24},{12,28},{16,0},{20,4},{24,8},{28,12},{1,17},{... | collective-permute-start | bytes 49160 | tf_op jit(solution)/shard_map/ppermute | solution.py:32
  13.1 3.7 %collective-permute-start.3 = (f32[8,512]{1,0:T(8,128)S(1)}, f32[8,512]{1,0:T(8,128)S(1)}, u32[]{:S(2)}, u32[]{:S(2)}) collective-permute-start(f32[8,512]{1,0:T(8,128)S(1)} %add.12), channel_id=1, source_target_pairs={{0,4},{4,0},{8,12},{12,8},{16,20},{20,16},{24,28},{28,24},{1,5},{5... | collective-permute-start | bytes 49160 | tf_op jit(solution)/shard_map/ppermute | solution.py:32
  16.9 3.7 %collective-permute-start.4 = (f32[8,512]{1,0:T(8,128)S(1)}, f32[8,512]{1,0:T(8,128)S(1)}, u32[]{:S(2)}, u32[]{:S(2)}) collective-permute-start(f32[8,512]{1,0:T(8,128)S(1)} %add.13.refs_2_), channel_id=1, source_target_pairs={{0,2},{1,3},{2,0},{3,1},{4,6},{5,7},{6,4},{7,5},{8,10},{9,11},{10,... | collective-permute-start | bytes 49160 | tf_op jit(solution)/shard_map/ppermute | solution.py:32
  18.4 2.3 %collective-permute-start.5 = (f32[8,512]{1,0:T(8,128)S(1)}, f32[8,512]{1,0:T(8,128)S(1)}, u32[]{:S(2)}, u32[]{:S(2)}) collective-permute-start(f32[8,512]{1,0:T(8,128)S(1)} %add.13.refs_2_), channel_id=1, source_target_pairs={{0,1},{1,0},{2,3},{3,2},{4,5},{5,4},{6,7},{7,6},{8,9},{9,8},{10,11... | collective-permute-start | bytes 49160 | tf_op jit(solution)/shard_map/ppermute | solution.py:32
  20.6 1.2 %collective-permute-start.6 = (f32[8,512]{1,0:T(8,128)S(1)}, f32[8,512]{1,0:T(8,128)S(1)}, u32[]{:S(2)}, u32[]{:S(2)}) collective-permute-start(f32[8,512]{1,0:T(8,128)S(1)} %collective-permute-done.4.refs_3_), channel_id=1, source_target_pairs={{0,1},{1,0},{2,3},{3,2},{4,5},{5,4},{6,7},{7,6},{8,9},{9,8},{10,11... | collective-permute-start | bytes 49160 | tf_op jit(solution)/shard_map/ppermute | solution.py:32
  21.8 5.0 %copy-start = (bf16[256,2048]{1,0:T(8,128)(2,1)S(1)}, bf16[256,2048]{1,0:T(8,128)(2,1)}, u32[]{:S(2)}) copy-start(bf16[256,2048]{1,0:T(8,128)(2,1)} %refs_2_.1) | copy-start | bytes 3145732
  21.8 6.4 %copy-start.10 = (f32[4,15,31]{2,0,1:T(4,128)S(1)}, f32[4,15,31]{2,0,1:T(4,128)}, u32[]{:S(2)}) copy-start(f32[4,15,31]{2,0,1:T(4,128)} %param.28) | copy-start | bytes 22324
  21.9 13.0 %copy-start.4 = (f32[64]{0:T(128)S(1)}, f32[64]{0:T(128)}, u32[]{:S(2)}) copy-start(f32[64]{0:T(128)} %param.26) | copy-start | bytes 772
  24.1 10.7 %copy-start.3 = (bf16[2048,256]{1,0:T(8,128)(2,1)S(1)}, bf16[2048,256]{1,0:T(8,128)(2,1)}, u32[]{:S(2)}) copy-start(bf16[2048,256]{1,0:T(8,128)(2,1)} %wq_ref.1) | copy-start | bytes 3145732
  24.1 11.4 %collective-permute-start.9 = (bf16[128,512]{1,0:T(8,128)(2,1)S(1)}, bf16[128,512]{1,0:T(8,128)(2,1)S(1)}, u32[]{:S(2)}, u32[]{:S(2)}) collective-permute-start(bf16[128,512]{1,0:T(8,128)(2,1)S(1)} %get-tuple-element.15.refs_1_), channel_id=1, source_target_pairs={{0,16},{4,20},{8,24},{12,28},{16,0},{20,4},{24,8},{28,12},{1,17},{... | collective-permute-start | bytes 393224 | tf_op jit(solution)/shard_map/ppermute | solution.py:32
  26.8 24.9 %collective-permute-start.16 = (bf16[256,2048]{1,0:T(8,128)(2,1)S(1)}, bf16[256,2048]{1,0:T(8,128)(2,1)S(1)}, u32[]{:S(2)}, u32[]{:S(2)}) collective-permute-start(bf16[256,2048]{1,0:T(8,128)(2,1)S(1)} %copy-done), channel_id=1, source_target_pairs={{0,2},{1,3},{2,0},{3,1},{4,6},{5,7},{6,4},{7,5},{8,10},{9,11},{10,... | collective-permute-start | bytes 3145736 | tf_op jit(solution)/shard_map/ppermute | solution.py:32
  29.3 22.4 %collective-permute-start.7 = (bf16[256,512]{1,0:T(8,128)(2,1)S(1)}, bf16[256,512]{1,0:T(8,128)(2,1)S(1)}, u32[]{:S(2)}, u32[]{:S(2)}) collective-permute-start(bf16[256,512]{1,0:T(8,128)(2,1)S(1)} %get-tuple-element.14.refs_0_), channel_id=1, source_target_pairs={{0,4},{4,0},{8,12},{12,8},{16,20},{20,16},{24,28},{28,24},{1,5},{5... | collective-permute-start | bytes 786440 | tf_op jit(solution)/shard_map/ppermute | solution.py:32
  29.9 21.9 %collective-permute-start.8 = (bf16[256,512]{1,0:T(8,128)(2,1)S(1)}, bf16[256,512]{1,0:T(8,128)(2,1)S(1)}, u32[]{:S(2)}, u32[]{:S(2)}) collective-permute-start(bf16[256,512]{1,0:T(8,128)(2,1)S(1)} %get-tuple-element.14.refs_0_), channel_id=1, source_target_pairs={{4,8},{12,16},{20,24},{8,4},{16,12},{24,20},{5,9},{13,17},{21,25},... | collective-permute-start | bytes 786440 | tf_op jit(solution)/shard_map/ppermute | solution.py:390
  30.6 14.0 %collective-permute-start.10 = (bf16[128,512]{1,0:T(8,128)(2,1)S(1)}, bf16[128,512]{1,0:T(8,128)(2,1)S(1)}, u32[]{:S(2)}, u32[]{:S(2)}) collective-permute-start(bf16[128,512]{1,0:T(8,128)(2,1)S(1)} %get-tuple-element.15.refs_1_), channel_id=1, source_target_pairs={{0,8},{4,12},{8,0},{12,4},{16,24},{20,28},{24,16},{28,20},{1,9},{5... | collective-permute-start | bytes 393224 | tf_op jit(solution)/shard_map/ppermute | solution.py:32
  35.6 16.2 %collective-permute-start.11 = (bf16[128,512]{1,0:T(8,128)(2,1)S(1)}, bf16[128,512]{1,0:T(8,128)(2,1)S(1)}, u32[]{:S(2)}, u32[]{:S(2)}) collective-permute-start(bf16[128,512]{1,0:T(8,128)(2,1)S(1)} %collective-permute-done.9.refs_2_), channel_id=1, source_target_pairs={{0,8},{4,12},{8,0},{12,4},{16,24},{20,28},{24,16},{28,20},{1,9},{5... | collective-permute-start | bytes 393224 | tf_op jit(solution)/shard_map/ppermute | solution.py:32
  44.5 15.4 %collective-permute-start.13 = (bf16[256,2048]{1,0:T(8,128)(2,1)S(1)}, bf16[256,2048]{1,0:T(8,128)(2,1)S(1)}, u32[]{:S(2)}, u32[]{:S(2)}) collective-permute-start(bf16[256,2048]{1,0:T(8,128)(2,1)S(1)} %copy-done), channel_id=1, source_target_pairs={{0,1},{1,0},{2,3},{3,2},{4,5},{5,4},{6,7},{7,6},{8,9},{9,8},{10,11... | collective-permute-start | bytes 3145736 | tf_op jit(solution)/shard_map/ppermute | solution.py:32
  51.7 9.7 %collective-permute-start.17 = (bf16[256,2048]{1,0:T(8,128)(2,1)S(1)}, bf16[256,2048]{1,0:T(8,128)(2,1)S(1)}, u32[]{:S(2)}, u32[]{:S(2)}) collective-permute-start(bf16[256,2048]{1,0:T(8,128)(2,1)S(1)} %collective-permute-done.16.refs_2_), channel_id=1, source_target_pairs={{0,1},{1,0},{2,3},{3,2},{4,5},{5,4},{6,7},{7,6},{8,9},{9,8},{10,11... | collective-permute-start | bytes 3145736 | tf_op jit(solution)/shard_map/ppermute | solution.py:32
  53.9 7.6 %copy-start.2 = (bf16[256,2048]{1,0:T(8,128)(2,1)S(1)}, bf16[256,2048]{1,0:T(8,128)(2,1)}, u32[]{:S(2)}) copy-start(bf16[256,2048]{1,0:T(8,128)(2,1)} %lat_ref.3) | copy-start | bytes 3145732
  53.9 6.0 %collective-permute-start.14 = (bf16[256,256]{1,0:T(8,128)(2,1)S(1)}, bf16[256,256]{1,0:T(8,128)(2,1)S(1)}, u32[]{:S(2)}, u32[]{:S(2)}) collective-permute-start(bf16[256,256]{1,0:T(8,128)(2,1)S(1)} %shard_map.150.refs_0_), channel_id=1, source_target_pairs={{0,2},{1,3},{2,0},{3,1},{4,6},{5,7},{6,4},{7,5},{8,10},{9,11},{10,... | collective-permute-start | bytes 393224 | tf_op jit(solution)/shard_map/ppermute | solution.py:32
  55.5 4.4 %collective-permute-start.12 = (bf16[256,256]{1,0:T(8,128)(2,1)S(1)}, bf16[256,256]{1,0:T(8,128)(2,1)S(1)}, u32[]{:S(2)}, u32[]{:S(2)}) collective-permute-start(bf16[256,256]{1,0:T(8,128)(2,1)S(1)} %shard_map.150.refs_0_), channel_id=1, source_target_pairs={{0,1},{1,0},{2,3},{3,2},{4,5},{5,4},{6,7},{7,6},{8,9},{9,8},{10,11... | collective-permute-start | bytes 393224 | tf_op jit(solution)/shard_map/ppermute | solution.py:32
  59.9 1.6 %collective-permute-start.15 = (bf16[256,256]{1,0:T(8,128)(2,1)S(1)}, bf16[256,256]{1,0:T(8,128)(2,1)S(1)}, u32[]{:S(2)}, u32[]{:S(2)}) collective-permute-start(bf16[256,256]{1,0:T(8,128)(2,1)S(1)} %collective-permute-done.14.refs_0_), channel_id=1, source_target_pairs={{0,1},{1,0},{2,3},{3,2},{4,5},{5,4},{6,7},{7,6},{8,9},{9,8},{10,11... | collective-permute-start | bytes 393224 | tf_op jit(solution)/shard_map/ppermute | solution.py:32
where the time goes:
time: 64.4 us; the launch traced here: 64.3 us
  waiting for transfers between devices  30.5 us (47%)
  starting transfers between devices  20.4 us (32%)
  Pallas kernels  13 us (20%)
    ppermute x17, waiting for transfers between devices, swap(): lax.ppermute(x, axis, [(i, i ^ code) for i in range(lax.axis_size(axis))])  30.5 us
    ppermute x17, starting transfers between devices, swap(): lax.ppermute(x, axis, [(i, i ^ code) for i in range(lax.axis_size(axis))])  19.8 us
    pallas_call x8, Pallas kernels, run(): return pl.pallas_call(*args, **kwargs)(*operands)  13 us
  transfers between devices with their start and end apart: 18, of which 8 were waited for; matrix products, arithmetic and copies ran while one was open for 0% of the time, Pallas kernels for 12%

commit v1 on v0

--- a/solution.py
+++ b/solution.py
@@ -119,17 +119,17 @@
 
 
 def project_body(codes, n_ctx, lat_ref, *refs):
-    count = len(codes)
     ctx_refs, refs = refs[:n_ctx], refs[n_ctx:]
-    blocks, refs = refs[:count], refs[count:]
+    part_ref, beside_ref, refs = refs[0], refs[1], refs[2:]
     gain_ref, kg_ref, wk, wv = refs[:4]
     kv_ref, ckv_ref, lat_hid_ref, gate_ref = refs[4:8]
     vec_ref, hid_ref = refs[8:]
-    width = blocks[0].shape[1]
+    width = part_ref.shape[1]
     me = lax.axis_index("tp")
-    for code, block in zip(codes, blocks):
-        at = pl.multiple_of((me ^ code) * width, width)
-        vec_ref[:, pl.ds(at, width)] = block[...]
+    for n, code in enumerate(codes):
+        for ref, flip in ((part_ref, 0), (beside_ref, 1)):
+            at = pl.multiple_of((me ^ code ^ flip) * width, width)
+            vec_ref[:, pl.ds(at, width)] = ref[8 * n : 8 * n + 8, :]
     gate_ref[...] = vec_ref[4:5, :]
     lat_count = lat_ref.shape[0]
     gain = gain_ref[...]
@@ -260,6 +260,19 @@
             ref[...] = value
 
 
+def stash_body(*refs):
+    count = len(refs) // 2
+    sems = refs[-1]
+    copies = [
+        pltpu.make_async_copy(src, dst, sems.at[n])
+        for n, (src, dst) in enumerate(zip(refs[:count], refs[count : 2 * count]))
+    ]
+    for copy in copies:
+        copy.start()
+    for copy in copies:
+        copy.wait()
+
+
 def first_body(count, *refs):
     att, weights, sum_ref = refs[:count], refs[count : 2 * count], refs[2 * count]
     branch = None
@@ -334,9 +347,14 @@
         compiler_params=params(16),
         cost_estimate=pl.CostEstimate(flops=1 << 37, bytes_accessed=1 << 20, transcendentals=0),
     )(*[in_hbm(x) for x in (condition[None], ctx_condition[None], shift_weight, scale_weight, gate_weight)])
+    codes = [0]
+    for code in tp_bits:
+        if code > 1:
+            part = jnp.concatenate([part, swap(part, "tp", code)], axis=0)
+            codes = codes + [had ^ code for had in codes]
     for code in sp_bits[1:] + sp_bits[:1]:
         part = part + swap(part, "sp", code)
-    vec_blocks = gather_tp(part, tp_bits)
+    beside = swap(part, "tp", 1)
     ow_blocks = gather_tp(out_weight, tp_bits)
 
     padded_bias = jnp.pad(offset_bias, ((0, 0), (0, 0), (0, LANES - offset_bias.shape[2])))
@@ -348,17 +366,16 @@
         compiler_params=params(16),
     )(padded_bias)
 
-    codes = tuple(code for code, _ in vec_blocks)
     ctx_count = len(ctx_parts) * ctx_parts[0].shape[0]
     kv, ctx_kv, hidden, gate = call(
-        functools.partial(project_body, codes, len(ctx_parts)),
+        functools.partial(project_body, tuple(codes), len(ctx_parts)),
         out_shape=(
             jax.ShapeDtypeStruct((tokens, 2 * cols), BF16),
             jax.ShapeDtypeStruct((ctx_count, 2 * cols), BF16),
             jax.ShapeDtypeStruct((tokens, width), BF16),
             jax.ShapeDtypeStruct((1, width), F32),
         ),
-        in_specs=vmem(1 + len(ctx_parts) + len(codes) + 4),
+        in_specs=vmem(1 + len(ctx_parts) + 2 + 4),
         out_specs=vmem(4),
         scratch_shapes=[
             pltpu.VMEM((8, width), F32),
@@ -369,7 +386,8 @@
     )(
         latent,
         *ctx_parts,
-        *[block for _, block in vec_blocks],
+        part,
+        beside,
         norm_gain[None],
         key_gain[None],
         key_weight,
@@ -420,6 +438,17 @@
     att_spec = pl.BlockSpec((tokens, cols), lambda n: (0, 0))
     weight_spec = pl.BlockSpec((cols, tile), lambda n: (0, n))
     wide_spec = pl.BlockSpec((tokens, tile), lambda n: (0, n))
+    kept = [n for n, (code, _) in enumerate(ow_blocks) if code in (0, 1) + tuple(code for code in tp_bits if code > 1)]
+    stashed = call(
+        stash_body,
+        out_shape=tuple(jax.ShapeDtypeStruct((cols, width), BF16) for _ in kept),
+        in_specs=raw(len(kept)),
+        out_specs=tuple(vmem(len(kept))),
+        scratch_shapes=[pltpu.SemaphoreType.DMA((len(kept),))],
+        compiler_params=params(8),
+    )(*[in_hbm(ow_blocks[n][1]) for n in kept])
+    for n, w in zip(kept, stashed):
+        ow_blocks[n] = (ow_blocks[n][0], w)
     partial_sum = call(
         functools.partial(first_body, len(near)),
         grid=(width // tile,),

time: 64.4 us -> 66.5 us (1.033)
  waiting for transfers between devices: 30.5 us -> 26.5 us
  starting transfers between devices: 20.4 us -> 23.5 us
  Pallas kernels: 13 us -> 15 us
  local copies, waits for them, and re-layouts: 0.07 us -> 1.05 us
    ppermute x17 -> x16, waiting for transfers between devices: 30.5 us -> 26.5 us  [swap(): lax.ppermute(x, axis, [(i, i ^ code) for i in range(lax.axis_size(axis))])]
    ppermute x17 -> x16, starting transfers between devices: 19.8 us -> 22.8 us  [swap(): lax.ppermute(x, axis, [(i, i ^ code) for i in range(lax.axis_size(axis))])]
    pallas_call x8 -> x9, Pallas kernels: 13 us -> 15 us  [run(): return pl.pallas_call(*args, **kwargs)(*operands)]
    unnamed x23 -> x27, local copies, waits for them, and re-layouts: 0.06 us -> 1.04 us
  transfers between devices with their start and end apart: 18 -> 17, of which waited for: 8 -> 8; matrix products, arithmetic and copies ran while one was open for 0% -> 0% of each run, Pallas kernels for 12% -> 13%
where the time goes in v1:
time: 66.5 us; the launch traced here: 66.3 us
  waiting for transfers between devices  26.5 us (40%)
  starting transfers between devices  23.5 us (35%)
  Pallas kernels  15 us (23%)
  local copies, waits for them, and re-layouts  1.05 us (2%)
    ppermute x16, waiting for transfers between devices, swap(): lax.ppermute(x, axis, [(i, i ^ code) for i in range(lax.axis_size(axis))])  26.5 us
    ppermute x16, starting transfers between devices, swap(): lax.ppermute(x, axis, [(i, i ^ code) for i in range(lax.axis_size(axis))])  22.8 us
    pallas_call x9, Pallas kernels, run(): return pl.pallas_call(*args, **kwargs)(*operands)  15 us
  transfers between devices with their start and end apart: 17, of which 8 were waited for; matrix products, arithmetic and copies ran while one was open for 0% of the time, Pallas kernels for 13%

profile of v1, /device:TPU:0, one launch (start us, length us, event | category | flops | bytes accessed | tf_op | source)
XLA Modules:
  0.0 66.3 jit_solution(9391609167405735969)
XLA Ops:
  0.0 1.6 %shard_map.145 = f32[8,512]{1,0:T(8,128)S(1)} custom-call(f32[1,256]{1,0:T(1,128)} %bitcast.8, f32[1,256]{1,0:T(1,128)} %bitcast.9, bf16[256,512]{1,0:T(8,128)(2,1)} %shift_ref.1, bf16[256,512]{1,0:T(8,128)(2,1)} %scale_ref.1, bf16[256,512]{1,0:T(8,128)(2,1)} %gate_ref.1), custom_call_target="tpu_custom_call" | custom-call | flops 137438953472 | bytes 1048576 | tf_op jit(solution)/shard_map/pallas_call | solution.py:37
  1.7 3.0 %collective-permute-start.1 = (f32[8,512]{1,0:T(8,128)S(1)}, f32[8,512]{1,0:T(8,128)S(1)}, u32[]{:S(2)}, u32[]{:S(2)}) collective-permute-start(f32[8,512]{1,0:T(8,128)S(1)} %shard_map.145), channel_id=1, source_target_pairs={{0,2},{1,3},{2,0},{3,1},{4,6},{5,7},{6,4},{7,5},{8,10},{9,11},{10,... | collective-permute-start | bytes 49160 | tf_op jit(solution)/shard_map/ppermute | solution.py:32
  4.7 1.7 %collective-permute-done.1 = f32[8,512]{1,0:T(8,128)S(1)} collective-permute-done((f32[8,512]{1,0:T(8,128)S(1)}, f32[8,512]{1,0:T(8,128)S(1)}, u32[]{:S(2)}, u32[]{:S(2)}) %collective-permute-start.1) | collective-permute-done | bytes 16416 | tf_op jit(solution)/shard_map/ppermute | solution.py:32
  6.4 2.1 %collective-permute-start.2 = (f32[16,512]{1,0:T(8,128)S(1)}, f32[16,512]{1,0:T(8,128)S(1)}, u32[]{:S(2)}, u32[]{:S(2)}) collective-permute-start(f32[16,512]{1,0:T(8,128)S(1)} %pad_maximum_fusion), channel_id=1, source_target_pairs={{0,8},{4,12},{8,0},{12,4},{16,24},{20,28},{24,16},{28,20},{1,9},{5... | collective-permute-start | bytes 98312 | tf_op jit(solution)/shard_map/ppermute | solution.py:32
  8.5 1.5 %collective-permute-start = (bf16[64,2048]{1,0:T(8,128)(2,1)S(1)}, bf16[64,2048]{1,0:T(8,128)(2,1)S(1)}, u32[]{:S(2)}, u32[]{:S(2)}) collective-permute-start(bf16[64,2048]{1,0:T(8,128)(2,1)S(1)} %copy-done.6), channel_id=1, source_target_pairs={{0,4},{4,0},{8,12},{12,8},{16,20},{20,16},{24,28},{28,24},{1,5},{5... | collective-permute-start | bytes 786440 | tf_op jit(solution)/shard_map/ppermute | solution.py:32
  10.1 0.4 collective-permute-done.2
  10.4 3.0 %collective-permute-start.3 = (f32[16,512]{1,0:T(8,128)S(1)}, f32[16,512]{1,0:T(8,128)S(1)}, u32[]{:S(2)}, u32[]{:S(2)}) collective-permute-start(f32[16,512]{1,0:T(8,128)S(1)} %fusion), channel_id=1, source_target_pairs={{0,16},{4,20},{8,24},{12,28},{16,0},{20,4},{24,8},{28,12},{1,17},{... | collective-permute-start | bytes 98312 | tf_op jit(solution)/shard_map/ppermute | solution.py:32
  13.5 1.9 %collective-permute-done.3 = f32[16,512]{1,0:T(8,128)S(1)} collective-permute-done((f32[16,512]{1,0:T(8,128)S(1)}, f32[16,512]{1,0:T(8,128)S(1)}, u32[]{:S(2)}, u32[]{:S(2)}) %collective-permute-start.3) | collective-permute-done | bytes 32800 | tf_op jit(solution)/shard_map/ppermute | solution.py:32
  15.4 1.9 %collective-permute-start.4 = (f32[16,512]{1,0:T(8,128)S(1)}, f32[16,512]{1,0:T(8,128)S(1)}, u32[]{:S(2)}, u32[]{:S(2)}) collective-permute-start(f32[16,512]{1,0:T(8,128)S(1)} %add.12), channel_id=1, source_target_pairs={{0,4},{4,0},{8,12},{12,8},{16,20},{20,16},{24,28},{28,24},{1,5},{5... | collective-permute-start | bytes 98312 | tf_op jit(solution)/shard_map/ppermute | solution.py:32
  17.2 2.1 %collective-permute-done.4 = f32[16,512]{1,0:T(8,128)S(1)} collective-permute-done((f32[16,512]{1,0:T(8,128)S(1)}, f32[16,512]{1,0:T(8,128)S(1)}, u32[]{:S(2)}, u32[]{:S(2)}) %collective-permute-start.4) | collective-permute-done | bytes 32800 | tf_op jit(solution)/shard_map/ppermute | solution.py:32
  19.3 1.2 %collective-permute-done.5.refs_3_ = f32[16,512]{1,0:T(8,128)S(1)} collective-permute-done((f32[16,512]{1,0:T(8,128)S(1)}, f32[16,512]{1,0:T(8,128)S(1)}, u32[]{:S(2)}, u32[]{:S(2)}) %collective-permute-start.5) | collective-permute-done | bytes 32800 | tf_op jit(solution)/shard_map/ppermute | solution.py:32
  20.5 0.0 copy-start.9
  20.6 2.2 %shard_map.146 = (bf16[256,512]{1,0:T(8,128)(2,1)S(1)}, bf16[128,512]{1,0:T(8,128)(2,1)S(1)}, bf16[256,2048]{1,0:T(8,128)(2,1)S(1)}, f32[1,2048]{1,0:T(1,128)S(1)}) custom-call(bf16[256,2048]{1,0:T(8,128)(2,1)S(1)} %copy-done, bf16[64,2048]{1,0:T(8,128)(2,1)S(1)} %copy-done.6, bf16[64,2048]{1,0:T(8,128)(2,1)S(1)} %collective-permute-done.refs_1_, ...), custom_call_target="tpu_custom_call" | custom-call | flops 137438953472 | bytes 1048576 | tf_op jit(solution)/shard_map/pallas_call | solution.py:37
  22.8 3.0 %collective-permute-start.8 = (bf16[128,512]{1,0:T(8,128)(2,1)S(1)}, bf16[128,512]{1,0:T(8,128)(2,1)S(1)}, u32[]{:S(2)}, u32[]{:S(2)}) collective-permute-start(bf16[128,512]{1,0:T(8,128)(2,1)S(1)} %get-tuple-element.18.refs_1_), channel_id=1, source_target_pairs={{0,16},{4,20},{8,24},{12,28},{16,0},{20,4},{24,8},{28,12},{1,17},{... | collective-permute-start | bytes 393224 | tf_op jit(solution)/shard_map/ppermute | solution.py:32
  25.8 1.5 %collective-permute-start.12 = (bf16[256,2048]{1,0:T(8,128)(2,1)S(1)}, bf16[256,2048]{1,0:T(8,128)(2,1)S(1)}, u32[]{:S(2)}, u32[]{:S(2)}) collective-permute-start(bf16[256,2048]{1,0:T(8,128)(2,1)S(1)} %copy-done.9), channel_id=1, source_target_pairs={{0,2},{1,3},{2,0},{3,1},{4,6},{5,7},{6,4},{7,5},{8,10},{9,11},{10,... | collective-permute-start | bytes 3145736 | tf_op jit(solution)/shard_map/ppermute | solution.py:32
  27.4 1.0 %shard_map.148.refs_2_.refs_5_ = f32[4,14,64,128]{3,2,1,0:T(8,128)S(1)} custom-call(f32[4,15,128]{2,1,0:T(8,128)S(1)} %pad.4.bias_ref), custom_call_target="tpu_custom_call" | custom-call | tf_op jit(solution)/shard_map/pallas_call | solution.py:37
  28.4 1.6 %collective-permute-start.6 = (bf16[256,512]{1,0:T(8,128)(2,1)S(1)}, bf16[256,512]{1,0:T(8,128)(2,1)S(1)}, u32[]{:S(2)}, u32[]{:S(2)}) collective-permute-start(bf16[256,512]{1,0:T(8,128)(2,1)S(1)} %get-tuple-element.17.refs_0_), channel_id=1, source_target_pairs={{0,4},{4,0},{8,12},{12,8},{16,20},{20,16},{24,28},{28,24},{1,5},{5... | collective-permute-start | bytes 786440 | tf_op jit(solution)/shard_map/ppermute | solution.py:32
  30.0 0.7 %collective-permute-start.7 = (bf16[256,512]{1,0:T(8,128)(2,1)S(1)}, bf16[256,512]{1,0:T(8,128)(2,1)S(1)}, u32[]{:S(2)}, u32[]{:S(2)}) collective-permute-start(bf16[256,512]{1,0:T(8,128)(2,1)S(1)} %get-tuple-element.17.refs_0_), channel_id=1, source_target_pairs={{4,8},{12,16},{20,24},{8,4},{16,12},{24,20},{5,9},{13,17},{21,25},... | collective-permute-start | bytes 786440 | tf_op jit(solution)/shard_map/ppermute | solution.py:408
  30.6 3.3 %collective-permute-start.9 = (bf16[128,512]{1,0:T(8,128)(2,1)S(1)}, bf16[128,512]{1,0:T(8,128)(2,1)S(1)}, u32[]{:S(2)}, u32[]{:S(2)}) collective-permute-start(bf16[128,512]{1,0:T(8,128)(2,1)S(1)} %get-tuple-element.18.refs_1_), channel_id=1, source_target_pairs={{0,8},{4,12},{8,0},{12,4},{16,24},{20,28},{24,16},{28,20},{1,9},{5... | collective-permute-start | bytes 393224 | tf_op jit(solution)/shard_map/ppermute | solution.py:32
  33.9 0.7 %shard_map.147.q_ref = bf16[256,256]{1,0:T(8,128)(2,1)S(1)} custom-call(bf16[256,2048]{1,0:T(8,128)(2,1)S(1)} %get-tuple-element.16.hid_ref, bf16[2048,256]{1,0:T(8,128)(2,1)S(1)} %copy-done.2, f32[1,64]{1,0:T(1,128)S(1)} %bitcast.5), custom_call_target="tpu_custom_call" | custom-call | tf_op jit(solution)/shard_map/pallas_call | solution.py:37
  34.6 0.1 collective-permute-start.10
  34.7 1.0 %shard_map.149 = (f32[256,256]{1,0:T(8,128)S(1)}, f32[256,256]{1,0:T(8,128)S(1)}, f32[256,256]{1,0:T(8,128)S(1)}) custom-call(bf16[256,256]{1,0:T(8,128)(2,1)S(1)} %shard_map.147.q_ref, bf16[256,512]{1,0:T(8,128)(2,1)S(1)} %get-tuple-element.17.refs_0_, bf16[128,512]{1,0:T(8,128)(2,1)S(1)} %get-tuple-element.18.refs_1_, ...), custom_call_target="tpu_custom_call" | custom-call | flops 137438953472 | bytes 1048576 | tf_op jit(solution)/shard_map/pallas_call | solution.py:37
  35.7 8.0 %collective-permute-done.9.refs_3_ = bf16[128,512]{1,0:T(8,128)(2,1)S(1)} collective-permute-done((bf16[128,512]{1,0:T(8,128)(2,1)S(1)}, bf16[128,512]{1,0:T(8,128)(2,1)S(1)}, u32[]{:S(2)}, u32[]{:S(2)}) %collective-permute-start.9) | collective-permute-done | bytes 131104 | tf_op jit(solution)/shard_map/ppermute | solution.py:32
  43.7 7.1 %collective-permute-done.12.refs_1_ = bf16[256,2048]{1,0:T(8,128)(2,1)S(1)} collective-permute-done((bf16[256,2048]{1,0:T(8,128)(2,1)S(1)}, bf16[256,2048]{1,0:T(8,128)(2,1)S(1)}, u32[]{:S(2)}, u32[]{:S(2)}) %collective-permute-start.12) | collective-permute-done | bytes 1048608 | tf_op jit(solution)/shard_map/ppermute | solution.py:32
  50.8 2.3 %shard_map.150.refs_0_ = bf16[256,256]{1,0:T(8,128)(2,1)S(1)} custom-call(bf16[256,256]{1,0:T(8,128)(2,1)S(1)} %shard_map.147.q_ref, bf16[256,512]{1,0:T(8,128)(2,1)S(1)} %collective-permute-done.6.refs_0_, bf16[256,512]{1,0:T(8,128)(2,1)S(1)} %collective-permute-done.7.refs_1_, bf16[128,512]{1,0:T(8,128)(2,1)S(1)} %collective-permute-done.8.refs_2_, ...), custom_call_target="tpu_custom_call" | custom-call | flops 137438953472 | bytes 1048576 | tf_op jit(solution)/shard_map/pallas_call | solution.py:37
  53.1 1.6 %collective-permute-start.14 = (bf16[256,256]{1,0:T(8,128)(2,1)S(1)}, bf16[256,256]{1,0:T(8,128)(2,1)S(1)}, u32[]{:S(2)}, u32[]{:S(2)}) collective-permute-start(bf16[256,256]{1,0:T(8,128)(2,1)S(1)} %shard_map.150.refs_0_), channel_id=1, source_target_pairs={{0,2},{1,3},{2,0},{3,1},{4,6},{5,7},{6,4},{7,5},{8,10},{9,11},{10,... | collective-permute-start | bytes 393224 | tf_op jit(solution)/shard_map/ppermute | solution.py:32
  54.7 0.2 collective-permute-start.11
  54.9 4.2 %collective-permute-done.14.refs_0_ = bf16[256,256]{1,0:T(8,128)(2,1)S(1)} collective-permute-done((bf16[256,256]{1,0:T(8,128)(2,1)S(1)}, bf16[256,256]{1,0:T(8,128)(2,1)S(1)}, u32[]{:S(2)}, u32[]{:S(2)}) %collective-permute-start.14) | collective-permute-done | bytes 131104 | tf_op jit(solution)/shard_map/ppermute | solution.py:32
  59.1 1.0 %copy-done.11 = bf16[256,2048]{1,0:T(8,128)(2,1)} copy-done((bf16[256,2048]{1,0:T(8,128)(2,1)}, bf16[256,2048]{1,0:T(8,128)(2,1)S(1)}, u32[]{:S(2)}) %copy-start.11) | copy-done | bytes 1048600
  60.0 1.9 %shard_map.151 = (bf16[256,2048]{1,0:T(8,128)(2,1)S(1)}, bf16[256,2048]{1,0:T(8,128)(2,1)S(1)}, bf16[256,2048]{1,0:T(8,128)(2,1)S(1)}) custom-call(bf16[256,2048]{1,0:T(8,128)(2,1)} %refs_0_.3, bf16[256,2048]{1,0:T(8,128)(2,1)} %copy-done.10, bf16[256,2048]{1,0:T(8,128)(2,1)} %copy-done.11), custom_call_target="tpu_custom_call" | custom-call | tf_op jit(solution)/shard_map/pallas_call | solution.py:37
  61.9 1.6 %shard_map.152.sum_ref = f32[256,2048]{1,0:T(8,128)S(1)} custom-call(bf16[256,256]{1,0:T(8,128)(2,1)S(1)} %shard_map.150.refs_0_, bf16[256,256]{1,0:T(8,128)(2,1)S(1)} %collective-permute-done.11.refs_1_, bf16[256,2048]{1,0:T(8,128)(2,1)S(1)} %get-tuple-element.22.refs_2_, bf16[256,2048]{1,0:T(8,128)(2,1)S(1)} %get-tuple-element.23.refs_3_), custom_call_target="tpu_custom_call" | custom-call | tf_op jit(solution)/shard_map/pallas_call | solution.py:37
  63.6 2.8 %shard_map.153 = bf16[256,2048]{1,0:T(8,128)(2,1)} custom-call(bf16[256,2048]{1,0:T(8,128)(2,1)S(1)} %copy-done.1, f32[1,2048]{1,0:T(1,128)S(1)} %get-tuple-element.15.gate_ref, f32[256,2048]{1,0:T(8,128)S(1)} %shard_map.152.sum_ref, bf16[256,256]{1,0:T(8,128)(2,1)S(1)} %collective-permute-done.14.refs_0_, ...), custom_call_target="tpu_custom_call" | custom-call | tf_op jit(solution)/shard_map/pallas_call | solution.py:37
  (43 shorter events, 0.1 us)
Async XLA Ops:
  0.0 8.5 %copy-start.6 = (bf16[64,2048]{1,0:T(8,128)(2,1)S(1)}, bf16[64,2048]{1,0:T(8,128)(2,1)}, u32[]{:S(2)}) copy-start(bf16[64,2048]{1,0:T(8,128)(2,1)} %refs_0_.2) | copy-start | bytes 786436
  0.0 20.5 %copy-start = (bf16[256,2048]{1,0:T(8,128)(2,1)S(1)}, bf16[256,2048]{1,0:T(8,128)(2,1)}, u32[]{:S(2)}) copy-start(bf16[256,2048]{1,0:T(8,128)(2,1)} %lat_ref.3) | copy-start | bytes 3145732
  0.0 20.5 %copy-start.4 = (bf16[2048,256]{1,0:T(8,128)(2,1)S(1)}, bf16[2048,256]{1,0:T(8,128)(2,1)}, u32[]{:S(2)}) copy-start(bf16[2048,256]{1,0:T(8,128)(2,1)} %refs_6_.1) | copy-start | bytes 3145732
  0.0 20.5 %copy-start.5 = (bf16[2048,256]{1,0:T(8,128)(2,1)S(1)}, bf16[2048,256]{1,0:T(8,128)(2,1)}, u32[]{:S(2)}) copy-start(bf16[2048,256]{1,0:T(8,128)(2,1)} %refs_7_.1) | copy-start | bytes 3145732
  0.0 20.5 %copy-start.7 = (f32[2048]{0:T(1024)S(1)}, f32[2048]{0:T(1024)}, u32[]{:S(2)}) copy-start(f32[2048]{0:T(1024)} %param.22) | copy-start | bytes 24580
  0.0 20.5 %copy-start.8 = (f32[64]{0:T(128)S(1)}, f32[64]{0:T(128)}, u32[]{:S(2)}) copy-start(f32[64]{0:T(128)} %param.27) | copy-start | bytes 772
  1.7 4.8 %collective-permute-start.1 = (f32[8,512]{1,0:T(8,128)S(1)}, f32[8,512]{1,0:T(8,128)S(1)}, u32[]{:S(2)}, u32[]{:S(2)}) collective-permute-start(f32[8,512]{1,0:T(8,128)S(1)} %shard_map.145), channel_id=1, source_target_pairs={{0,2},{1,3},{2,0},{3,1},{4,6},{5,7},{6,4},{7,5},{8,10},{9,11},{10,... | collective-permute-start | bytes 49160 | tf_op jit(solution)/shard_map/ppermute | solution.py:32
  6.4 4.0 %collective-permute-start.2 = (f32[16,512]{1,0:T(8,128)S(1)}, f32[16,512]{1,0:T(8,128)S(1)}, u32[]{:S(2)}, u32[]{:S(2)}) collective-permute-start(f32[16,512]{1,0:T(8,128)S(1)} %pad_maximum_fusion), channel_id=1, source_target_pairs={{0,8},{4,12},{8,0},{12,4},{16,24},{20,28},{24,16},{28,20},{1,9},{5... | collective-permute-start | bytes 98312 | tf_op jit(solution)/shard_map/ppermute | solution.py:32
  8.5 12.0 %collective-permute-start = (bf16[64,2048]{1,0:T(8,128)(2,1)S(1)}, bf16[64,2048]{1,0:T(8,128)(2,1)S(1)}, u32[]{:S(2)}, u32[]{:S(2)}) collective-permute-start(bf16[64,2048]{1,0:T(8,128)(2,1)S(1)} %copy-done.6), channel_id=1, source_target_pairs={{0,4},{4,0},{8,12},{12,8},{16,20},{20,16},{24,28},{28,24},{1,5},{5... | collective-permute-start | bytes 786440 | tf_op jit(solution)/shard_map/ppermute | solution.py:32
  10.4 4.9 %collective-permute-start.3 = (f32[16,512]{1,0:T(8,128)S(1)}, f32[16,512]{1,0:T(8,128)S(1)}, u32[]{:S(2)}, u32[]{:S(2)}) collective-permute-start(f32[16,512]{1,0:T(8,128)S(1)} %fusion), channel_id=1, source_target_pairs={{0,16},{4,20},{8,24},{12,28},{16,0},{20,4},{24,8},{28,12},{1,17},{... | collective-permute-start | bytes 98312 | tf_op jit(solution)/shard_map/ppermute | solution.py:32
  15.4 3.9 %collective-permute-start.4 = (f32[16,512]{1,0:T(8,128)S(1)}, f32[16,512]{1,0:T(8,128)S(1)}, u32[]{:S(2)}, u32[]{:S(2)}) collective-permute-start(f32[16,512]{1,0:T(8,128)S(1)} %add.12), channel_id=1, source_target_pairs={{0,4},{4,0},{8,12},{12,8},{16,20},{20,16},{24,28},{28,24},{1,5},{5... | collective-permute-start | bytes 98312 | tf_op jit(solution)/shard_map/ppermute | solution.py:32
  19.3 1.2 %collective-permute-start.5 = (f32[16,512]{1,0:T(8,128)S(1)}, f32[16,512]{1,0:T(8,128)S(1)}, u32[]{:S(2)}, u32[]{:S(2)}) collective-permute-start(f32[16,512]{1,0:T(8,128)S(1)} %add.13.refs_2_), channel_id=1, source_target_pairs={{0,1},{1,0},{2,3},{3,2},{4,5},{5,4},{6,7},{7,6},{8,9},{9,8},{10,11... | collective-permute-start | bytes 98312 | tf_op jit(solution)/shard_map/ppermute | solution.py:32
  20.5 5.3 %copy-start.9 = (bf16[256,2048]{1,0:T(8,128)(2,1)S(1)}, bf16[256,2048]{1,0:T(8,128)(2,1)}, u32[]{:S(2)}) copy-start(bf16[256,2048]{1,0:T(8,128)(2,1)} %refs_0_.3) | copy-start | bytes 3145732
  20.6 6.8 %copy-start.12 = (f32[4,15,31]{2,0,1:T(4,128)S(1)}, f32[4,15,31]{2,0,1:T(4,128)}, u32[]{:S(2)}) copy-start(f32[4,15,31]{2,0,1:T(4,128)} %param.28) | copy-start | bytes 22324
  20.6 13.3 %copy-start.3 = (f32[64]{0:T(128)S(1)}, f32[64]{0:T(128)}, u32[]{:S(2)}) copy-start(f32[64]{0:T(128)} %param.26) | copy-start | bytes 772
  22.8 11.1 %copy-start.2 = (bf16[2048,256]{1,0:T(8,128)(2,1)S(1)}, bf16[2048,256]{1,0:T(8,128)(2,1)}, u32[]{:S(2)}) copy-start(bf16[2048,256]{1,0:T(8,128)(2,1)} %wq_ref.1) | copy-start | bytes 3145732
  22.8 11.8 %collective-permute-start.8 = (bf16[128,512]{1,0:T(8,128)(2,1)S(1)}, bf16[128,512]{1,0:T(8,128)(2,1)S(1)}, u32[]{:S(2)}, u32[]{:S(2)}) collective-permute-start(bf16[128,512]{1,0:T(8,128)(2,1)S(1)} %get-tuple-element.18.refs_1_), channel_id=1, source_target_pairs={{0,16},{4,20},{8,24},{12,28},{16,0},{20,4},{24,8},{28,12},{1,17},{... | collective-permute-start | bytes 393224 | tf_op jit(solution)/shard_map/ppermute | solution.py:32
  25.8 24.9 %collective-permute-start.12 = (bf16[256,2048]{1,0:T(8,128)(2,1)S(1)}, bf16[256,2048]{1,0:T(8,128)(2,1)S(1)}, u32[]{:S(2)}, u32[]{:S(2)}) collective-permute-start(bf16[256,2048]{1,0:T(8,128)(2,1)S(1)} %copy-done.9), channel_id=1, source_target_pairs={{0,2},{1,3},{2,0},{3,1},{4,6},{5,7},{6,4},{7,5},{8,10},{9,11},{10,... | collective-permute-start | bytes 3145736 | tf_op jit(solution)/shard_map/ppermute | solution.py:32
  28.4 22.4 %collective-permute-start.6 = (bf16[256,512]{1,0:T(8,128)(2,1)S(1)}, bf16[256,512]{1,0:T(8,128)(2,1)S(1)}, u32[]{:S(2)}, u32[]{:S(2)}) collective-permute-start(bf16[256,512]{1,0:T(8,128)(2,1)S(1)} %get-tuple-element.17.refs_0_), channel_id=1, source_target_pairs={{0,4},{4,0},{8,12},{12,8},{16,20},{20,16},{24,28},{28,24},{1,5},{5... | collective-permute-start | bytes 786440 | tf_op jit(solution)/shard_map/ppermute | solution.py:32
  30.0 20.8 %collective-permute-start.7 = (bf16[256,512]{1,0:T(8,128)(2,1)S(1)}, bf16[256,512]{1,0:T(8,128)(2,1)S(1)}, u32[]{:S(2)}, u32[]{:S(2)}) collective-permute-start(bf16[256,512]{1,0:T(8,128)(2,1)S(1)} %get-tuple-element.17.refs_0_), channel_id=1, source_target_pairs={{4,8},{12,16},{20,24},{8,4},{16,12},{24,20},{5,9},{13,17},{21,25},... | collective-permute-start | bytes 786440 | tf_op jit(solution)/shard_map/ppermute | solution.py:408
  30.6 13.0 %collective-permute-start.9 = (bf16[128,512]{1,0:T(8,128)(2,1)S(1)}, bf16[128,512]{1,0:T(8,128)(2,1)S(1)}, u32[]{:S(2)}, u32[]{:S(2)}) collective-permute-start(bf16[128,512]{1,0:T(8,128)(2,1)S(1)} %get-tuple-element.18.refs_1_), channel_id=1, source_target_pairs={{0,8},{4,12},{8,0},{12,4},{16,24},{20,28},{24,16},{28,20},{1,9},{5... | collective-permute-start | bytes 393224 | tf_op jit(solution)/shard_map/ppermute | solution.py:32
  34.6 16.2 %collective-permute-start.10 = (bf16[128,512]{1,0:T(8,128)(2,1)S(1)}, bf16[128,512]{1,0:T(8,128)(2,1)S(1)}, u32[]{:S(2)}, u32[]{:S(2)}) collective-permute-start(bf16[128,512]{1,0:T(8,128)(2,1)S(1)} %collective-permute-done.8.refs_2_), channel_id=1, source_target_pairs={{0,8},{4,12},{8,0},{12,4},{16,24},{20,28},{24,16},{28,20},{1,9},{5... | collective-permute-start | bytes 393224 | tf_op jit(solution)/shard_map/ppermute | solution.py:32
  43.7 15.4 %collective-permute-start.13 = (bf16[256,2048]{1,0:T(8,128)(2,1)S(1)}, bf16[256,2048]{1,0:T(8,128)(2,1)S(1)}, u32[]{:S(2)}, u32[]{:S(2)}) collective-permute-start(bf16[256,2048]{1,0:T(8,128)(2,1)S(1)} %copy-done.9), channel_id=1, source_target_pairs={{0,1},{1,0},{2,3},{3,2},{4,5},{5,4},{6,7},{7,6},{8,9},{9,8},{10,11... | collective-permute-start | bytes 3145736 | tf_op jit(solution)/shard_map/ppermute | solution.py:32
  50.8 2.3 %copy-start.10 = (bf16[256,2048]{1,0:T(8,128)(2,1)}, bf16[256,2048]{1,0:T(8,128)(2,1)S(1)}, u32[]{:S(2)}) copy-start(bf16[256,2048]{1,0:T(8,128)(2,1)S(1)} %collective-permute-done.12.refs_1_) | copy-start | bytes 3145732
  50.8 12.8 %collective-permute-start.16 = (bf16[256,2048]{1,0:T(8,128)(2,1)S(1)}, bf16[256,2048]{1,0:T(8,128)(2,1)S(1)}, u32[]{:S(2)}, u32[]{:S(2)}) collective-permute-start(bf16[256,2048]{1,0:T(8,128)(2,1)S(1)} %collective-permute-done.12.refs_1_), channel_id=1, source_target_pairs={{0,1},{1,0},{2,3},{3,2},{4,5},{5,4},{6,7},{7,6},{8,9},{9,8},{10,11... | collective-permute-start | bytes 3145736 | tf_op jit(solution)/shard_map/ppermute | solution.py:32
  53.1 6.0 %collective-permute-start.14 = (bf16[256,256]{1,0:T(8,128)(2,1)S(1)}, bf16[256,256]{1,0:T(8,128)(2,1)S(1)}, u32[]{:S(2)}, u32[]{:S(2)}) collective-permute-start(bf16[256,256]{1,0:T(8,128)(2,1)S(1)} %shard_map.150.refs_0_), channel_id=1, source_target_pairs={{0,2},{1,3},{2,0},{3,1},{4,6},{5,7},{6,4},{7,5},{8,10},{9,11},{10,... | collective-permute-start | bytes 393224 | tf_op jit(solution)/shard_map/ppermute | solution.py:32
  54.7 7.3 %collective-permute-start.11 = (bf16[256,256]{1,0:T(8,128)(2,1)S(1)}, bf16[256,256]{1,0:T(8,128)(2,1)S(1)}, u32[]{:S(2)}, u32[]{:S(2)}) collective-permute-start(bf16[256,256]{1,0:T(8,128)(2,1)S(1)} %shard_map.150.refs_0_), channel_id=1, source_target_pairs={{0,1},{1,0},{2,3},{3,2},{4,5},{5,4},{6,7},{7,6},{8,9},{9,8},{10,11... | collective-permute-start | bytes 393224 | tf_op jit(solution)/shard_map/ppermute | solution.py:32
  59.0 4.5 %collective-permute-start.15 = (bf16[256,256]{1,0:T(8,128)(2,1)S(1)}, bf16[256,256]{1,0:T(8,128)(2,1)S(1)}, u32[]{:S(2)}, u32[]{:S(2)}) collective-permute-start(bf16[256,256]{1,0:T(8,128)(2,1)S(1)} %collective-permute-done.14.refs_0_), channel_id=1, source_target_pairs={{0,1},{1,0},{2,3},{3,2},{4,5},{5,4},{6,7},{7,6},{8,9},{9,8},{10,11... | collective-permute-start | bytes 393224 | tf_op jit(solution)/shard_map/ppermute | solution.py:32
  59.1 1.0 %copy-start.11 = (bf16[256,2048]{1,0:T(8,128)(2,1)}, bf16[256,2048]{1,0:T(8,128)(2,1)S(1)}, u32[]{:S(2)}) copy-start(bf16[256,2048]{1,0:T(8,128)(2,1)S(1)} %collective-permute-done.13.refs_2_) | copy-start | bytes 3145732
  61.9 1.6 %copy-start.1 = (bf16[256,2048]{1,0:T(8,128)(2,1)S(1)}, bf16[256,2048]{1,0:T(8,128)(2,1)}, u32[]{:S(2)}) copy-start(bf16[256,2048]{1,0:T(8,128)(2,1)} %lat_ref.3) | copy-start | bytes 3145732

commit v2 on v1

--- a/solution.py
+++ b/solution.py
@@ -57,15 +57,25 @@
 
 
 def partials_body(
-    cond_ref, ctx_cond_ref, shift_ref, scale_ref, gate_ref, out_ref, rows_ref, *scratch
+    cond_ref, ctx_cond_ref, shift_ref, scale_ref, gate_ref, ctx_ref, lat_ref,
+    out_ref, ctx_half_ref, lat_half_ref, rows_ref, *scratch
 ):
     weights, sems = scratch[:3], scratch[3]
+    half = ctx_half_ref.shape[1]
+    at = pl.multiple_of(lax.rem(lax.axis_index("tp"), 2) * half, half)
     copies = [
-        pltpu.make_async_copy(cond_ref, rows_ref.at[0:1], sems.at[3]),
-        pltpu.make_async_copy(ctx_cond_ref, rows_ref.at[1:2], sems.at[4]),
-    ] + [
         pltpu.make_async_copy(src, dst, sems.at[n])
-        for n, (src, dst) in enumerate(zip((shift_ref, scale_ref, gate_ref), weights))
+        for n, (src, dst) in enumerate(
+            (
+                (cond_ref, rows_ref.at[0:1]),
+                (ctx_cond_ref, rows_ref.at[1:2]),
+                (shift_ref, weights[0]),
+                (scale_ref, weights[1]),
+                (gate_ref, weights[2]),
+                (ctx_ref.at[:, pl.ds(at, half)], ctx_half_ref),
+                (lat_ref.at[:, pl.ds(at, half)], lat_half_ref),
+            )
+        )
     ]
     for copy in copies:
         copy.start()
@@ -79,6 +89,8 @@
             act, weights[n][...], preferred_element_type=F32
         )
     out_ref[6:8, :] = jnp.zeros((2, out_ref.shape[1]), F32)
+    copies[5].wait()
+    copies[6].wait()
 
 
 def table_body(bias_ref, out_ref):
@@ -118,40 +130,52 @@
     return x * lax.rsqrt(mean + EPS) * head_gain
 
 
-def project_body(codes, n_ctx, lat_ref, *refs):
-    ctx_refs, refs = refs[:n_ctx], refs[n_ctx:]
-    part_ref, beside_ref, refs = refs[0], refs[1], refs[2:]
+def modulated(values, vec_ref, gain_ref, row):
+    mult = gain_ref[...] * (1.0 + vec_ref[2 + row : 3 + row, :])
+    shift = vec_ref[row : row + 1, :]
+    mean = jnp.mean(values * values, axis=-1, keepdims=True)
+    return (values * lax.rsqrt(mean + EPS) * mult + shift).astype(BF16)
+
+
+def join_halves(mine_ref, passed_ref, out_ref):
+    half = mine_ref.shape[1]
+    core = lax.rem(lax.axis_index("tp"), 2)
+    out_ref[:, pl.ds(pl.multiple_of(core * half, half), half)] = mine_ref[...]
+    out_ref[:, pl.ds(pl.multiple_of((1 - core) * half, half), half)] = passed_ref[...]
+
+
+def row_steps(count):
+    step = 32 if count % 32 == 0 else count
+    return [slice(at, at + step) for at in range(0, count, step)]
+
+
+def project_body(codes, lat_ref, ctx_ref, mine_ref, passed_ref, part_ref, beside_ref, *refs):
     gain_ref, kg_ref, wk, wv = refs[:4]
-    kv_ref, ckv_ref, lat_hid_ref, gate_ref = refs[4:8]
-    vec_ref, hid_ref = refs[8:]
+    kv_ref, ckv_ref, lat_hid_ref, vec_ref = refs[4:8]
+    hid_ref, ctx_two_ref = refs[8:]
     width = part_ref.shape[1]
     me = lax.axis_index("tp")
     for n, code in enumerate(codes):
         for ref, flip in ((part_ref, 0), (beside_ref, 1)):
             at = pl.multiple_of((me ^ code ^ flip) * width, width)
             vec_ref[:, pl.ds(at, width)] = ref[8 * n : 8 * n + 8, :]
-    gate_ref[...] = vec_ref[4:5, :]
+    join_halves(mine_ref, passed_ref, ctx_two_ref)
     lat_count = lat_ref.shape[0]
-    gain = gain_ref[...]
-
-    def modulated(values, row):
-        mult = gain * (1.0 + vec_ref[2 + row : 3 + row, :])
-        shift = vec_ref[row : row + 1, :]
-        mean = jnp.mean(values * values, axis=-1, keepdims=True)
-        return (values * lax.rsqrt(mean + EPS) * mult + shift).astype(BF16)
-
-    step = 32
-    for at in range(0, lat_count, step):
-        hid_ref[at : at + step, :] = modulated(lat_ref[at : at + step, :].astype(F32), 0)
-    if ctx_refs[0].shape[0] % step:
-        both = jnp.concatenate([c[...].astype(F32) for c in ctx_refs], axis=0)
-        hid_ref[lat_count:, :] = modulated(both, 1)
+    ctx_count = ctx_ref.shape[0]
+    for here in row_steps(lat_count):
+        hid_ref[here, :] = modulated(lat_ref[here, :].astype(F32), vec_ref, gain_ref, 0)
+    if ctx_count % 32:
+        both = jnp.concatenate(
+            [ctx_ref[...].astype(F32), ctx_two_ref[...].astype(F32)], axis=0
+        )
+        hid_ref[lat_count:, :] = modulated(both, vec_ref, gain_ref, 1)
     else:
-        base = lat_count
-        for c in ctx_refs:
-            for at in range(0, c.shape[0], step):
-                hid_ref[base : base + step, :] = modulated(c[at : at + step, :].astype(F32), 1)
-                base += step
+        for n, ref in enumerate((ctx_ref, ctx_two_ref)):
+            base = lat_count + n * ctx_count
+            for here in row_steps(ctx_count):
+                hid_ref[base + here.start : base + here.stop, :] = modulated(
+                    ref[here, :].astype(F32), vec_ref, gain_ref, 1
+                )
     cols = wk.shape[1]
     hidden = hid_ref[...]
     keys = head_norm(jnp.dot(hidden, wk[...], preferred_element_type=F32), kg_ref).astype(BF16)
@@ -161,6 +185,18 @@
     kv_ref[:, cols:] = values[:lat_count]
     ckv_ref[:, cols:] = values[lat_count:]
     lat_hid_ref[...] = hidden[:lat_count]
+
+
+def near_body(mine_ref, passed_ref, vec_ref, gain_ref, kg_ref, wk, wv, kv_ref, lat_ref, hid_ref):
+    join_halves(mine_ref, passed_ref, lat_ref)
+    for here in row_steps(lat_ref.shape[0]):
+        hid_ref[here, :] = modulated(lat_ref[here, :].astype(F32), vec_ref, gain_ref, 0)
+    cols = wk.shape[1]
+    hidden = hid_ref[...]
+    kv_ref[:, :cols] = head_norm(
+        jnp.dot(hidden, wk[...], preferred_element_type=F32), kg_ref
+    ).astype(BF16)
+    kv_ref[:, cols:] = jnp.dot(hidden, wv[...], preferred_element_type=F32).astype(BF16)
 
 
 def query_body(hid_ref, wq_ref, qg_ref, q_ref):
@@ -273,9 +309,11 @@
         copy.wait()
 
 
-def first_body(count, *refs):
+def first_body(count, has_prev, *refs):
+    branch = None
+    if has_prev:
+        branch, refs = refs[0][...], refs[1:]
     att, weights, sum_ref = refs[:count], refs[count : 2 * count], refs[2 * count]
-    branch = None
     for a, w in zip(att, weights):
         part = jnp.dot(a[...], w[...], preferred_element_type=F32).astype(BF16).astype(F32)
         branch = part if branch is None else branch + part
@@ -291,7 +329,7 @@
         branch = branch + jnp.dot(a[...], w[...], preferred_element_type=F32).astype(
             BF16
         ).astype(F32)
-    out_ref[...] = (lat_ref[...].astype(F32) + gate_ref[...] * branch).astype(BF16)
+    out_ref[...] = (lat_ref[...].astype(F32) + gate_ref[4:5, :] * branch).astype(BF16)
 
 
 def gather_pieces(x, axis, codes):
@@ -334,25 +372,46 @@
     heads = cols // HEAD_DIM
     block_cols = shift_weight.shape[1]
 
-    raw_codes = [code for code in RAW_CODES if code in sp_bits]
-    ctx_parts = gather_pieces(context, "sp", raw_codes)
-    part = call(
+    half = width // 2
+    part, ctx_half, lat_half = call(
         partials_body,
-        out_shape=jax.ShapeDtypeStruct((8, block_cols), F32),
-        in_specs=raw(5),
-        out_specs=vmem(1)[0],
+        out_shape=(
+            jax.ShapeDtypeStruct((8, block_cols), F32),
+            jax.ShapeDtypeStruct((context.shape[0], half), BF16),
+            jax.ShapeDtypeStruct((tokens, half), BF16),
+        ),
+        in_specs=raw(7),
+        out_specs=tuple(vmem(3)),
         scratch_shapes=[pltpu.VMEM((2, condition.shape[0]), F32)]
         + [pltpu.VMEM(shift_weight.shape, BF16)] * 3
-        + [pltpu.SemaphoreType.DMA((5,))],
+        + [pltpu.SemaphoreType.DMA((7,))],
         compiler_params=params(16),
         cost_estimate=pl.CostEstimate(flops=1 << 37, bytes_accessed=1 << 20, transcendentals=0),
-    )(*[in_hbm(x) for x in (condition[None], ctx_condition[None], shift_weight, scale_weight, gate_weight)])
+    )(
+        *[
+            in_hbm(x)
+            for x in (
+                condition[None],
+                ctx_condition[None],
+                shift_weight,
+                scale_weight,
+                gate_weight,
+                context,
+                latent,
+            )
+        ]
+    )
+    raw_code = sp_bits[min(2, len(sp_bits) - 1)]
+    ctx_mine = swap(ctx_half, "sp", raw_code)
+    ctx_passed = swap(ctx_mine, "tp", 1)
+    near_mine = swap(lat_half, "sp", 1)
+    near_passed = swap(near_mine, "tp", 1)
     codes = [0]
     for code in tp_bits:
         if code > 1:
             part = jnp.concatenate([part, swap(part, "tp", code)], axis=0)
             codes = codes + [had ^ code for had in codes]
-    for code in sp_bits[1:] + sp_bits[:1]:
+    for code in sp_bits:
         part = part + swap(part, "sp", code)
     beside = swap(part, "tp", 1)
     ow_blocks = gather_tp(out_weight, tp_bits)
@@ -366,33 +425,44 @@
         compiler_params=params(16),
     )(padded_bias)
 
-    ctx_count = len(ctx_parts) * ctx_parts[0].shape[0]
-    kv, ctx_kv, hidden, gate = call(
-        functools.partial(project_body, tuple(codes), len(ctx_parts)),
+    ctx_count = 2 * context.shape[0]
+    gain = norm_gain[None]
+    kv, ctx_kv, hidden, vec = call(
+        functools.partial(project_body, tuple(codes)),
         out_shape=(
             jax.ShapeDtypeStruct((tokens, 2 * cols), BF16),
             jax.ShapeDtypeStruct((ctx_count, 2 * cols), BF16),
             jax.ShapeDtypeStruct((tokens, width), BF16),
-            jax.ShapeDtypeStruct((1, width), F32),
+            jax.ShapeDtypeStruct((8, width), F32),
         ),
-        in_specs=vmem(1 + len(ctx_parts) + 2 + 4),
+        in_specs=vmem(10),
         out_specs=vmem(4),
         scratch_shapes=[
-            pltpu.VMEM((8, width), F32),
             pltpu.VMEM((tokens + ctx_count, width), BF16),
+            pltpu.VMEM(context.shape, BF16),
         ],
         compiler_params=params(20),
         cost_estimate=pl.CostEstimate(flops=1 << 37, bytes_accessed=1 << 20, transcendentals=0),
     )(
         latent,
-        *ctx_parts,
+        context,
+        ctx_mine,
+        ctx_passed,
         part,
         beside,
-        norm_gain[None],
+        gain,
         key_gain[None],
         key_weight,
         value_weight,
     )
+    near_kv = call(
+        near_body,
+        out_shape=jax.ShapeDtypeStruct((tokens, 2 * cols), BF16),
+        in_specs=vmem(7),
+        out_specs=vmem(1)[0],
+        scratch_shapes=[pltpu.VMEM((tokens, width), BF16)] * 2,
+        compiler_params=params(20),
+    )(near_mine, near_passed, vec, gain, key_gain[None], key_weight, value_weight)
     queries = call(
         query_body,
         out_shape=jax.ShapeDtypeStruct((tokens, cols), BF16),
@@ -404,11 +474,8 @@
     sp_count = lax.axis_size("sp")
     other_pairs = [(i, i + 1) for i in range(1, sp_count - 1, 2)]
     other_pairs += [(j, i) for i, j in other_pairs]
-    near_kv = swap(kv, "sp", 1)
     other_kv = lax.ppermute(kv, "sp", other_pairs)
-    ctx_pieces = gather_pieces(
-        ctx_kv, "sp", [code for code in sp_bits[::-1] if code not in raw_codes]
-    )
+    ctx_pieces = gather_pieces(ctx_kv, "sp", [code for code in sp_bits if code != raw_code])
 
     def attend(lat, lat_kinds, ctx, prev, is_last):
         shape = (tokens, cols)
@@ -428,54 +495,65 @@
             ),
         )(*operands)
 
-    state = attend([kv], (OWN,), ctx_pieces[:1], (), False)
-    attended = attend([near_kv, other_kv], (NEAR, OTHER), ctx_pieces[1:], state, True)
+    state = attend([kv, near_kv], (OWN, NEAR), ctx_pieces[:1], (), False)
+    attended = attend([other_kv], (OTHER,), ctx_pieces[1:], state, True)
 
     att_blocks = gather_tp(attended, tp_bits)
+
+    def stash(index):
+        code, w = ow_blocks[index]
+        (held,) = call(
+            stash_body,
+            out_shape=(jax.ShapeDtypeStruct((cols, width), BF16),),
+            in_specs=raw(1),
+            out_specs=tuple(vmem(1)),
+            scratch_shapes=[pltpu.SemaphoreType.DMA((1,))],
+            compiler_params=params(8),
+        )(in_hbm(w))
+        ow_blocks[index] = (code, held)
+
+    for n in range(len(ow_blocks) // 2):
+        stash(n)
+
     near = [n for n, (code, _) in enumerate(att_blocks) if code < 2]
-    far = [n for n in range(len(att_blocks)) if n not in near]
+    cross = [n for n, (code, _) in enumerate(att_blocks) if code > 1 and n < len(att_blocks) // 2]
+    far = [n for n in range(len(att_blocks)) if n not in near + cross]
     tile = min(512, width)
     att_spec = pl.BlockSpec((tokens, cols), lambda n: (0, 0))
     weight_spec = pl.BlockSpec((cols, tile), lambda n: (0, n))
     wide_spec = pl.BlockSpec((tokens, tile), lambda n: (0, n))
-    kept = [n for n, (code, _) in enumerate(ow_blocks) if code in (0, 1) + tuple(code for code in tp_bits if code > 1)]
-    stashed = call(
-        stash_body,
-        out_shape=tuple(jax.ShapeDtypeStruct((cols, width), BF16) for _ in kept),
-        in_specs=raw(len(kept)),
-        out_specs=tuple(vmem(len(kept))),
-        scratch_shapes=[pltpu.SemaphoreType.DMA((len(kept),))],
-        compiler_params=params(8),
-    )(*[in_hbm(ow_blocks[n][1]) for n in kept])
-    for n, w in zip(kept, stashed):
-        ow_blocks[n] = (ow_blocks[n][0], w)
+
+    def operands(which):
+        return [att_blocks[n][1] for n in which] + [ow_blocks[n][1] for n in which]
+
+    def specs(which):
+        return [att_spec] * len(which) + [weight_spec] * len(which)
+
     partial_sum = call(
-        functools.partial(first_body, len(near)),
+        functools.partial(first_body, len(near), False),
         grid=(width // tile,),
         out_shape=jax.ShapeDtypeStruct((tokens, width), F32),
-        in_specs=[att_spec] * len(near) + [weight_spec] * len(near),
+        in_specs=specs(near),
         out_specs=wide_spec,
         compiler_params=params(24),
-    )(*[att_blocks[n][1] for n in near], *[ow_blocks[n][1] for n in near])
+    )(*operands(near))
+    partial_sum = call(
+        functools.partial(first_body, len(cross), True),
+        grid=(width // tile,),
+        out_shape=jax.ShapeDtypeStruct((tokens, width), F32),
+        in_specs=[wide_spec] + specs(cross),
+        out_specs=wide_spec,
+        compiler_params=params(24),
+    )(partial_sum, *operands(cross))
     return call(
         functools.partial(output_body, len(far)),
         grid=(width // tile,),
         out_shape=jax.ShapeDtypeStruct((tokens, width), BF16),
-        in_specs=[wide_spec, pl.BlockSpec((1, tile), lambda n: (0, n)), wide_spec]
-        + [att_spec] * len(far)
-        + [weight_spec] * len(far),
+        in_specs=[wide_spec, pl.BlockSpec((8, tile), lambda n: (0, n)), wide_spec]
+        + specs(far),
         out_specs=wide_spec,
         compiler_params=params(24),
-    )(
-        latent,
-        gate,
-        partial_sum,
-        *[att_blocks[n][1] for n in far],
-        *[ow_blocks[n][1] for n in far],
-    )
-
-
-RAW_CODES = (1,)
+    )(latent, vec, partial_sum, *operands(far))
 
 
 def solution(mesh):

time: 66.5 us -> 74.7 us (1.12)
  Pallas kernels: 15 us -> 19.9 us
  waiting for transfers between devices: 26.5 us -> 30.5 us
  local copies, waits for them, and re-layouts: 1.05 us -> 0.08 us
    pallas_call x9 -> x12, Pallas kernels: 15 us -> 19.9 us  [run(): return pl.pallas_call(*args, **kwargs)(*operands)]
    ppermute x16 -> x18, waiting for transfers between devices: 26.5 us -> 30.5 us  [swap(): lax.ppermute(x, axis, [(i, i ^ code) for i in range(lax.axis_size(axis))])]
    unnamed x27 -> x28, local copies, waits for them, and re-layouts: 1.04 us -> 0.07 us
    ppermute x16 -> x18, starting transfers between devices: 22.8 us -> 23 us  [swap(): lax.ppermute(x, axis, [(i, i ^ code) for i in range(lax.axis_size(axis))])]
  transfers between devices with their start and end apart: 17 -> 19, of which waited for: 8 -> 7; matrix products, arithmetic and copies ran while one was open for 0% -> 0% of each run, Pallas kernels for 13% -> 21%
where the time goes in v2:
time: 74.7 us; the launch traced here: 74.5 us
  waiting for transfers between devices  30.5 us (41%)
  starting transfers between devices  23.6 us (32%)
  Pallas kernels  19.9 us (27%)
    ppermute x18, waiting for transfers between devices, swap(): lax.ppermute(x, axis, [(i, i ^ code) for i in range(lax.axis_size(axis))])  30.5 us
    ppermute x18, starting transfers between devices, swap(): lax.ppermute(x, axis, [(i, i ^ code) for i in range(lax.axis_size(axis))])  23 us
    pallas_call x12, Pallas kernels, run(): return pl.pallas_call(*args, **kwargs)(*operands)  19.9 us
  transfers between devices with their start and end apart: 19, of which 7 were waited for; matrix products, arithmetic and copies ran while one was open for 0% of the time, Pallas kernels for 21%

profile of v2, /device:TPU:0, one launch (start us, length us, event | category | flops | bytes accessed | tf_op | source)
XLA Modules:
  0.0 74.5 jit_solution(8948870825256279380)
XLA Ops:
  0.0 1.6 %shard_map.145 = (f32[8,512]{1,0:T(8,128)S(1)}, bf16[64,1024]{1,0:T(8,128)(2,1)S(1)}, bf16[256,1024]{1,0:T(8,128)(2,1)S(1)}) custom-call(f32[1,256]{1,0:T(1,128)} %bitcast.10, f32[1,256]{1,0:T(1,128)} %bitcast.11, bf16[256,512]{1,0:T(8,128)(2,1)} %shift_ref.1, bf16[256,512]{1,0:T(8,128)(2,1)} %scale_ref.1, bf16[256,512]{1,0:T(8,128)(2,1)} %gate_ref.1, ...), custom_call_target="tpu_custom_call" | custom-call | flops 137438953472 | bytes 1048576 | tf_op jit(solution)/shard_map/pallas_call | solution.py:37
  1.7 3.1 %collective-permute-start.11 = (bf16[256,1024]{1,0:T(8,128)(2,1)S(1)}, bf16[256,1024]{1,0:T(8,128)(2,1)S(1)}, u32[]{:S(2)}, u32[]{:S(2)}) collective-permute-start(bf16[256,1024]{1,0:T(8,128)(2,1)S(1)} %get-tuple-element.21), channel_id=1, source_target_pairs={{0,4},{4,0},{8,12},{12,8},{16,20},{20,16},{24,28},{28,24},{1,5},{5... | collective-permute-start | bytes 1572872 | tf_op jit(solution)/shard_map/ppermute | solution.py:32
  4.8 1.5 %collective-permute-start.2 = (f32[8,512]{1,0:T(8,128)S(1)}, f32[8,512]{1,0:T(8,128)S(1)}, u32[]{:S(2)}, u32[]{:S(2)}) collective-permute-start(f32[8,512]{1,0:T(8,128)S(1)} %get-tuple-element.16), channel_id=1, source_target_pairs={{0,2},{1,3},{2,0},{3,1},{4,6},{5,7},{6,4},{7,5},{8,10},{9,11},{10,... | collective-permute-start | bytes 49160 | tf_op jit(solution)/shard_map/ppermute | solution.py:32
  6.2 2.6 %collective-permute-start = (bf16[64,1024]{1,0:T(8,128)(2,1)S(1)}, bf16[64,1024]{1,0:T(8,128)(2,1)S(1)}, u32[]{:S(2)}, u32[]{:S(2)}) collective-permute-start(bf16[64,1024]{1,0:T(8,128)(2,1)S(1)} %get-tuple-element.15), channel_id=1, source_target_pairs={{0,16},{4,20},{8,24},{12,28},{16,0},{20,4},{24,8},{28,12},{1,17},{... | collective-permute-start | bytes 393224 | tf_op jit(solution)/shard_map/ppermute | solution.py:32
  8.8 0.6 collective-permute-start.3
  9.4 5.2 %collective-permute-done.mine_ref = bf16[64,1024]{1,0:T(8,128)(2,1)S(1)} collective-permute-done((bf16[64,1024]{1,0:T(8,128)(2,1)S(1)}, bf16[64,1024]{1,0:T(8,128)(2,1)S(1)}, u32[]{:S(2)}, u32[]{:S(2)}) %collective-permute-start) | collective-permute-done | bytes 131104 | tf_op jit(solution)/shard_map/ppermute | solution.py:32
  14.6 2.7 %collective-permute-done.3 = f32[16,512]{1,0:T(8,128)S(1)} collective-permute-done((f32[16,512]{1,0:T(8,128)S(1)}, f32[16,512]{1,0:T(8,128)S(1)}, u32[]{:S(2)}, u32[]{:S(2)}) %collective-permute-start.3) | collective-permute-done | bytes 32800 | tf_op jit(solution)/shard_map/ppermute | solution.py:32
  17.4 1.8 %collective-permute-start.4 = (f32[16,512]{1,0:T(8,128)S(1)}, f32[16,512]{1,0:T(8,128)S(1)}, u32[]{:S(2)}, u32[]{:S(2)}) collective-permute-start(f32[16,512]{1,0:T(8,128)S(1)} %add.11), channel_id=1, source_target_pairs={{0,8},{4,12},{8,0},{12,4},{16,24},{20,28},{24,16},{28,20},{1,9},{5... | collective-permute-start | bytes 98312 | tf_op jit(solution)/shard_map/ppermute | solution.py:32
  19.2 2.1 %collective-permute-done.4 = f32[16,512]{1,0:T(8,128)S(1)} collective-permute-done((f32[16,512]{1,0:T(8,128)S(1)}, f32[16,512]{1,0:T(8,128)S(1)}, u32[]{:S(2)}, u32[]{:S(2)}) %collective-permute-start.4) | collective-permute-done | bytes 32800 | tf_op jit(solution)/shard_map/ppermute | solution.py:32
  21.3 2.8 %collective-permute-start.5 = (f32[16,512]{1,0:T(8,128)S(1)}, f32[16,512]{1,0:T(8,128)S(1)}, u32[]{:S(2)}, u32[]{:S(2)}) collective-permute-start(f32[16,512]{1,0:T(8,128)S(1)} %add.12), channel_id=1, source_target_pairs={{0,16},{4,20},{8,24},{12,28},{16,0},{20,4},{24,8},{28,12},{1,17},{... | collective-permute-start | bytes 98312 | tf_op jit(solution)/shard_map/ppermute | solution.py:32
  24.1 2.0 %collective-permute-done.5 = f32[16,512]{1,0:T(8,128)S(1)} collective-permute-done((f32[16,512]{1,0:T(8,128)S(1)}, f32[16,512]{1,0:T(8,128)S(1)}, u32[]{:S(2)}, u32[]{:S(2)}) %collective-permute-start.5) | collective-permute-done | bytes 32800 | tf_op jit(solution)/shard_map/ppermute | solution.py:32
  26.2 0.5 collective-permute-start.12
  26.6 0.7 collective-permute-done.6.beside_ref
  27.4 2.2 %shard_map.146 = (bf16[256,512]{1,0:T(8,128)(2,1)S(1)}, bf16[128,512]{1,0:T(8,128)(2,1)S(1)}, bf16[256,2048]{1,0:T(8,128)(2,1)S(1)}, f32[8,2048]{1,0:T(8,128)S(1)}) custom-call(bf16[256,2048]{1,0:T(8,128)(2,1)S(1)} %copy-done.3, bf16[64,2048]{1,0:T(8,128)(2,1)S(1)} %copy-done.10, bf16[64,1024]{1,0:T(8,128)(2,1)S(1)} %collective-permute-done.mine_ref, ...), custom_call_target="tpu_custom_call" | custom-call | flops 137438953472 | bytes 1048576 | tf_op jit(solution)/shard_map/pallas_call | solution.py:37
  29.7 1.8 %collective-permute-start.8 = (bf16[128,512]{1,0:T(8,128)(2,1)S(1)}, bf16[128,512]{1,0:T(8,128)(2,1)S(1)}, u32[]{:S(2)}, u32[]{:S(2)}) collective-permute-start(bf16[128,512]{1,0:T(8,128)(2,1)S(1)} %get-tuple-element.20.refs_2_), channel_id=1, source_target_pairs={{0,4},{4,0},{8,12},{12,8},{16,20},{20,16},{24,28},{28,24},{1,5},{5... | collective-permute-start | bytes 393224 | tf_op jit(solution)/shard_map/ppermute | solution.py:32
  31.5 1.5 %collective-permute-start.16 = (bf16[256,2048]{1,0:T(8,128)(2,1)}, bf16[256,2048]{1,0:T(8,128)(2,1)S(1)}, u32[]{:S(2)}, u32[]{:S(2)}) collective-permute-start(bf16[256,2048]{1,0:T(8,128)(2,1)} %refs_0_.1), channel_id=1, source_target_pairs={{0,2},{1,3},{2,0},{3,1},{4,6},{5,7},{6,4},{7,5},{8,10},{9,11},{10,... | collective-permute-start | bytes 3145736 | tf_op jit(solution)/shard_map/ppermute | solution.py:32
  33.0 1.0 %shard_map.148.refs_3_.refs_4_ = f32[4,14,64,128]{3,2,1,0:T(8,128)S(1)} custom-call(f32[4,15,128]{2,1,0:T(8,128)S(1)} %pad.4.bias_ref), custom_call_target="tpu_custom_call" | custom-call | tf_op jit(solution)/shard_map/pallas_call | solution.py:37
  34.0 1.6 %collective-permute-start.9 = (bf16[128,512]{1,0:T(8,128)(2,1)S(1)}, bf16[128,512]{1,0:T(8,128)(2,1)S(1)}, u32[]{:S(2)}, u32[]{:S(2)}) collective-permute-start(bf16[128,512]{1,0:T(8,128)(2,1)S(1)} %get-tuple-element.20.refs_2_), channel_id=1, source_target_pairs={{0,8},{4,12},{8,0},{12,4},{16,24},{20,28},{24,16},{28,20},{1,9},{5... | collective-permute-start | bytes 393224 | tf_op jit(solution)/shard_map/ppermute | solution.py:32
  35.7 0.7 shard_map.147.q_ref
  36.4 0.7 collective-permute-start.7
  37.1 3.4 %collective-permute-start.10 = (bf16[128,512]{1,0:T(8,128)(2,1)S(1)}, bf16[128,512]{1,0:T(8,128)(2,1)S(1)}, u32[]{:S(2)}, u32[]{:S(2)}) collective-permute-start(bf16[128,512]{1,0:T(8,128)(2,1)S(1)} %collective-permute-done.8.refs_1_), channel_id=1, source_target_pairs={{0,8},{4,12},{8,0},{12,4},{16,24},{20,28},{24,16},{28,20},{1,9},{5... | collective-permute-start | bytes 393224 | tf_op jit(solution)/shard_map/ppermute | solution.py:32
  40.5 1.8 %shard_map.149.refs_1_ = bf16[256,512]{1,0:T(8,128)(2,1)S(1)} custom-call(bf16[256,1024]{1,0:T(8,128)(2,1)S(1)} %collective-permute-done.11.mine_ref, bf16[256,1024]{1,0:T(8,128)(2,1)S(1)} %collective-permute-done.12.passed_ref, f32[8,2048]{1,0:T(8,128)S(1)} %get-tuple-element.17.vec_ref.gate_ref, f32[1,2048]{1,0:T(1,128)S(1)} %bitcast.6, ...), custom_call_target="tpu_custom_call" | custom-call | tf_op jit(solution)/shard_map/pallas_call | solution.py:37
  42.3 1.4 %shard_map.150 = (f32[256,256]{1,0:T(8,128)S(1)}, f32[256,256]{1,0:T(8,128)S(1)}, f32[256,256]{1,0:T(8,128)S(1)}) custom-call(bf16[256,256]{1,0:T(8,128)(2,1)S(1)} %shard_map.147.q_ref, bf16[256,512]{1,0:T(8,128)(2,1)S(1)} %get-tuple-element.19.refs_0_, bf16[256,512]{1,0:T(8,128)(2,1)S(1)} %shard_map.149.refs_1_, ...), custom_call_target="tpu_custom_call" | custom-call | flops 137438953472 | bytes 1048576 | tf_op jit(solution)/shard_map/pallas_call | solution.py:37
  43.7 13.6 %collective-permute-done.16.refs_0_ = bf16[256,2048]{1,0:T(8,128)(2,1)S(1)} collective-permute-done((bf16[256,2048]{1,0:T(8,128)(2,1)}, bf16[256,2048]{1,0:T(8,128)(2,1)S(1)}, u32[]{:S(2)}, u32[]{:S(2)}) %collective-permute-start.16) | collective-permute-done | bytes 1048608 | tf_op jit(solution)/shard_map/ppermute | solution.py:32
  57.3 1.8 %shard_map.151.refs_0_ = bf16[256,256]{1,0:T(8,128)(2,1)S(1)} custom-call(bf16[256,256]{1,0:T(8,128)(2,1)S(1)} %shard_map.147.q_ref, bf16[256,512]{1,0:T(8,128)(2,1)S(1)} %collective-permute-done.7.refs_0_, bf16[128,512]{1,0:T(8,128)(2,1)S(1)} %collective-permute-done.8.refs_1_, bf16[128,512]{1,0:T(8,128)(2,1)S(1)} %collective-permute-done.9.refs_2_, ...), custom_call_target="tpu_custom_call" | custom-call | flops 137438953472 | bytes 1048576 | tf_op jit(solution)/shard_map/pallas_call | solution.py:37
  59.1 1.6 %collective-permute-start.15 = (bf16[256,256]{1,0:T(8,128)(2,1)S(1)}, bf16[256,256]{1,0:T(8,128)(2,1)S(1)}, u32[]{:S(2)}, u32[]{:S(2)}) collective-permute-start(bf16[256,256]{1,0:T(8,128)(2,1)S(1)} %shard_map.151.refs_0_), channel_id=1, source_target_pairs={{0,2},{1,3},{2,0},{3,1},{4,6},{5,7},{6,4},{7,5},{8,10},{9,11},{10,... | collective-permute-start | bytes 393224 | tf_op jit(solution)/shard_map/ppermute | solution.py:32
  60.9 4.2 %collective-permute-done.15.refs_1_ = bf16[256,256]{1,0:T(8,128)(2,1)S(1)} collective-permute-done((bf16[256,256]{1,0:T(8,128)(2,1)S(1)}, bf16[256,256]{1,0:T(8,128)(2,1)S(1)}, u32[]{:S(2)}, u32[]{:S(2)}) %collective-permute-start.15) | collective-permute-done | bytes 131104 | tf_op jit(solution)/shard_map/ppermute | solution.py:32
  65.1 1.2 %shard_map.152.refs_2_ = bf16[256,2048]{1,0:T(8,128)(2,1)S(1)} custom-call(bf16[256,2048]{1,0:T(8,128)(2,1)} %refs_0_.1), custom_call_target="tpu_custom_call" | custom-call | tf_op jit(solution)/shard_map/pallas_call | solution.py:37
  66.3 1.2 %shard_map.154.refs_2_ = bf16[256,2048]{1,0:T(8,128)(2,1)S(1)} custom-call(bf16[256,2048]{1,0:T(8,128)(2,1)} %copy-done.11), custom_call_target="tpu_custom_call" | custom-call | tf_op jit(solution)/shard_map/pallas_call | solution.py:37
  67.6 3.0 %shard_map.153.refs_0_ = f32[256,2048]{1,0:T(8,128)S(1)} custom-call(bf16[256,256]{1,0:T(8,128)(2,1)S(1)} %shard_map.151.refs_0_, bf16[256,256]{1,0:T(8,128)(2,1)S(1)} %collective-permute-done.13.refs_1_, bf16[256,2048]{1,0:T(8,128)(2,1)S(1)} %shard_map.152.refs_2_, bf16[256,2048]{1,0:T(8,128)(2,1)} %collective-permute-done.14.refs_3_), custom_call_target="tpu_custom_call" | custom-call | tf_op jit(solution)/shard_map/pallas_call | solution.py:37
  70.6 1.4 %shard_map.155.sum_ref = f32[256,2048]{1,0:T(8,128)S(1)} custom-call(f32[256,2048]{1,0:T(8,128)S(1)} %shard_map.153.refs_0_, bf16[256,256]{1,0:T(8,128)(2,1)S(1)} %collective-permute-done.15.refs_1_, bf16[256,2048]{1,0:T(8,128)(2,1)S(1)} %shard_map.154.refs_2_), custom_call_target="tpu_custom_call" | custom-call | tf_op jit(solution)/shard_map/pallas_call | solution.py:37
  72.0 2.5 %shard_map.156 = bf16[256,2048]{1,0:T(8,128)(2,1)} custom-call(bf16[256,2048]{1,0:T(8,128)(2,1)S(1)} %copy-done.4, f32[8,2048]{1,0:T(8,128)S(1)} %copy-done.6, f32[256,2048]{1,0:T(8,128)S(1)} %shard_map.155.sum_ref, bf16[256,256]{1,0:T(8,128)(2,1)S(1)} %collective-permute-done.17.refs_0_, bf16[256,2048]{1,0:T(8,128)(2,1)S(1)} %collective-permute-done.18.refs_1_), custom_call_target="tpu_custom_call" | custom-call | tf_op jit(solution)/shard_map/pallas_call | solution.py:37
  (51 shorter events, 0.4 us)
Async XLA Ops:
  0.0 27.3 %copy-start.1 = (bf16[2048,256]{1,0:T(8,128)(2,1)S(1)}, bf16[2048,256]{1,0:T(8,128)(2,1)}, u32[]{:S(2)}) copy-start(bf16[2048,256]{1,0:T(8,128)(2,1)} %wk.1) | copy-start | bytes 3145732
  0.0 27.3 %copy-start.2 = (bf16[2048,256]{1,0:T(8,128)(2,1)S(1)}, bf16[2048,256]{1,0:T(8,128)(2,1)}, u32[]{:S(2)}) copy-start(bf16[2048,256]{1,0:T(8,128)(2,1)} %wv.1) | copy-start | bytes 3145732
  0.0 27.4 %copy-start.3 = (bf16[256,2048]{1,0:T(8,128)(2,1)S(1)}, bf16[256,2048]{1,0:T(8,128)(2,1)}, u32[]{:S(2)}) copy-start(bf16[256,2048]{1,0:T(8,128)(2,1)} %lat_ref.5) | copy-start | bytes 3145732
  0.0 27.4 %copy-start.7 = (f32[2048]{0:T(1024)S(1)}, f32[2048]{0:T(1024)}, u32[]{:S(2)}) copy-start(f32[2048]{0:T(1024)} %param.22) | copy-start | bytes 24580
  0.0 27.4 %copy-start.9 = (f32[64]{0:T(128)S(1)}, f32[64]{0:T(128)}, u32[]{:S(2)}) copy-start(f32[64]{0:T(128)} %param.27) | copy-start | bytes 772
  0.0 27.4 %copy-start.10 = (bf16[64,2048]{1,0:T(8,128)(2,1)S(1)}, bf16[64,2048]{1,0:T(8,128)(2,1)}, u32[]{:S(2)}) copy-start(bf16[64,2048]{1,0:T(8,128)(2,1)} %ctx_ref.3) | copy-start | bytes 786436
  1.7 24.5 %collective-permute-start.11 = (bf16[256,1024]{1,0:T(8,128)(2,1)S(1)}, bf16[256,1024]{1,0:T(8,128)(2,1)S(1)}, u32[]{:S(2)}, u32[]{:S(2)}) collective-permute-start(bf16[256,1024]{1,0:T(8,128)(2,1)S(1)} %get-tuple-element.21), channel_id=1, source_target_pairs={{0,4},{4,0},{8,12},{12,8},{16,20},{20,16},{24,28},{28,24},{1,5},{5... | collective-permute-start | bytes 1572872 | tf_op jit(solution)/shard_map/ppermute | solution.py:32
  4.8 4.1 %collective-permute-start.2 = (f32[8,512]{1,0:T(8,128)S(1)}, f32[8,512]{1,0:T(8,128)S(1)}, u32[]{:S(2)}, u32[]{:S(2)}) collective-permute-start(f32[8,512]{1,0:T(8,128)S(1)} %get-tuple-element.16), channel_id=1, source_target_pairs={{0,2},{1,3},{2,0},{3,1},{4,6},{5,7},{6,4},{7,5},{8,10},{9,11},{10,... | collective-permute-start | bytes 49160 | tf_op jit(solution)/shard_map/ppermute | solution.py:32
  6.2 8.4 %collective-permute-start = (bf16[64,1024]{1,0:T(8,128)(2,1)S(1)}, bf16[64,1024]{1,0:T(8,128)(2,1)S(1)}, u32[]{:S(2)}, u32[]{:S(2)}) collective-permute-start(bf16[64,1024]{1,0:T(8,128)(2,1)S(1)} %get-tuple-element.15), channel_id=1, source_target_pairs={{0,16},{4,20},{8,24},{12,28},{16,0},{20,4},{24,8},{28,12},{1,17},{... | collective-permute-start | bytes 393224 | tf_op jit(solution)/shard_map/ppermute | solution.py:32
  8.8 8.5 %collective-permute-start.3 = (f32[16,512]{1,0:T(8,128)S(1)}, f32[16,512]{1,0:T(8,128)S(1)}, u32[]{:S(2)}, u32[]{:S(2)}) collective-permute-start(f32[16,512]{1,0:T(8,128)S(1)} %constant_dynamic-update-slice_fusion), channel_id=1, source_target_pairs={{0,4},{4,0},{8,12},{12,8},{16,20},{20,16},{24,28},{28,24},{1,5},{5... | collective-permute-start | bytes 98312 | tf_op jit(solution)/shard_map/ppermute | solution.py:32
  14.6 12.7 %collective-permute-start.1 = (bf16[64,1024]{1,0:T(8,128)(2,1)S(1)}, bf16[64,1024]{1,0:T(8,128)(2,1)S(1)}, u32[]{:S(2)}, u32[]{:S(2)}) collective-permute-start(bf16[64,1024]{1,0:T(8,128)(2,1)S(1)} %collective-permute-done.mine_ref), channel_id=1, source_target_pairs={{0,1},{1,0},{2,3},{3,2},{4,5},{5,4},{6,7},{7,6},{8,9},{9,8},{10,11... | collective-permute-start | bytes 393224 | tf_op jit(solution)/shard_map/ppermute | solution.py:32
  17.4 3.9 %collective-permute-start.4 = (f32[16,512]{1,0:T(8,128)S(1)}, f32[16,512]{1,0:T(8,128)S(1)}, u32[]{:S(2)}, u32[]{:S(2)}) collective-permute-start(f32[16,512]{1,0:T(8,128)S(1)} %add.11), channel_id=1, source_target_pairs={{0,8},{4,12},{8,0},{12,4},{16,24},{20,28},{24,16},{28,20},{1,9},{5... | collective-permute-start | bytes 98312 | tf_op jit(solution)/shard_map/ppermute | solution.py:32
  21.3 4.8 %collective-permute-start.5 = (f32[16,512]{1,0:T(8,128)S(1)}, f32[16,512]{1,0:T(8,128)S(1)}, u32[]{:S(2)}, u32[]{:S(2)}) collective-permute-start(f32[16,512]{1,0:T(8,128)S(1)} %add.12), channel_id=1, source_target_pairs={{0,16},{4,20},{8,24},{12,28},{16,0},{20,4},{24,8},{28,12},{1,17},{... | collective-permute-start | bytes 98312 | tf_op jit(solution)/shard_map/ppermute | solution.py:32
  26.1 1.2 %collective-permute-start.6 = (f32[16,512]{1,0:T(8,128)S(1)}, f32[16,512]{1,0:T(8,128)S(1)}, u32[]{:S(2)}, u32[]{:S(2)}) collective-permute-start(f32[16,512]{1,0:T(8,128)S(1)} %add.13.part_ref), channel_id=1, source_target_pairs={{0,1},{1,0},{2,3},{3,2},{4,5},{5,4},{6,7},{7,6},{8,9},{9,8},{10,11... | collective-permute-start | bytes 98312 | tf_op jit(solution)/shard_map/ppermute | solution.py:32
  26.2 10.9 %collective-permute-start.12 = (bf16[256,1024]{1,0:T(8,128)(2,1)S(1)}, bf16[256,1024]{1,0:T(8,128)(2,1)S(1)}, u32[]{:S(2)}, u32[]{:S(2)}) collective-permute-start(bf16[256,1024]{1,0:T(8,128)(2,1)S(1)} %collective-permute-done.11.mine_ref), channel_id=1, source_target_pairs={{0,1},{1,0},{2,3},{3,2},{4,5},{5,4},{6,7},{7,6},{8,9},{9,8},{10,11... | collective-permute-start | bytes 1572872 | tf_op jit(solution)/shard_map/ppermute | solution.py:32
  27.4 5.6 %copy-start.12 = (f32[4,15,31]{2,0,1:T(4,128)S(1)}, f32[4,15,31]{2,0,1:T(4,128)}, u32[]{:S(2)}) copy-start(f32[4,15,31]{2,0,1:T(4,128)} %param.28) | copy-start | bytes 22324
  27.4 8.3 %copy-start.8 = (f32[64]{0:T(128)S(1)}, f32[64]{0:T(128)}, u32[]{:S(2)}) copy-start(f32[64]{0:T(128)} %param.26) | copy-start | bytes 772
  29.7 10.8 %copy-start.5 = (f32[8,2048]{1,0:T(8,128)}, f32[8,2048]{1,0:T(8,128)S(1)}, u32[]{:S(2)}) copy-start(f32[8,2048]{1,0:T(8,128)S(1)} %get-tuple-element.17.vec_ref.gate_ref) | copy-start | bytes 196612
  29.7 6.0 %copy-start = (bf16[2048,256]{1,0:T(8,128)(2,1)S(1)}, bf16[2048,256]{1,0:T(8,128)(2,1)}, u32[]{:S(2)}) copy-start(bf16[2048,256]{1,0:T(8,128)(2,1)} %wq_ref.1) | copy-start | bytes 3145732
  29.7 6.7 %collective-permute-start.8 = (bf16[128,512]{1,0:T(8,128)(2,1)S(1)}, bf16[128,512]{1,0:T(8,128)(2,1)S(1)}, u32[]{:S(2)}, u32[]{:S(2)}) collective-permute-start(bf16[128,512]{1,0:T(8,128)(2,1)S(1)} %get-tuple-element.20.refs_2_), channel_id=1, source_target_pairs={{0,4},{4,0},{8,12},{12,8},{16,20},{20,16},{24,28},{28,24},{1,5},{5... | collective-permute-start | bytes 393224 | tf_op jit(solution)/shard_map/ppermute | solution.py:32
  31.5 36.1 %collective-permute-start.14 = (bf16[256,2048]{1,0:T(8,128)(2,1)}, bf16[256,2048]{1,0:T(8,128)(2,1)}, u32[]{:S(2)}, u32[]{:S(2)}) collective-permute-start(bf16[256,2048]{1,0:T(8,128)(2,1)} %refs_0_.1), channel_id=1, source_target_pairs={{0,1},{1,0},{2,3},{3,2},{4,5},{5,4},{6,7},{7,6},{8,9},{9,8},{10,11... | collective-permute-start | bytes 3145736 | tf_op jit(solution)/shard_map/ppermute | solution.py:32
  31.5 25.8 %collective-permute-start.16 = (bf16[256,2048]{1,0:T(8,128)(2,1)}, bf16[256,2048]{1,0:T(8,128)(2,1)S(1)}, u32[]{:S(2)}, u32[]{:S(2)}) collective-permute-start(bf16[256,2048]{1,0:T(8,128)(2,1)} %refs_0_.1), channel_id=1, source_target_pairs={{0,2},{1,3},{2,0},{3,1},{4,6},{5,7},{6,4},{7,5},{8,10},{9,11},{10,... | collective-permute-start | bytes 3145736 | tf_op jit(solution)/shard_map/ppermute | solution.py:32
  34.0 23.3 %collective-permute-start.9 = (bf16[128,512]{1,0:T(8,128)(2,1)S(1)}, bf16[128,512]{1,0:T(8,128)(2,1)S(1)}, u32[]{:S(2)}, u32[]{:S(2)}) collective-permute-start(bf16[128,512]{1,0:T(8,128)(2,1)S(1)} %get-tuple-element.20.refs_2_), channel_id=1, source_target_pairs={{0,8},{4,12},{8,0},{12,4},{16,24},{20,28},{24,16},{28,20},{1,9},{5... | collective-permute-start | bytes 393224 | tf_op jit(solution)/shard_map/ppermute | solution.py:32
  36.4 20.9 %collective-permute-start.7 = (bf16[256,512]{1,0:T(8,128)(2,1)S(1)}, bf16[256,512]{1,0:T(8,128)(2,1)S(1)}, u32[]{:S(2)}, u32[]{:S(2)}) collective-permute-start(bf16[256,512]{1,0:T(8,128)(2,1)S(1)} %get-tuple-element.19.refs_0_), channel_id=1, source_target_pairs={{4,8},{12,16},{20,24},{8,4},{16,12},{24,20},{5,9},{13,17},{21,25},... | collective-permute-start | bytes 786440 | tf_op jit(solution)/shard_map/ppermute | solution.py:477
  37.1 20.2 %collective-permute-start.10 = (bf16[128,512]{1,0:T(8,128)(2,1)S(1)}, bf16[128,512]{1,0:T(8,128)(2,1)S(1)}, u32[]{:S(2)}, u32[]{:S(2)}) collective-permute-start(bf16[128,512]{1,0:T(8,128)(2,1)S(1)} %collective-permute-done.8.refs_1_), channel_id=1, source_target_pairs={{0,8},{4,12},{8,0},{12,4},{16,24},{20,28},{24,16},{28,20},{1,9},{5... | collective-permute-start | bytes 393224 | tf_op jit(solution)/shard_map/ppermute | solution.py:32
  57.3 1.8 %copy-start.11 = (bf16[256,2048]{1,0:T(8,128)(2,1)}, bf16[256,2048]{1,0:T(8,128)(2,1)S(1)}, u32[]{:S(2)}) copy-start(bf16[256,2048]{1,0:T(8,128)(2,1)S(1)} %collective-permute-done.16.refs_0_) | copy-start | bytes 3145732
  57.3 14.7 %collective-permute-start.18 = (bf16[256,2048]{1,0:T(8,128)(2,1)S(1)}, bf16[256,2048]{1,0:T(8,128)(2,1)S(1)}, u32[]{:S(2)}, u32[]{:S(2)}) collective-permute-start(bf16[256,2048]{1,0:T(8,128)(2,1)S(1)} %collective-permute-done.16.refs_0_), channel_id=1, source_target_pairs={{0,1},{1,0},{2,3},{3,2},{4,5},{5,4},{6,7},{7,6},{8,9},{9,8},{10,11... | collective-permute-start | bytes 3145736 | tf_op jit(solution)/shard_map/ppermute | solution.py:32
  59.1 6.0 %collective-permute-start.15 = (bf16[256,256]{1,0:T(8,128)(2,1)S(1)}, bf16[256,256]{1,0:T(8,128)(2,1)S(1)}, u32[]{:S(2)}, u32[]{:S(2)}) collective-permute-start(bf16[256,256]{1,0:T(8,128)(2,1)S(1)} %shard_map.151.refs_0_), channel_id=1, source_target_pairs={{0,2},{1,3},{2,0},{3,1},{4,6},{5,7},{6,4},{7,5},{8,10},{9,11},{10,... | collective-permute-start | bytes 393224 | tf_op jit(solution)/shard_map/ppermute | solution.py:32
  60.7 6.9 %collective-permute-start.13 = (bf16[256,256]{1,0:T(8,128)(2,1)S(1)}, bf16[256,256]{1,0:T(8,128)(2,1)S(1)}, u32[]{:S(2)}, u32[]{:S(2)}) collective-permute-start(bf16[256,256]{1,0:T(8,128)(2,1)S(1)} %shard_map.151.refs_0_), channel_id=1, source_target_pairs={{0,1},{1,0},{2,3},{3,2},{4,5},{5,4},{6,7},{7,6},{8,9},{9,8},{10,11... | collective-permute-start | bytes 393224 | tf_op jit(solution)/shard_map/ppermute | solution.py:32
  65.1 6.9 %collective-permute-start.17 = (bf16[256,256]{1,0:T(8,128)(2,1)S(1)}, bf16[256,256]{1,0:T(8,128)(2,1)S(1)}, u32[]{:S(2)}, u32[]{:S(2)}) collective-permute-start(bf16[256,256]{1,0:T(8,128)(2,1)S(1)} %collective-permute-done.15.refs_1_), channel_id=1, source_target_pairs={{0,1},{1,0},{2,3},{3,2},{4,5},{5,4},{6,7},{7,6},{8,9},{9,8},{10,11... | collective-permute-start | bytes 393224 | tf_op jit(solution)/shard_map/ppermute | solution.py:32
  70.6 1.4 %copy-start.4 = (bf16[256,2048]{1,0:T(8,128)(2,1)S(1)}, bf16[256,2048]{1,0:T(8,128)(2,1)}, u32[]{:S(2)}) copy-start(bf16[256,2048]{1,0:T(8,128)(2,1)} %lat_ref.5) | copy-start | bytes 3145732
  70.6 1.4 %copy-start.6 = (f32[8,2048]{1,0:T(8,128)S(1)}, f32[8,2048]{1,0:T(8,128)}, u32[]{:S(2)}) copy-start(f32[8,2048]{1,0:T(8,128)} %copy-done.5) | copy-start | bytes 196612

commit v3 on v2

--- a/solution.py
+++ b/solution.py
@@ -163,28 +163,25 @@
     lat_count = lat_ref.shape[0]
     ctx_count = ctx_ref.shape[0]
     for here in row_steps(lat_count):
-        hid_ref[here, :] = modulated(lat_ref[here, :].astype(F32), vec_ref, gain_ref, 0)
+        lat_hid_ref[here, :] = modulated(lat_ref[here, :].astype(F32), vec_ref, gain_ref, 0)
     if ctx_count % 32:
         both = jnp.concatenate(
             [ctx_ref[...].astype(F32), ctx_two_ref[...].astype(F32)], axis=0
         )
-        hid_ref[lat_count:, :] = modulated(both, vec_ref, gain_ref, 1)
+        hid_ref[...] = modulated(both, vec_ref, gain_ref, 1)
     else:
         for n, ref in enumerate((ctx_ref, ctx_two_ref)):
-            base = lat_count + n * ctx_count
+            base = n * ctx_count
             for here in row_steps(ctx_count):
                 hid_ref[base + here.start : base + here.stop, :] = modulated(
                     ref[here, :].astype(F32), vec_ref, gain_ref, 1
                 )
     cols = wk.shape[1]
-    hidden = hid_ref[...]
-    keys = head_norm(jnp.dot(hidden, wk[...], preferred_element_type=F32), kg_ref).astype(BF16)
-    kv_ref[:, :cols] = keys[:lat_count]
-    ckv_ref[:, :cols] = keys[lat_count:]
-    values = jnp.dot(hidden, wv[...], preferred_element_type=F32).astype(BF16)
-    kv_ref[:, cols:] = values[:lat_count]
-    ckv_ref[:, cols:] = values[lat_count:]
-    lat_hid_ref[...] = hidden[:lat_count]
+    for out, src in ((kv_ref, lat_hid_ref[...]), (ckv_ref, hid_ref[...])):
+        out[:, :cols] = head_norm(
+            jnp.dot(src, wk[...], preferred_element_type=F32), kg_ref
+        ).astype(BF16)
+        out[:, cols:] = jnp.dot(src, wv[...], preferred_element_type=F32).astype(BF16)
 
 
 def near_body(mine_ref, passed_ref, vec_ref, gain_ref, kg_ref, wk, wv, kv_ref, lat_ref, hid_ref):
@@ -192,11 +189,15 @@
     for here in row_steps(lat_ref.shape[0]):
         hid_ref[here, :] = modulated(lat_ref[here, :].astype(F32), vec_ref, gain_ref, 0)
     cols = wk.shape[1]
-    hidden = hid_ref[...]
-    kv_ref[:, :cols] = head_norm(
-        jnp.dot(hidden, wk[...], preferred_element_type=F32), kg_ref
-    ).astype(BF16)
-    kv_ref[:, cols:] = jnp.dot(hidden, wv[...], preferred_element_type=F32).astype(BF16)
+    step = lat_ref.shape[0] // 2
+    for at in range(0, lat_ref.shape[0], step):
+        hidden = hid_ref[at : at + step, :]
+        kv_ref[at : at + step, :cols] = head_norm(
+            jnp.dot(hidden, wk[...], preferred_element_type=F32), kg_ref
+        ).astype(BF16)
+        kv_ref[at : at + step, cols:] = jnp.dot(
+            hidden, wv[...], preferred_element_type=F32
+        ).astype(BF16)
 
 
 def query_body(hid_ref, wq_ref, qg_ref, q_ref):
@@ -249,13 +250,13 @@
                 opens[n, i, p] = jnp.where(
                     (row >= start) & (row < start + WIN_ROWS), 0.0, MASKED
                 )
-    tops = jnp.zeros((tokens, cols), F32)
-    sums = jnp.zeros((tokens, cols), F32)
-    total = jnp.zeros((tokens, cols), F32)
-    for h in range(heads):
-        mine = lane_head == h
+    masks = [lane_head == h for h in range(heads)]
+    all_scores = []
+    for mine in masks:
         q_h = jnp.where(mine, q_all, jnp.zeros_like(q_all))
-        scores = [bt_dot(q_h, k) for k in keys]
+        all_scores.append([bt_dot(q_h, k) for k in keys])
+    all_powers, tops, sums = [], None, None
+    for h, scores in enumerate(all_scores):
         for n in range(n_lat):
             lines = []
             for i in range(rows):
@@ -271,16 +272,16 @@
         top = functools.reduce(jnp.maximum, [jnp.max(s, axis=1, keepdims=True) for s in scores])
         powers = [jnp.exp(s - top) for s in scores]
         denom = functools.reduce(jnp.add, [jnp.sum(e, axis=1, keepdims=True) for e in powers])
+        all_powers.append([e.astype(BF16) for e in powers])
+        tops = jnp.broadcast_to(top, (tokens, cols)) if h == 0 else jnp.where(masks[h], top, tops)
+        sums = jnp.broadcast_to(denom, (tokens, cols)) if h == 0 else jnp.where(masks[h], denom, sums)
+    total = None
+    for h, powers in enumerate(all_powers):
         acc = functools.reduce(
             jnp.add,
-            [
-                jnp.dot(e.astype(BF16), v, preferred_element_type=F32)
-                for e, v in zip(powers, values)
-            ],
+            [jnp.dot(e, v, preferred_element_type=F32) for e, v in zip(powers, values)],
         )
-        tops = jnp.where(mine, top, tops)
-        sums = jnp.where(mine, denom, sums)
-        total = jnp.where(mine, acc, total)
+        total = acc if h == 0 else jnp.where(masks[h], acc, total)
     if has_prev:
         before = prev[0][...]
         both = jnp.maximum(before, tops)
@@ -438,7 +439,7 @@
         in_specs=vmem(10),
         out_specs=vmem(4),
         scratch_shapes=[
-            pltpu.VMEM((tokens + ctx_count, width), BF16),
+            pltpu.VMEM((ctx_count, width), BF16),
             pltpu.VMEM(context.shape, BF16),
         ],
         compiler_params=params(20),
@@ -518,7 +519,7 @@
     near = [n for n, (code, _) in enumerate(att_blocks) if code < 2]
     cross = [n for n, (code, _) in enumerate(att_blocks) if code > 1 and n < len(att_blocks) // 2]
     far = [n for n in range(len(att_blocks)) if n not in near + cross]
-    tile = min(512, width)
+    tile = min(1024, width)
     att_spec = pl.BlockSpec((tokens, cols), lambda n: (0, 0))
     weight_spec = pl.BlockSpec((cols, tile), lambda n: (0, n))
     wide_spec = pl.BlockSpec((tokens, tile), lambda n: (0, n))
@@ -531,18 +532,16 @@
 
     partial_sum = call(
         functools.partial(first_body, len(near), False),
-        grid=(width // tile,),
         out_shape=jax.ShapeDtypeStruct((tokens, width), F32),
-        in_specs=specs(near),
-        out_specs=wide_spec,
+        in_specs=vmem(2 * len(near)),
+        out_specs=vmem(1)[0],
         compiler_params=params(24),
     )(*operands(near))
     partial_sum = call(
         functools.partial(first_body, len(cross), True),
-        grid=(width // tile,),
         out_shape=jax.ShapeDtypeStruct((tokens, width), F32),
-        in_specs=[wide_spec] + specs(cross),
-        out_specs=wide_spec,
+        in_specs=vmem(1 + 2 * len(cross)),
+        out_specs=vmem(1)[0],
         compiler_params=params(24),
     )(partial_sum, *operands(cross))
     return call(

time: 74.7 us -> 72.4 us (0.969)
  Pallas kernels: 19.9 us -> 16.5 us
    pallas_call x12, Pallas kernels: 19.9 us -> 16.5 us  [run(): return pl.pallas_call(*args, **kwargs)(*operands)]
  transfers between devices with their start and end apart: 19 -> 19, of which waited for: 7 -> 7; matrix products, arithmetic and copies ran while one was open for 0% -> 0% of each run, Pallas kernels for 21% -> 18%
where the time goes in v3:
time: 72.4 us; the launch traced here: 72.2 us
  waiting for transfers between devices  30.9 us (43%)
  starting transfers between devices  23.6 us (33%)
  Pallas kernels  16.5 us (23%)
  local copies, waits for them, and re-layouts  0.81 us (1%)
    ppermute x18, waiting for transfers between devices, swap(): lax.ppermute(x, axis, [(i, i ^ code) for i in range(lax.axis_size(axis))])  30.9 us
    ppermute x18, starting transfers between devices, swap(): lax.ppermute(x, axis, [(i, i ^ code) for i in range(lax.axis_size(axis))])  22.9 us
    pallas_call x12, Pallas kernels, run(): return pl.pallas_call(*args, **kwargs)(*operands)  16.5 us
  transfers between devices with their start and end apart: 19, of which 7 were waited for; matrix products, arithmetic and copies ran while one was open for 0% of the time, Pallas kernels for 18%

profile of v3, /device:TPU:0, one launch (start us, length us, event | category | flops | bytes accessed | tf_op | source)
XLA Modules:
  0.0 72.2 jit_solution(14076588177033333731)
XLA Ops:
  0.0 1.6 %shard_map.145 = (f32[8,512]{1,0:T(8,128)S(1)}, bf16[64,1024]{1,0:T(8,128)(2,1)S(1)}, bf16[256,1024]{1,0:T(8,128)(2,1)S(1)}) custom-call(f32[1,256]{1,0:T(1,128)} %bitcast.10, f32[1,256]{1,0:T(1,128)} %bitcast.11, bf16[256,512]{1,0:T(8,128)(2,1)} %shift_ref.1, bf16[256,512]{1,0:T(8,128)(2,1)} %scale_ref.1, bf16[256,512]{1,0:T(8,128)(2,1)} %gate_ref.1, ...), custom_call_target="tpu_custom_call" | custom-call | flops 137438953472 | bytes 1048576 | tf_op jit(solution)/shard_map/pallas_call | solution.py:37
  1.7 3.1 %collective-permute-start.11 = (bf16[256,1024]{1,0:T(8,128)(2,1)S(1)}, bf16[256,1024]{1,0:T(8,128)(2,1)S(1)}, u32[]{:S(2)}, u32[]{:S(2)}) collective-permute-start(bf16[256,1024]{1,0:T(8,128)(2,1)S(1)} %get-tuple-element.21), channel_id=1, source_target_pairs={{0,4},{4,0},{8,12},{12,8},{16,20},{20,16},{24,28},{28,24},{1,5},{5... | collective-permute-start | bytes 1572872 | tf_op jit(solution)/shard_map/ppermute | solution.py:32
  4.8 1.5 %collective-permute-start.2 = (f32[8,512]{1,0:T(8,128)S(1)}, f32[8,512]{1,0:T(8,128)S(1)}, u32[]{:S(2)}, u32[]{:S(2)}) collective-permute-start(f32[8,512]{1,0:T(8,128)S(1)} %get-tuple-element.16), channel_id=1, source_target_pairs={{0,2},{1,3},{2,0},{3,1},{4,6},{5,7},{6,4},{7,5},{8,10},{9,11},{10,... | collective-permute-start | bytes 49160 | tf_op jit(solution)/shard_map/ppermute | solution.py:32
  6.2 2.6 %collective-permute-start = (bf16[64,1024]{1,0:T(8,128)(2,1)S(1)}, bf16[64,1024]{1,0:T(8,128)(2,1)S(1)}, u32[]{:S(2)}, u32[]{:S(2)}) collective-permute-start(bf16[64,1024]{1,0:T(8,128)(2,1)S(1)} %get-tuple-element.15), channel_id=1, source_target_pairs={{0,16},{4,20},{8,24},{12,28},{16,0},{20,4},{24,8},{28,12},{1,17},{... | collective-permute-start | bytes 393224 | tf_op jit(solution)/shard_map/ppermute | solution.py:32
  8.8 0.6 collective-permute-start.3
  9.4 5.2 %collective-permute-done.mine_ref = bf16[64,1024]{1,0:T(8,128)(2,1)S(1)} collective-permute-done((bf16[64,1024]{1,0:T(8,128)(2,1)S(1)}, bf16[64,1024]{1,0:T(8,128)(2,1)S(1)}, u32[]{:S(2)}, u32[]{:S(2)}) %collective-permute-start) | collective-permute-done | bytes 131104 | tf_op jit(solution)/shard_map/ppermute | solution.py:32
  14.6 2.7 %collective-permute-done.3 = f32[16,512]{1,0:T(8,128)S(1)} collective-permute-done((f32[16,512]{1,0:T(8,128)S(1)}, f32[16,512]{1,0:T(8,128)S(1)}, u32[]{:S(2)}, u32[]{:S(2)}) %collective-permute-start.3) | collective-permute-done | bytes 32800 | tf_op jit(solution)/shard_map/ppermute | solution.py:32
  17.4 1.8 %collective-permute-start.4 = (f32[16,512]{1,0:T(8,128)S(1)}, f32[16,512]{1,0:T(8,128)S(1)}, u32[]{:S(2)}, u32[]{:S(2)}) collective-permute-start(f32[16,512]{1,0:T(8,128)S(1)} %add.11), channel_id=1, source_target_pairs={{0,8},{4,12},{8,0},{12,4},{16,24},{20,28},{24,16},{28,20},{1,9},{5... | collective-permute-start | bytes 98312 | tf_op jit(solution)/shard_map/ppermute | solution.py:32
  19.2 2.1 %collective-permute-done.4 = f32[16,512]{1,0:T(8,128)S(1)} collective-permute-done((f32[16,512]{1,0:T(8,128)S(1)}, f32[16,512]{1,0:T(8,128)S(1)}, u32[]{:S(2)}, u32[]{:S(2)}) %collective-permute-start.4) | collective-permute-done | bytes 32800 | tf_op jit(solution)/shard_map/ppermute | solution.py:32
  21.3 2.8 %collective-permute-start.5 = (f32[16,512]{1,0:T(8,128)S(1)}, f32[16,512]{1,0:T(8,128)S(1)}, u32[]{:S(2)}, u32[]{:S(2)}) collective-permute-start(f32[16,512]{1,0:T(8,128)S(1)} %add.12), channel_id=1, source_target_pairs={{0,16},{4,20},{8,24},{12,28},{16,0},{20,4},{24,8},{28,12},{1,17},{... | collective-permute-start | bytes 98312 | tf_op jit(solution)/shard_map/ppermute | solution.py:32
  24.1 2.0 %collective-permute-done.5 = f32[16,512]{1,0:T(8,128)S(1)} collective-permute-done((f32[16,512]{1,0:T(8,128)S(1)}, f32[16,512]{1,0:T(8,128)S(1)}, u32[]{:S(2)}, u32[]{:S(2)}) %collective-permute-start.5) | collective-permute-done | bytes 32800 | tf_op jit(solution)/shard_map/ppermute | solution.py:32
  26.2 0.5 collective-permute-start.12
  26.6 0.7 collective-permute-done.6.beside_ref
  27.4 2.0 %shard_map.146 = (bf16[256,512]{1,0:T(8,128)(2,1)S(1)}, bf16[128,512]{1,0:T(8,128)(2,1)S(1)}, bf16[256,2048]{1,0:T(8,128)(2,1)S(1)}, f32[8,2048]{1,0:T(8,128)S(1)}) custom-call(bf16[256,2048]{1,0:T(8,128)(2,1)S(1)} %copy-done.3, bf16[64,2048]{1,0:T(8,128)(2,1)S(1)} %copy-done.10, bf16[64,1024]{1,0:T(8,128)(2,1)S(1)} %collective-permute-done.mine_ref, ...), custom_call_target="tpu_custom_call" | custom-call | flops 137438953472 | bytes 1048576 | tf_op jit(solution)/shard_map/pallas_call | solution.py:37
  29.5 1.8 %collective-permute-start.8 = (bf16[128,512]{1,0:T(8,128)(2,1)S(1)}, bf16[128,512]{1,0:T(8,128)(2,1)S(1)}, u32[]{:S(2)}, u32[]{:S(2)}) collective-permute-start(bf16[128,512]{1,0:T(8,128)(2,1)S(1)} %get-tuple-element.20.refs_2_), channel_id=1, source_target_pairs={{0,4},{4,0},{8,12},{12,8},{16,20},{20,16},{24,28},{28,24},{1,5},{5... | collective-permute-start | bytes 393224 | tf_op jit(solution)/shard_map/ppermute | solution.py:32
  31.3 1.5 %collective-permute-start.16 = (bf16[256,2048]{1,0:T(8,128)(2,1)}, bf16[256,2048]{1,0:T(8,128)(2,1)S(1)}, u32[]{:S(2)}, u32[]{:S(2)}) collective-permute-start(bf16[256,2048]{1,0:T(8,128)(2,1)} %refs_0_.1), channel_id=1, source_target_pairs={{0,2},{1,3},{2,0},{3,1},{4,6},{5,7},{6,4},{7,5},{8,10},{9,11},{10,... | collective-permute-start | bytes 3145736 | tf_op jit(solution)/shard_map/ppermute | solution.py:32
  32.8 1.0 %shard_map.148.refs_3_.refs_4_ = f32[4,14,64,128]{3,2,1,0:T(8,128)S(1)} custom-call(f32[4,15,128]{2,1,0:T(8,128)S(1)} %pad.4.bias_ref), custom_call_target="tpu_custom_call" | custom-call | tf_op jit(solution)/shard_map/pallas_call | solution.py:37
  33.8 1.6 %collective-permute-start.9 = (bf16[128,512]{1,0:T(8,128)(2,1)S(1)}, bf16[128,512]{1,0:T(8,128)(2,1)S(1)}, u32[]{:S(2)}, u32[]{:S(2)}) collective-permute-start(bf16[128,512]{1,0:T(8,128)(2,1)S(1)} %get-tuple-element.20.refs_2_), channel_id=1, source_target_pairs={{0,8},{4,12},{8,0},{12,4},{16,24},{20,28},{24,16},{28,20},{1,9},{5... | collective-permute-start | bytes 393224 | tf_op jit(solution)/shard_map/ppermute | solution.py:32
  35.5 0.7 shard_map.147.q_ref
  36.2 0.7 collective-permute-start.7
  36.9 3.4 %collective-permute-start.10 = (bf16[128,512]{1,0:T(8,128)(2,1)S(1)}, bf16[128,512]{1,0:T(8,128)(2,1)S(1)}, u32[]{:S(2)}, u32[]{:S(2)}) collective-permute-start(bf16[128,512]{1,0:T(8,128)(2,1)S(1)} %collective-permute-done.8.refs_1_), channel_id=1, source_target_pairs={{0,8},{4,12},{8,0},{12,4},{16,24},{20,28},{24,16},{28,20},{1,9},{5... | collective-permute-start | bytes 393224 | tf_op jit(solution)/shard_map/ppermute | solution.py:32
  40.3 1.6 %shard_map.149.refs_1_ = bf16[256,512]{1,0:T(8,128)(2,1)S(1)} custom-call(bf16[256,1024]{1,0:T(8,128)(2,1)S(1)} %collective-permute-done.11.mine_ref, bf16[256,1024]{1,0:T(8,128)(2,1)S(1)} %collective-permute-done.12.passed_ref, f32[8,2048]{1,0:T(8,128)S(1)} %get-tuple-element.17.vec_ref.gate_ref, f32[1,2048]{1,0:T(1,128)S(1)} %bitcast.6, ...), custom_call_target="tpu_custom_call" | custom-call | tf_op jit(solution)/shard_map/pallas_call | solution.py:37
  41.9 1.2 %shard_map.150 = (f32[256,256]{1,0:T(8,128)S(1)}, f32[256,256]{1,0:T(8,128)S(1)}, f32[256,256]{1,0:T(8,128)S(1)}) custom-call(bf16[256,256]{1,0:T(8,128)(2,1)S(1)} %shard_map.147.q_ref, bf16[256,512]{1,0:T(8,128)(2,1)S(1)} %get-tuple-element.19.refs_0_, bf16[256,512]{1,0:T(8,128)(2,1)S(1)} %shard_map.149.refs_1_, ...), custom_call_target="tpu_custom_call" | custom-call | flops 137438953472 | bytes 1048576 | tf_op jit(solution)/shard_map/pallas_call | solution.py:37
  43.1 13.9 %collective-permute-done.16.refs_0_ = bf16[256,2048]{1,0:T(8,128)(2,1)S(1)} collective-permute-done((bf16[256,2048]{1,0:T(8,128)(2,1)}, bf16[256,2048]{1,0:T(8,128)(2,1)S(1)}, u32[]{:S(2)}, u32[]{:S(2)}) %collective-permute-start.16) | collective-permute-done | bytes 1048608 | tf_op jit(solution)/shard_map/ppermute | solution.py:32
  57.1 1.5 %shard_map.151.refs_0_ = bf16[256,256]{1,0:T(8,128)(2,1)S(1)} custom-call(bf16[256,256]{1,0:T(8,128)(2,1)S(1)} %shard_map.147.q_ref, bf16[256,512]{1,0:T(8,128)(2,1)S(1)} %collective-permute-done.7.refs_0_, bf16[128,512]{1,0:T(8,128)(2,1)S(1)} %collective-permute-done.8.refs_1_, bf16[128,512]{1,0:T(8,128)(2,1)S(1)} %collective-permute-done.9.refs_2_, ...), custom_call_target="tpu_custom_call" | custom-call | flops 137438953472 | bytes 1048576 | tf_op jit(solution)/shard_map/pallas_call | solution.py:37
  58.7 1.6 %collective-permute-start.15 = (bf16[256,256]{1,0:T(8,128)(2,1)S(1)}, bf16[256,256]{1,0:T(8,128)(2,1)S(1)}, u32[]{:S(2)}, u32[]{:S(2)}) collective-permute-start(bf16[256,256]{1,0:T(8,128)(2,1)S(1)} %shard_map.151.refs_0_), channel_id=1, source_target_pairs={{0,2},{1,3},{2,0},{3,1},{4,6},{5,7},{6,4},{7,5},{8,10},{9,11},{10,... | collective-permute-start | bytes 393224 | tf_op jit(solution)/shard_map/ppermute | solution.py:32
  60.4 4.2 %collective-permute-done.15.refs_1_ = bf16[256,256]{1,0:T(8,128)(2,1)S(1)} collective-permute-done((bf16[256,256]{1,0:T(8,128)(2,1)S(1)}, bf16[256,256]{1,0:T(8,128)(2,1)S(1)}, u32[]{:S(2)}, u32[]{:S(2)}) %collective-permute-start.15) | collective-permute-done | bytes 131104 | tf_op jit(solution)/shard_map/ppermute | solution.py:32
  64.6 1.2 %shard_map.152.refs_2_ = bf16[256,2048]{1,0:T(8,128)(2,1)S(1)} custom-call(bf16[256,2048]{1,0:T(8,128)(2,1)} %refs_0_.1), custom_call_target="tpu_custom_call" | custom-call | tf_op jit(solution)/shard_map/pallas_call | solution.py:37
  65.9 1.2 %shard_map.154.refs_2_ = bf16[256,2048]{1,0:T(8,128)(2,1)S(1)} custom-call(bf16[256,2048]{1,0:T(8,128)(2,1)} %copy-done.11), custom_call_target="tpu_custom_call" | custom-call | tf_op jit(solution)/shard_map/pallas_call | solution.py:37
  67.1 1.9 %shard_map.153.refs_0_ = f32[256,2048]{1,0:T(8,128)S(1)} custom-call(bf16[256,256]{1,0:T(8,128)(2,1)S(1)} %shard_map.151.refs_0_, bf16[256,256]{1,0:T(8,128)(2,1)S(1)} %collective-permute-done.13.refs_1_, bf16[256,2048]{1,0:T(8,128)(2,1)S(1)} %shard_map.152.refs_2_, bf16[256,2048]{1,0:T(8,128)(2,1)} %collective-permute-done.14.refs_3_), custom_call_target="tpu_custom_call" | custom-call | tf_op jit(solution)/shard_map/pallas_call | solution.py:37
  69.6 0.7 %copy-done.4 = bf16[256,2048]{1,0:T(8,128)(2,1)S(1)} copy-done((bf16[256,2048]{1,0:T(8,128)(2,1)S(1)}, bf16[256,2048]{1,0:T(8,128)(2,1)}, u32[]{:S(2)}) %copy-start.4) | copy-done | bytes 1048600
  70.3 1.9 %shard_map.156 = bf16[256,2048]{1,0:T(8,128)(2,1)} custom-call(bf16[256,2048]{1,0:T(8,128)(2,1)S(1)} %copy-done.4, f32[8,2048]{1,0:T(8,128)S(1)} %copy-done.6, f32[256,2048]{1,0:T(8,128)S(1)} %shard_map.155.sum_ref, bf16[256,256]{1,0:T(8,128)(2,1)S(1)} %collective-permute-done.17.refs_0_, bf16[256,2048]{1,0:T(8,128)(2,1)S(1)} %collective-permute-done.18.refs_1_), custom_call_target="tpu_custom_call" | custom-call | tf_op jit(solution)/shard_map/pallas_call | solution.py:37
  (51 shorter events, 0.8 us)
Async XLA Ops:
  0.0 27.3 %copy-start.1 = (bf16[2048,256]{1,0:T(8,128)(2,1)S(1)}, bf16[2048,256]{1,0:T(8,128)(2,1)}, u32[]{:S(2)}) copy-start(bf16[2048,256]{1,0:T(8,128)(2,1)} %wk.1) | copy-start | bytes 3145732
  0.0 27.3 %copy-start.2 = (bf16[2048,256]{1,0:T(8,128)(2,1)S(1)}, bf16[2048,256]{1,0:T(8,128)(2,1)}, u32[]{:S(2)}) copy-start(bf16[2048,256]{1,0:T(8,128)(2,1)} %wv.1) | copy-start | bytes 3145732
  0.0 27.4 %copy-start.3 = (bf16[256,2048]{1,0:T(8,128)(2,1)S(1)}, bf16[256,2048]{1,0:T(8,128)(2,1)}, u32[]{:S(2)}) copy-start(bf16[256,2048]{1,0:T(8,128)(2,1)} %lat_ref.5) | copy-start | bytes 3145732
  0.0 27.4 %copy-start.7 = (f32[2048]{0:T(1024)S(1)}, f32[2048]{0:T(1024)}, u32[]{:S(2)}) copy-start(f32[2048]{0:T(1024)} %param.22) | copy-start | bytes 24580
  0.0 27.4 %copy-start.9 = (f32[64]{0:T(128)S(1)}, f32[64]{0:T(128)}, u32[]{:S(2)}) copy-start(f32[64]{0:T(128)} %param.27) | copy-start | bytes 772
  0.0 27.4 %copy-start.10 = (bf16[64,2048]{1,0:T(8,128)(2,1)S(1)}, bf16[64,2048]{1,0:T(8,128)(2,1)}, u32[]{:S(2)}) copy-start(bf16[64,2048]{1,0:T(8,128)(2,1)} %ctx_ref.3) | copy-start | bytes 786436
  1.7 24.5 %collective-permute-start.11 = (bf16[256,1024]{1,0:T(8,128)(2,1)S(1)}, bf16[256,1024]{1,0:T(8,128)(2,1)S(1)}, u32[]{:S(2)}, u32[]{:S(2)}) collective-permute-start(bf16[256,1024]{1,0:T(8,128)(2,1)S(1)} %get-tuple-element.21), channel_id=1, source_target_pairs={{0,4},{4,0},{8,12},{12,8},{16,20},{20,16},{24,28},{28,24},{1,5},{5... | collective-permute-start | bytes 1572872 | tf_op jit(solution)/shard_map/ppermute | solution.py:32
  4.8 4.1 %collective-permute-start.2 = (f32[8,512]{1,0:T(8,128)S(1)}, f32[8,512]{1,0:T(8,128)S(1)}, u32[]{:S(2)}, u32[]{:S(2)}) collective-permute-start(f32[8,512]{1,0:T(8,128)S(1)} %get-tuple-element.16), channel_id=1, source_target_pairs={{0,2},{1,3},{2,0},{3,1},{4,6},{5,7},{6,4},{7,5},{8,10},{9,11},{10,... | collective-permute-start | bytes 49160 | tf_op jit(solution)/shard_map/ppermute | solution.py:32
  6.2 8.4 %collective-permute-start = (bf16[64,1024]{1,0:T(8,128)(2,1)S(1)}, bf16[64,1024]{1,0:T(8,128)(2,1)S(1)}, u32[]{:S(2)}, u32[]{:S(2)}) collective-permute-start(bf16[64,1024]{1,0:T(8,128)(2,1)S(1)} %get-tuple-element.15), channel_id=1, source_target_pairs={{0,16},{4,20},{8,24},{12,28},{16,0},{20,4},{24,8},{28,12},{1,17},{... | collective-permute-start | bytes 393224 | tf_op jit(solution)/shard_map/ppermute | solution.py:32
  8.8 8.5 %collective-permute-start.3 = (f32[16,512]{1,0:T(8,128)S(1)}, f32[16,512]{1,0:T(8,128)S(1)}, u32[]{:S(2)}, u32[]{:S(2)}) collective-permute-start(f32[16,512]{1,0:T(8,128)S(1)} %constant_dynamic-update-slice_fusion), channel_id=1, source_target_pairs={{0,4},{4,0},{8,12},{12,8},{16,20},{20,16},{24,28},{28,24},{1,5},{5... | collective-permute-start | bytes 98312 | tf_op jit(solution)/shard_map/ppermute | solution.py:32
  14.6 12.7 %collective-permute-start.1 = (bf16[64,1024]{1,0:T(8,128)(2,1)S(1)}, bf16[64,1024]{1,0:T(8,128)(2,1)S(1)}, u32[]{:S(2)}, u32[]{:S(2)}) collective-permute-start(bf16[64,1024]{1,0:T(8,128)(2,1)S(1)} %collective-permute-done.mine_ref), channel_id=1, source_target_pairs={{0,1},{1,0},{2,3},{3,2},{4,5},{5,4},{6,7},{7,6},{8,9},{9,8},{10,11... | collective-permute-start | bytes 393224 | tf_op jit(solution)/shard_map/ppermute | solution.py:32
  17.4 3.9 %collective-permute-start.4 = (f32[16,512]{1,0:T(8,128)S(1)}, f32[16,512]{1,0:T(8,128)S(1)}, u32[]{:S(2)}, u32[]{:S(2)}) collective-permute-start(f32[16,512]{1,0:T(8,128)S(1)} %add.11), channel_id=1, source_target_pairs={{0,8},{4,12},{8,0},{12,4},{16,24},{20,28},{24,16},{28,20},{1,9},{5... | collective-permute-start | bytes 98312 | tf_op jit(solution)/shard_map/ppermute | solution.py:32
  21.3 4.8 %collective-permute-start.5 = (f32[16,512]{1,0:T(8,128)S(1)}, f32[16,512]{1,0:T(8,128)S(1)}, u32[]{:S(2)}, u32[]{:S(2)}) collective-permute-start(f32[16,512]{1,0:T(8,128)S(1)} %add.12), channel_id=1, source_target_pairs={{0,16},{4,20},{8,24},{12,28},{16,0},{20,4},{24,8},{28,12},{1,17},{... | collective-permute-start | bytes 98312 | tf_op jit(solution)/shard_map/ppermute | solution.py:32
  26.1 1.2 %collective-permute-start.6 = (f32[16,512]{1,0:T(8,128)S(1)}, f32[16,512]{1,0:T(8,128)S(1)}, u32[]{:S(2)}, u32[]{:S(2)}) collective-permute-start(f32[16,512]{1,0:T(8,128)S(1)} %add.13.part_ref), channel_id=1, source_target_pairs={{0,1},{1,0},{2,3},{3,2},{4,5},{5,4},{6,7},{7,6},{8,9},{9,8},{10,11... | collective-permute-start | bytes 98312 | tf_op jit(solution)/shard_map/ppermute | solution.py:32
  26.2 10.7 %collective-permute-start.12 = (bf16[256,1024]{1,0:T(8,128)(2,1)S(1)}, bf16[256,1024]{1,0:T(8,128)(2,1)S(1)}, u32[]{:S(2)}, u32[]{:S(2)}) collective-permute-start(bf16[256,1024]{1,0:T(8,128)(2,1)S(1)} %collective-permute-done.11.mine_ref), channel_id=1, source_target_pairs={{0,1},{1,0},{2,3},{3,2},{4,5},{5,4},{6,7},{7,6},{8,9},{9,8},{10,11... | collective-permute-start | bytes 1572872 | tf_op jit(solution)/shard_map/ppermute | solution.py:32
  27.4 5.4 %copy-start.12 = (f32[4,15,31]{2,0,1:T(4,128)S(1)}, f32[4,15,31]{2,0,1:T(4,128)}, u32[]{:S(2)}) copy-start(f32[4,15,31]{2,0,1:T(4,128)} %param.28) | copy-start | bytes 22324
  27.4 8.1 %copy-start.8 = (f32[64]{0:T(128)S(1)}, f32[64]{0:T(128)}, u32[]{:S(2)}) copy-start(f32[64]{0:T(128)} %param.26) | copy-start | bytes 772
  29.5 10.8 %copy-start.5 = (f32[8,2048]{1,0:T(8,128)}, f32[8,2048]{1,0:T(8,128)S(1)}, u32[]{:S(2)}) copy-start(f32[8,2048]{1,0:T(8,128)S(1)} %get-tuple-element.17.vec_ref.gate_ref) | copy-start | bytes 196612
  29.5 6.0 %copy-start = (bf16[2048,256]{1,0:T(8,128)(2,1)S(1)}, bf16[2048,256]{1,0:T(8,128)(2,1)}, u32[]{:S(2)}) copy-start(bf16[2048,256]{1,0:T(8,128)(2,1)} %wq_ref.1) | copy-start | bytes 3145732
  29.5 6.7 %collective-permute-start.8 = (bf16[128,512]{1,0:T(8,128)(2,1)S(1)}, bf16[128,512]{1,0:T(8,128)(2,1)S(1)}, u32[]{:S(2)}, u32[]{:S(2)}) collective-permute-start(bf16[128,512]{1,0:T(8,128)(2,1)S(1)} %get-tuple-element.20.refs_2_), channel_id=1, source_target_pairs={{0,4},{4,0},{8,12},{12,8},{16,20},{20,16},{24,28},{28,24},{1,5},{5... | collective-permute-start | bytes 393224 | tf_op jit(solution)/shard_map/ppermute | solution.py:32
  31.3 35.8 %collective-permute-start.14 = (bf16[256,2048]{1,0:T(8,128)(2,1)}, bf16[256,2048]{1,0:T(8,128)(2,1)}, u32[]{:S(2)}, u32[]{:S(2)}) collective-permute-start(bf16[256,2048]{1,0:T(8,128)(2,1)} %refs_0_.1), channel_id=1, source_target_pairs={{0,1},{1,0},{2,3},{3,2},{4,5},{5,4},{6,7},{7,6},{8,9},{9,8},{10,11... | collective-permute-start | bytes 3145736 | tf_op jit(solution)/shard_map/ppermute | solution.py:32
  31.3 25.8 %collective-permute-start.16 = (bf16[256,2048]{1,0:T(8,128)(2,1)}, bf16[256,2048]{1,0:T(8,128)(2,1)S(1)}, u32[]{:S(2)}, u32[]{:S(2)}) collective-permute-start(bf16[256,2048]{1,0:T(8,128)(2,1)} %refs_0_.1), channel_id=1, source_target_pairs={{0,2},{1,3},{2,0},{3,1},{4,6},{5,7},{6,4},{7,5},{8,10},{9,11},{10,... | collective-permute-start | bytes 3145736 | tf_op jit(solution)/shard_map/ppermute | solution.py:32
  33.8 23.3 %collective-permute-start.9 = (bf16[128,512]{1,0:T(8,128)(2,1)S(1)}, bf16[128,512]{1,0:T(8,128)(2,1)S(1)}, u32[]{:S(2)}, u32[]{:S(2)}) collective-permute-start(bf16[128,512]{1,0:T(8,128)(2,1)S(1)} %get-tuple-element.20.refs_2_), channel_id=1, source_target_pairs={{0,8},{4,12},{8,0},{12,4},{16,24},{20,28},{24,16},{28,20},{1,9},{5... | collective-permute-start | bytes 393224 | tf_op jit(solution)/shard_map/ppermute | solution.py:32
  36.2 20.9 %collective-permute-start.7 = (bf16[256,512]{1,0:T(8,128)(2,1)S(1)}, bf16[256,512]{1,0:T(8,128)(2,1)S(1)}, u32[]{:S(2)}, u32[]{:S(2)}) collective-permute-start(bf16[256,512]{1,0:T(8,128)(2,1)S(1)} %get-tuple-element.19.refs_0_), channel_id=1, source_target_pairs={{4,8},{12,16},{20,24},{8,4},{16,12},{24,20},{5,9},{13,17},{21,25},... | collective-permute-start | bytes 786440 | tf_op jit(solution)/shard_map/ppermute | solution.py:478
  36.9 20.2 %collective-permute-start.10 = (bf16[128,512]{1,0:T(8,128)(2,1)S(1)}, bf16[128,512]{1,0:T(8,128)(2,1)S(1)}, u32[]{:S(2)}, u32[]{:S(2)}) collective-permute-start(bf16[128,512]{1,0:T(8,128)(2,1)S(1)} %collective-permute-done.8.refs_1_), channel_id=1, source_target_pairs={{0,8},{4,12},{8,0},{12,4},{16,24},{20,28},{24,16},{28,20},{1,9},{5... | collective-permute-start | bytes 393224 | tf_op jit(solution)/shard_map/ppermute | solution.py:32
  57.1 1.6 %copy-start.11 = (bf16[256,2048]{1,0:T(8,128)(2,1)}, bf16[256,2048]{1,0:T(8,128)(2,1)S(1)}, u32[]{:S(2)}) copy-start(bf16[256,2048]{1,0:T(8,128)(2,1)S(1)} %collective-permute-done.16.refs_0_) | copy-start | bytes 3145732
  57.1 12.5 %collective-permute-start.18 = (bf16[256,2048]{1,0:T(8,128)(2,1)S(1)}, bf16[256,2048]{1,0:T(8,128)(2,1)S(1)}, u32[]{:S(2)}, u32[]{:S(2)}) collective-permute-start(bf16[256,2048]{1,0:T(8,128)(2,1)S(1)} %collective-permute-done.16.refs_0_), channel_id=1, source_target_pairs={{0,1},{1,0},{2,3},{3,2},{4,5},{5,4},{6,7},{7,6},{8,9},{9,8},{10,11... | collective-permute-start | bytes 3145736 | tf_op jit(solution)/shard_map/ppermute | solution.py:32
  58.7 6.0 %collective-permute-start.15 = (bf16[256,256]{1,0:T(8,128)(2,1)S(1)}, bf16[256,256]{1,0:T(8,128)(2,1)S(1)}, u32[]{:S(2)}, u32[]{:S(2)}) collective-permute-start(bf16[256,256]{1,0:T(8,128)(2,1)S(1)} %shard_map.151.refs_0_), channel_id=1, source_target_pairs={{0,2},{1,3},{2,0},{3,1},{4,6},{5,7},{6,4},{7,5},{8,10},{9,11},{10,... | collective-permute-start | bytes 393224 | tf_op jit(solution)/shard_map/ppermute | solution.py:32
  60.2 6.9 %collective-permute-start.13 = (bf16[256,256]{1,0:T(8,128)(2,1)S(1)}, bf16[256,256]{1,0:T(8,128)(2,1)S(1)}, u32[]{:S(2)}, u32[]{:S(2)}) collective-permute-start(bf16[256,256]{1,0:T(8,128)(2,1)S(1)} %shard_map.151.refs_0_), channel_id=1, source_target_pairs={{0,1},{1,0},{2,3},{3,2},{4,5},{5,4},{6,7},{7,6},{8,9},{9,8},{10,11... | collective-permute-start | bytes 393224 | tf_op jit(solution)/shard_map/ppermute | solution.py:32
  64.6 4.9 %collective-permute-start.17 = (bf16[256,256]{1,0:T(8,128)(2,1)S(1)}, bf16[256,256]{1,0:T(8,128)(2,1)S(1)}, u32[]{:S(2)}, u32[]{:S(2)}) collective-permute-start(bf16[256,256]{1,0:T(8,128)(2,1)S(1)} %collective-permute-done.15.refs_1_), channel_id=1, source_target_pairs={{0,1},{1,0},{2,3},{3,2},{4,5},{5,4},{6,7},{7,6},{8,9},{9,8},{10,11... | collective-permute-start | bytes 393224 | tf_op jit(solution)/shard_map/ppermute | solution.py:32
  69.1 1.2 %copy-start.4 = (bf16[256,2048]{1,0:T(8,128)(2,1)S(1)}, bf16[256,2048]{1,0:T(8,128)(2,1)}, u32[]{:S(2)}) copy-start(bf16[256,2048]{1,0:T(8,128)(2,1)} %lat_ref.5) | copy-start | bytes 3145732
  69.1 1.2 %copy-start.6 = (f32[8,2048]{1,0:T(8,128)S(1)}, f32[8,2048]{1,0:T(8,128)}, u32[]{:S(2)}) copy-start(f32[8,2048]{1,0:T(8,128)} %copy-done.5) | copy-start | bytes 196612

commit v4 on v3

--- a/solution.py
+++ b/solution.py
@@ -184,7 +184,14 @@
         out[:, cols:] = jnp.dot(src, wv[...], preferred_element_type=F32).astype(BF16)
 
 
-def near_body(mine_ref, passed_ref, vec_ref, gain_ref, kg_ref, wk, wv, kv_ref, lat_ref, hid_ref):
+def near_body(
+    mine_ref, passed_ref, vec_ref, gain_ref, kg_ref, wk, wv, own_hid_ref, wq, qg_ref,
+    kv_ref, q_ref, lat_ref, hid_ref,
+):
+    queries = head_norm(
+        jnp.dot(own_hid_ref[...], wq[...], preferred_element_type=F32), qg_ref
+    ).astype(BF16)
+    q_ref[...] = (queries.astype(F32) * HEAD_DIM ** (-0.5)).astype(BF16)
     join_halves(mine_ref, passed_ref, lat_ref)
     for here in row_steps(lat_ref.shape[0]):
         hid_ref[here, :] = modulated(lat_ref[here, :].astype(F32), vec_ref, gain_ref, 0)
@@ -198,13 +205,6 @@
         kv_ref[at : at + step, cols:] = jnp.dot(
             hidden, wv[...], preferred_element_type=F32
         ).astype(BF16)
-
-
-def query_body(hid_ref, wq_ref, qg_ref, q_ref):
-    queries = head_norm(
-        jnp.dot(hid_ref[...], wq_ref[...], preferred_element_type=F32), qg_ref
-    ).astype(BF16)
-    q_ref[...] = (queries.astype(F32) * HEAD_DIM ** (-0.5)).astype(BF16)
 
 
 OWN, NEAR, OTHER = range(3)
@@ -456,22 +456,28 @@
         key_weight,
         value_weight,
     )
-    near_kv = call(
+    near_kv, queries = call(
         near_body,
-        out_shape=jax.ShapeDtypeStruct((tokens, 2 * cols), BF16),
-        in_specs=vmem(7),
-        out_specs=vmem(1)[0],
+        out_shape=(
+            jax.ShapeDtypeStruct((tokens, 2 * cols), BF16),
+            jax.ShapeDtypeStruct((tokens, cols), BF16),
+        ),
+        in_specs=vmem(10),
+        out_specs=tuple(vmem(2)),
         scratch_shapes=[pltpu.VMEM((tokens, width), BF16)] * 2,
         compiler_params=params(20),
-    )(near_mine, near_passed, vec, gain, key_gain[None], key_weight, value_weight)
-    queries = call(
-        query_body,
-        out_shape=jax.ShapeDtypeStruct((tokens, cols), BF16),
-        in_specs=vmem(3),
-        out_specs=vmem(1)[0],
-        compiler_params=params(8),
-    )(hidden, query_weight, query_gain[None])
-
+    )(
+        near_mine,
+        near_passed,
+        vec,
+        gain,
+        key_gain[None],
+        key_weight,
+        value_weight,
+        hidden,
+        query_weight,
+        query_gain[None],
+    )
     sp_count = lax.axis_size("sp")
     other_pairs = [(i, i + 1) for i in range(1, sp_count - 1, 2)]
     other_pairs += [(j, i) for i, j in other_pairs]

time: 72.4 us -> 72.4 us (level)
  starting transfers between devices: 23.6 us -> 24.4 us
    ppermute x18, starting transfers between devices: 22.9 us -> 23.7 us  [swap(): lax.ppermute(x, axis, [(i, i ^ code) for i in range(lax.axis_size(axis))])]
    pallas_call x12 -> x11, Pallas kernels: 16.5 us -> 15.9 us  [run(): return pl.pallas_call(*args, **kwargs)(*operands)]
  transfers between devices with their start and end apart: 19 -> 19, of which waited for: 7 -> 7; matrix products, arithmetic and copies ran while one was open for 0% -> 0% of each run, Pallas kernels for 18% -> 17%
where the time goes in v4:
time: 72.4 us; the launch traced here: 72.1 us
  waiting for transfers between devices  30.7 us (42%)
  starting transfers between devices  24.4 us (34%)
  Pallas kernels  15.9 us (22%)
  local copies, waits for them, and re-layouts  0.81 us (1%)
    ppermute x18, waiting for transfers between devices, swap(): lax.ppermute(x, axis, [(i, i ^ code) for i in range(lax.axis_size(axis))])  30.7 us
    ppermute x18, starting transfers between devices, swap(): lax.ppermute(x, axis, [(i, i ^ code) for i in range(lax.axis_size(axis))])  23.7 us
    pallas_call x11, Pallas kernels, run(): return pl.pallas_call(*args, **kwargs)(*operands)  15.9 us
  transfers between devices with their start and end apart: 19, of which 7 were waited for; matrix products, arithmetic and copies ran while one was open for 0% of the time, Pallas kernels for 17%

profile of v4, /device:TPU:0, one launch (start us, length us, event | category | flops | bytes accessed | tf_op | source)
XLA Modules:
  0.0 72.1 jit_solution(810266985369105730)
XLA Ops:
  0.0 1.6 %shard_map.145 = (f32[8,512]{1,0:T(8,128)S(1)}, bf16[64,1024]{1,0:T(8,128)(2,1)S(1)}, bf16[256,1024]{1,0:T(8,128)(2,1)S(1)}) custom-call(f32[1,256]{1,0:T(1,128)} %bitcast.10, f32[1,256]{1,0:T(1,128)} %bitcast.11, bf16[256,512]{1,0:T(8,128)(2,1)} %shift_ref.1, bf16[256,512]{1,0:T(8,128)(2,1)} %scale_ref.1, bf16[256,512]{1,0:T(8,128)(2,1)} %gate_ref.1, ...), custom_call_target="tpu_custom_call" | custom-call | flops 137438953472 | bytes 1048576 | tf_op jit(solution)/shard_map/pallas_call | solution.py:37
  1.7 3.1 %collective-permute-start.7 = (bf16[256,1024]{1,0:T(8,128)(2,1)S(1)}, bf16[256,1024]{1,0:T(8,128)(2,1)S(1)}, u32[]{:S(2)}, u32[]{:S(2)}) collective-permute-start(bf16[256,1024]{1,0:T(8,128)(2,1)S(1)} %get-tuple-element.20), channel_id=1, source_target_pairs={{0,4},{4,0},{8,12},{12,8},{16,20},{20,16},{24,28},{28,24},{1,5},{5... | collective-permute-start | bytes 1572872 | tf_op jit(solution)/shard_map/ppermute | solution.py:32
  4.8 1.5 %collective-permute-start.2 = (f32[8,512]{1,0:T(8,128)S(1)}, f32[8,512]{1,0:T(8,128)S(1)}, u32[]{:S(2)}, u32[]{:S(2)}) collective-permute-start(f32[8,512]{1,0:T(8,128)S(1)} %get-tuple-element.18), channel_id=1, source_target_pairs={{0,2},{1,3},{2,0},{3,1},{4,6},{5,7},{6,4},{7,5},{8,10},{9,11},{10,... | collective-permute-start | bytes 49160 | tf_op jit(solution)/shard_map/ppermute | solution.py:32
  6.2 2.6 %collective-permute-start = (bf16[64,1024]{1,0:T(8,128)(2,1)S(1)}, bf16[64,1024]{1,0:T(8,128)(2,1)S(1)}, u32[]{:S(2)}, u32[]{:S(2)}) collective-permute-start(bf16[64,1024]{1,0:T(8,128)(2,1)S(1)} %get-tuple-element.17), channel_id=1, source_target_pairs={{0,16},{4,20},{8,24},{12,28},{16,0},{20,4},{24,8},{28,12},{1,17},{... | collective-permute-start | bytes 393224 | tf_op jit(solution)/shard_map/ppermute | solution.py:32
  8.8 0.6 collective-permute-start.3
  9.4 5.2 %collective-permute-done.mine_ref = bf16[64,1024]{1,0:T(8,128)(2,1)S(1)} collective-permute-done((bf16[64,1024]{1,0:T(8,128)(2,1)S(1)}, bf16[64,1024]{1,0:T(8,128)(2,1)S(1)}, u32[]{:S(2)}, u32[]{:S(2)}) %collective-permute-start) | collective-permute-done | bytes 131104 | tf_op jit(solution)/shard_map/ppermute | solution.py:32
  14.6 2.7 %collective-permute-done.3 = f32[16,512]{1,0:T(8,128)S(1)} collective-permute-done((f32[16,512]{1,0:T(8,128)S(1)}, f32[16,512]{1,0:T(8,128)S(1)}, u32[]{:S(2)}, u32[]{:S(2)}) %collective-permute-start.3) | collective-permute-done | bytes 32800 | tf_op jit(solution)/shard_map/ppermute | solution.py:32
  17.4 1.8 %collective-permute-start.4 = (f32[16,512]{1,0:T(8,128)S(1)}, f32[16,512]{1,0:T(8,128)S(1)}, u32[]{:S(2)}, u32[]{:S(2)}) collective-permute-start(f32[16,512]{1,0:T(8,128)S(1)} %add.11), channel_id=1, source_target_pairs={{0,8},{4,12},{8,0},{12,4},{16,24},{20,28},{24,16},{28,20},{1,9},{5... | collective-permute-start | bytes 98312 | tf_op jit(solution)/shard_map/ppermute | solution.py:32
  19.2 2.1 %collective-permute-done.4 = f32[16,512]{1,0:T(8,128)S(1)} collective-permute-done((f32[16,512]{1,0:T(8,128)S(1)}, f32[16,512]{1,0:T(8,128)S(1)}, u32[]{:S(2)}, u32[]{:S(2)}) %collective-permute-start.4) | collective-permute-done | bytes 32800 | tf_op jit(solution)/shard_map/ppermute | solution.py:32
  21.3 2.8 %collective-permute-start.5 = (f32[16,512]{1,0:T(8,128)S(1)}, f32[16,512]{1,0:T(8,128)S(1)}, u32[]{:S(2)}, u32[]{:S(2)}) collective-permute-start(f32[16,512]{1,0:T(8,128)S(1)} %add.12), channel_id=1, source_target_pairs={{0,16},{4,20},{8,24},{12,28},{16,0},{20,4},{24,8},{28,12},{1,17},{... | collective-permute-start | bytes 98312 | tf_op jit(solution)/shard_map/ppermute | solution.py:32
  24.1 2.0 %collective-permute-done.5 = f32[16,512]{1,0:T(8,128)S(1)} collective-permute-done((f32[16,512]{1,0:T(8,128)S(1)}, f32[16,512]{1,0:T(8,128)S(1)}, u32[]{:S(2)}, u32[]{:S(2)}) %collective-permute-start.5) | collective-permute-done | bytes 32800 | tf_op jit(solution)/shard_map/ppermute | solution.py:32
  26.2 0.5 collective-permute-start.8
  26.6 0.7 collective-permute-done.6.beside_ref
  27.4 2.0 %shard_map.146 = (bf16[256,512]{1,0:T(8,128)(2,1)S(1)}, bf16[128,512]{1,0:T(8,128)(2,1)S(1)}, bf16[256,2048]{1,0:T(8,128)(2,1)S(1)}, f32[8,2048]{1,0:T(8,128)S(1)}) custom-call(bf16[256,2048]{1,0:T(8,128)(2,1)S(1)} %copy-done.3, bf16[64,2048]{1,0:T(8,128)(2,1)S(1)} %copy-done.10, bf16[64,1024]{1,0:T(8,128)(2,1)S(1)} %collective-permute-done.mine_ref, ...), custom_call_target="tpu_custom_call" | custom-call | flops 137438953472 | bytes 1048576 | tf_op jit(solution)/shard_map/pallas_call | solution.py:37
  29.4 1.8 %collective-permute-start.10 = (bf16[128,512]{1,0:T(8,128)(2,1)S(1)}, bf16[128,512]{1,0:T(8,128)(2,1)S(1)}, u32[]{:S(2)}, u32[]{:S(2)}) collective-permute-start(bf16[128,512]{1,0:T(8,128)(2,1)S(1)} %get-tuple-element.24.refs_2_), channel_id=1, source_target_pairs={{0,4},{4,0},{8,12},{12,8},{16,20},{20,16},{24,28},{28,24},{1,5},{5... | collective-permute-start | bytes 393224 | tf_op jit(solution)/shard_map/ppermute | solution.py:32
  31.2 1.5 %collective-permute-start.16 = (bf16[256,2048]{1,0:T(8,128)(2,1)}, bf16[256,2048]{1,0:T(8,128)(2,1)S(1)}, u32[]{:S(2)}, u32[]{:S(2)}) collective-permute-start(bf16[256,2048]{1,0:T(8,128)(2,1)} %refs_0_.1), channel_id=1, source_target_pairs={{0,2},{1,3},{2,0},{3,1},{4,6},{5,7},{6,4},{7,5},{8,10},{9,11},{10,... | collective-permute-start | bytes 3145736 | tf_op jit(solution)/shard_map/ppermute | solution.py:32
  32.7 1.0 %shard_map.148.refs_3_.refs_4_ = f32[4,14,64,128]{3,2,1,0:T(8,128)S(1)} custom-call(f32[4,15,128]{2,1,0:T(8,128)S(1)} %pad.4.bias_ref), custom_call_target="tpu_custom_call" | custom-call | tf_op jit(solution)/shard_map/pallas_call | solution.py:37
  33.7 1.6 %collective-permute-start.11 = (bf16[128,512]{1,0:T(8,128)(2,1)S(1)}, bf16[128,512]{1,0:T(8,128)(2,1)S(1)}, u32[]{:S(2)}, u32[]{:S(2)}) collective-permute-start(bf16[128,512]{1,0:T(8,128)(2,1)S(1)} %get-tuple-element.24.refs_2_), channel_id=1, source_target_pairs={{0,8},{4,12},{8,0},{12,4},{16,24},{20,28},{24,16},{28,20},{1,9},{5... | collective-permute-start | bytes 393224 | tf_op jit(solution)/shard_map/ppermute | solution.py:32
  35.4 0.7 collective-permute-start.9
  36.1 4.1 %collective-permute-start.12 = (bf16[128,512]{1,0:T(8,128)(2,1)S(1)}, bf16[128,512]{1,0:T(8,128)(2,1)S(1)}, u32[]{:S(2)}, u32[]{:S(2)}) collective-permute-start(bf16[128,512]{1,0:T(8,128)(2,1)S(1)} %collective-permute-done.10.refs_1_), channel_id=1, source_target_pairs={{0,8},{4,12},{8,0},{12,4},{16,24},{20,28},{24,16},{28,20},{1,9},{5... | collective-permute-start | bytes 393224 | tf_op jit(solution)/shard_map/ppermute | solution.py:32
  40.2 1.8 %shard_map.147 = (bf16[256,512]{1,0:T(8,128)(2,1)S(1)}, bf16[256,256]{1,0:T(8,128)(2,1)S(1)}) custom-call(bf16[256,1024]{1,0:T(8,128)(2,1)S(1)} %collective-permute-done.7.mine_ref, bf16[256,1024]{1,0:T(8,128)(2,1)S(1)} %collective-permute-done.8.passed_ref, f32[8,2048]{1,0:T(8,128)S(1)} %get-tuple-element.19.vec_ref.gate_ref, f32[1,2048]{1,0:T(1,128)S(1)} %bitcast.6, ...), custom_call_target="tpu_custom_call" | custom-call | tf_op jit(solution)/shard_map/pallas_call | solution.py:37
  42.1 1.2 %shard_map.149 = (f32[256,256]{1,0:T(8,128)S(1)}, f32[256,256]{1,0:T(8,128)S(1)}, f32[256,256]{1,0:T(8,128)S(1)}) custom-call(bf16[256,256]{1,0:T(8,128)(2,1)S(1)} %get-tuple-element.22.q_ref, bf16[256,512]{1,0:T(8,128)(2,1)S(1)} %get-tuple-element.23.refs_0_, bf16[256,512]{1,0:T(8,128)(2,1)S(1)} %get-tuple-element.25.refs_1_, ...), custom_call_target="tpu_custom_call" | custom-call | flops 137438953472 | bytes 1048576 | tf_op jit(solution)/shard_map/pallas_call | solution.py:37
  43.3 13.7 %collective-permute-done.16.refs_0_ = bf16[256,2048]{1,0:T(8,128)(2,1)S(1)} collective-permute-done((bf16[256,2048]{1,0:T(8,128)(2,1)}, bf16[256,2048]{1,0:T(8,128)(2,1)S(1)}, u32[]{:S(2)}, u32[]{:S(2)}) %collective-permute-start.16) | collective-permute-done | bytes 1048608 | tf_op jit(solution)/shard_map/ppermute | solution.py:32
  57.0 1.5 %shard_map.150.refs_0_ = bf16[256,256]{1,0:T(8,128)(2,1)S(1)} custom-call(bf16[256,256]{1,0:T(8,128)(2,1)S(1)} %get-tuple-element.22.q_ref, bf16[256,512]{1,0:T(8,128)(2,1)S(1)} %collective-permute-done.9.refs_0_, bf16[128,512]{1,0:T(8,128)(2,1)S(1)} %collective-permute-done.10.refs_1_, bf16[128,512]{1,0:T(8,128)(2,1)S(1)} %collective-permute-done.11.refs_2_, ...), custom_call_target="tpu_custom_call" | custom-call | flops 137438953472 | bytes 1048576 | tf_op jit(solution)/shard_map/pallas_call | solution.py:37
  58.6 1.6 %collective-permute-start.15 = (bf16[256,256]{1,0:T(8,128)(2,1)S(1)}, bf16[256,256]{1,0:T(8,128)(2,1)S(1)}, u32[]{:S(2)}, u32[]{:S(2)}) collective-permute-start(bf16[256,256]{1,0:T(8,128)(2,1)S(1)} %shard_map.150.refs_0_), channel_id=1, source_target_pairs={{0,2},{1,3},{2,0},{3,1},{4,6},{5,7},{6,4},{7,5},{8,10},{9,11},{10,... | collective-permute-start | bytes 393224 | tf_op jit(solution)/shard_map/ppermute | solution.py:32
  60.4 4.2 %collective-permute-done.15.refs_1_ = bf16[256,256]{1,0:T(8,128)(2,1)S(1)} collective-permute-done((bf16[256,256]{1,0:T(8,128)(2,1)S(1)}, bf16[256,256]{1,0:T(8,128)(2,1)S(1)}, u32[]{:S(2)}, u32[]{:S(2)}) %collective-permute-start.15) | collective-permute-done | bytes 131104 | tf_op jit(solution)/shard_map/ppermute | solution.py:32
  64.6 1.2 %shard_map.151.refs_2_ = bf16[256,2048]{1,0:T(8,128)(2,1)S(1)} custom-call(bf16[256,2048]{1,0:T(8,128)(2,1)} %refs_0_.1), custom_call_target="tpu_custom_call" | custom-call | tf_op jit(solution)/shard_map/pallas_call | solution.py:37
  65.8 1.2 %shard_map.153.refs_2_ = bf16[256,2048]{1,0:T(8,128)(2,1)S(1)} custom-call(bf16[256,2048]{1,0:T(8,128)(2,1)} %copy-done.11), custom_call_target="tpu_custom_call" | custom-call | tf_op jit(solution)/shard_map/pallas_call | solution.py:37
  67.1 1.9 %shard_map.152.refs_0_ = f32[256,2048]{1,0:T(8,128)S(1)} custom-call(bf16[256,256]{1,0:T(8,128)(2,1)S(1)} %shard_map.150.refs_0_, bf16[256,256]{1,0:T(8,128)(2,1)S(1)} %collective-permute-done.13.refs_1_, bf16[256,2048]{1,0:T(8,128)(2,1)S(1)} %shard_map.151.refs_2_, bf16[256,2048]{1,0:T(8,128)(2,1)} %collective-permute-done.14.refs_3_), custom_call_target="tpu_custom_call" | custom-call | tf_op jit(solution)/shard_map/pallas_call | solution.py:37
  69.0 0.4 shard_map.154.sum_ref
  69.5 0.7 %copy-done.4 = bf16[256,2048]{1,0:T(8,128)(2,1)S(1)} copy-done((bf16[256,2048]{1,0:T(8,128)(2,1)S(1)}, bf16[256,2048]{1,0:T(8,128)(2,1)}, u32[]{:S(2)}) %copy-start.4) | copy-done | bytes 1048600
  70.2 1.9 %shard_map.155 = bf16[256,2048]{1,0:T(8,128)(2,1)} custom-call(bf16[256,2048]{1,0:T(8,128)(2,1)S(1)} %copy-done.4, f32[8,2048]{1,0:T(8,128)S(1)} %copy-done.6, f32[256,2048]{1,0:T(8,128)S(1)} %shard_map.154.sum_ref, bf16[256,256]{1,0:T(8,128)(2,1)S(1)} %collective-permute-done.17.refs_0_, bf16[256,2048]{1,0:T(8,128)(2,1)S(1)} %collective-permute-done.18.refs_1_), custom_call_target="tpu_custom_call" | custom-call | tf_op jit(solution)/shard_map/pallas_call | solution.py:37
  (50 shorter events, 0.4 us)
Async XLA Ops:
  0.0 27.3 %copy-start = (bf16[2048,256]{1,0:T(8,128)(2,1)S(1)}, bf16[2048,256]{1,0:T(8,128)(2,1)}, u32[]{:S(2)}) copy-start(bf16[2048,256]{1,0:T(8,128)(2,1)} %wk.1) | copy-start | bytes 3145732
  0.0 27.3 %copy-start.1 = (bf16[2048,256]{1,0:T(8,128)(2,1)S(1)}, bf16[2048,256]{1,0:T(8,128)(2,1)}, u32[]{:S(2)}) copy-start(bf16[2048,256]{1,0:T(8,128)(2,1)} %wv.1) | copy-start | bytes 3145732
  0.0 27.4 %copy-start.3 = (bf16[256,2048]{1,0:T(8,128)(2,1)S(1)}, bf16[256,2048]{1,0:T(8,128)(2,1)}, u32[]{:S(2)}) copy-start(bf16[256,2048]{1,0:T(8,128)(2,1)} %lat_ref.5) | copy-start | bytes 3145732
  0.0 27.4 %copy-start.7 = (f32[2048]{0:T(1024)S(1)}, f32[2048]{0:T(1024)}, u32[]{:S(2)}) copy-start(f32[2048]{0:T(1024)} %param.22) | copy-start | bytes 24580
  0.0 27.4 %copy-start.8 = (f32[64]{0:T(128)S(1)}, f32[64]{0:T(128)}, u32[]{:S(2)}) copy-start(f32[64]{0:T(128)} %param.27) | copy-start | bytes 772
  0.0 27.4 %copy-start.10 = (bf16[64,2048]{1,0:T(8,128)(2,1)S(1)}, bf16[64,2048]{1,0:T(8,128)(2,1)}, u32[]{:S(2)}) copy-start(bf16[64,2048]{1,0:T(8,128)(2,1)} %ctx_ref.3) | copy-start | bytes 786436
  1.7 24.5 %collective-permute-start.7 = (bf16[256,1024]{1,0:T(8,128)(2,1)S(1)}, bf16[256,1024]{1,0:T(8,128)(2,1)S(1)}, u32[]{:S(2)}, u32[]{:S(2)}) collective-permute-start(bf16[256,1024]{1,0:T(8,128)(2,1)S(1)} %get-tuple-element.20), channel_id=1, source_target_pairs={{0,4},{4,0},{8,12},{12,8},{16,20},{20,16},{24,28},{28,24},{1,5},{5... | collective-permute-start | bytes 1572872 | tf_op jit(solution)/shard_map/ppermute | solution.py:32
  4.8 4.1 %collective-permute-start.2 = (f32[8,512]{1,0:T(8,128)S(1)}, f32[8,512]{1,0:T(8,128)S(1)}, u32[]{:S(2)}, u32[]{:S(2)}) collective-permute-start(f32[8,512]{1,0:T(8,128)S(1)} %get-tuple-element.18), channel_id=1, source_target_pairs={{0,2},{1,3},{2,0},{3,1},{4,6},{5,7},{6,4},{7,5},{8,10},{9,11},{10,... | collective-permute-start | bytes 49160 | tf_op jit(solution)/shard_map/ppermute | solution.py:32
  6.2 8.4 %collective-permute-start = (bf16[64,1024]{1,0:T(8,128)(2,1)S(1)}, bf16[64,1024]{1,0:T(8,128)(2,1)S(1)}, u32[]{:S(2)}, u32[]{:S(2)}) collective-permute-start(bf16[64,1024]{1,0:T(8,128)(2,1)S(1)} %get-tuple-element.17), channel_id=1, source_target_pairs={{0,16},{4,20},{8,24},{12,28},{16,0},{20,4},{24,8},{28,12},{1,17},{... | collective-permute-start | bytes 393224 | tf_op jit(solution)/shard_map/ppermute | solution.py:32
  8.8 8.5 %collective-permute-start.3 = (f32[16,512]{1,0:T(8,128)S(1)}, f32[16,512]{1,0:T(8,128)S(1)}, u32[]{:S(2)}, u32[]{:S(2)}) collective-permute-start(f32[16,512]{1,0:T(8,128)S(1)} %constant_dynamic-update-slice_fusion), channel_id=1, source_target_pairs={{0,4},{4,0},{8,12},{12,8},{16,20},{20,16},{24,28},{28,24},{1,5},{5... | collective-permute-start | bytes 98312 | tf_op jit(solution)/shard_map/ppermute | solution.py:32
  14.6 12.7 %collective-permute-start.1 = (bf16[64,1024]{1,0:T(8,128)(2,1)S(1)}, bf16[64,1024]{1,0:T(8,128)(2,1)S(1)}, u32[]{:S(2)}, u32[]{:S(2)}) collective-permute-start(bf16[64,1024]{1,0:T(8,128)(2,1)S(1)} %collective-permute-done.mine_ref), channel_id=1, source_target_pairs={{0,1},{1,0},{2,3},{3,2},{4,5},{5,4},{6,7},{7,6},{8,9},{9,8},{10,11... | collective-permute-start | bytes 393224 | tf_op jit(solution)/shard_map/ppermute | solution.py:32
  17.4 3.9 %collective-permute-start.4 = (f32[16,512]{1,0:T(8,128)S(1)}, f32[16,512]{1,0:T(8,128)S(1)}, u32[]{:S(2)}, u32[]{:S(2)}) collective-permute-start(f32[16,512]{1,0:T(8,128)S(1)} %add.11), channel_id=1, source_target_pairs={{0,8},{4,12},{8,0},{12,4},{16,24},{20,28},{24,16},{28,20},{1,9},{5... | collective-permute-start | bytes 98312 | tf_op jit(solution)/shard_map/ppermute | solution.py:32
  21.3 4.8 %collective-permute-start.5 = (f32[16,512]{1,0:T(8,128)S(1)}, f32[16,512]{1,0:T(8,128)S(1)}, u32[]{:S(2)}, u32[]{:S(2)}) collective-permute-start(f32[16,512]{1,0:T(8,128)S(1)} %add.12), channel_id=1, source_target_pairs={{0,16},{4,20},{8,24},{12,28},{16,0},{20,4},{24,8},{28,12},{1,17},{... | collective-permute-start | bytes 98312 | tf_op jit(solution)/shard_map/ppermute | solution.py:32
  26.1 1.2 %collective-permute-start.6 = (f32[16,512]{1,0:T(8,128)S(1)}, f32[16,512]{1,0:T(8,128)S(1)}, u32[]{:S(2)}, u32[]{:S(2)}) collective-permute-start(f32[16,512]{1,0:T(8,128)S(1)} %add.13.part_ref), channel_id=1, source_target_pairs={{0,1},{1,0},{2,3},{3,2},{4,5},{5,4},{6,7},{7,6},{8,9},{9,8},{10,11... | collective-permute-start | bytes 98312 | tf_op jit(solution)/shard_map/ppermute | solution.py:32
  26.2 9.9 %collective-permute-start.8 = (bf16[256,1024]{1,0:T(8,128)(2,1)S(1)}, bf16[256,1024]{1,0:T(8,128)(2,1)S(1)}, u32[]{:S(2)}, u32[]{:S(2)}) collective-permute-start(bf16[256,1024]{1,0:T(8,128)(2,1)S(1)} %collective-permute-done.7.mine_ref), channel_id=1, source_target_pairs={{0,1},{1,0},{2,3},{3,2},{4,5},{5,4},{6,7},{7,6},{8,9},{9,8},{10,11... | collective-permute-start | bytes 1572872 | tf_op jit(solution)/shard_map/ppermute | solution.py:32
  27.4 5.3 %copy-start.12 = (f32[4,15,31]{2,0,1:T(4,128)S(1)}, f32[4,15,31]{2,0,1:T(4,128)}, u32[]{:S(2)}) copy-start(f32[4,15,31]{2,0,1:T(4,128)} %param.28) | copy-start | bytes 22324
  27.4 12.8 %copy-start.9 = (f32[64]{0:T(128)S(1)}, f32[64]{0:T(128)}, u32[]{:S(2)}) copy-start(f32[64]{0:T(128)} %param.26) | copy-start | bytes 772
  29.4 12.7 %copy-start.5 = (f32[8,2048]{1,0:T(8,128)}, f32[8,2048]{1,0:T(8,128)S(1)}, u32[]{:S(2)}) copy-start(f32[8,2048]{1,0:T(8,128)S(1)} %get-tuple-element.19.vec_ref.gate_ref) | copy-start | bytes 196612
  29.4 10.8 %copy-start.2 = (bf16[2048,256]{1,0:T(8,128)(2,1)S(1)}, bf16[2048,256]{1,0:T(8,128)(2,1)}, u32[]{:S(2)}) copy-start(bf16[2048,256]{1,0:T(8,128)(2,1)} %wq.1) | copy-start | bytes 3145732
  29.4 6.0 %collective-permute-start.10 = (bf16[128,512]{1,0:T(8,128)(2,1)S(1)}, bf16[128,512]{1,0:T(8,128)(2,1)S(1)}, u32[]{:S(2)}, u32[]{:S(2)}) collective-permute-start(bf16[128,512]{1,0:T(8,128)(2,1)S(1)} %get-tuple-element.24.refs_2_), channel_id=1, source_target_pairs={{0,4},{4,0},{8,12},{12,8},{16,20},{20,16},{24,28},{28,24},{1,5},{5... | collective-permute-start | bytes 393224 | tf_op jit(solution)/shard_map/ppermute | solution.py:32
  31.2 35.8 %collective-permute-start.14 = (bf16[256,2048]{1,0:T(8,128)(2,1)}, bf16[256,2048]{1,0:T(8,128)(2,1)}, u32[]{:S(2)}, u32[]{:S(2)}) collective-permute-start(bf16[256,2048]{1,0:T(8,128)(2,1)} %refs_0_.1), channel_id=1, source_target_pairs={{0,1},{1,0},{2,3},{3,2},{4,5},{5,4},{6,7},{7,6},{8,9},{9,8},{10,11... | collective-permute-start | bytes 3145736 | tf_op jit(solution)/shard_map/ppermute | solution.py:32
  31.2 25.8 %collective-permute-start.16 = (bf16[256,2048]{1,0:T(8,128)(2,1)}, bf16[256,2048]{1,0:T(8,128)(2,1)S(1)}, u32[]{:S(2)}, u32[]{:S(2)}) collective-permute-start(bf16[256,2048]{1,0:T(8,128)(2,1)} %refs_0_.1), channel_id=1, source_target_pairs={{0,2},{1,3},{2,0},{3,1},{4,6},{5,7},{6,4},{7,5},{8,10},{9,11},{10,... | collective-permute-start | bytes 3145736 | tf_op jit(solution)/shard_map/ppermute | solution.py:32
  33.7 23.3 %collective-permute-start.11 = (bf16[128,512]{1,0:T(8,128)(2,1)S(1)}, bf16[128,512]{1,0:T(8,128)(2,1)S(1)}, u32[]{:S(2)}, u32[]{:S(2)}) collective-permute-start(bf16[128,512]{1,0:T(8,128)(2,1)S(1)} %get-tuple-element.24.refs_2_), channel_id=1, source_target_pairs={{0,8},{4,12},{8,0},{12,4},{16,24},{20,28},{24,16},{28,20},{1,9},{5... | collective-permute-start | bytes 393224 | tf_op jit(solution)/shard_map/ppermute | solution.py:32
  35.4 21.6 %collective-permute-start.9 = (bf16[256,512]{1,0:T(8,128)(2,1)S(1)}, bf16[256,512]{1,0:T(8,128)(2,1)S(1)}, u32[]{:S(2)}, u32[]{:S(2)}) collective-permute-start(bf16[256,512]{1,0:T(8,128)(2,1)S(1)} %get-tuple-element.23.refs_0_), channel_id=1, source_target_pairs={{4,8},{12,16},{20,24},{8,4},{16,12},{24,20},{5,9},{13,17},{21,25},... | collective-permute-start | bytes 786440 | tf_op jit(solution)/shard_map/ppermute | solution.py:484
  36.1 20.9 %collective-permute-start.12 = (bf16[128,512]{1,0:T(8,128)(2,1)S(1)}, bf16[128,512]{1,0:T(8,128)(2,1)S(1)}, u32[]{:S(2)}, u32[]{:S(2)}) collective-permute-start(bf16[128,512]{1,0:T(8,128)(2,1)S(1)} %collective-permute-done.10.refs_1_), channel_id=1, source_target_pairs={{0,8},{4,12},{8,0},{12,4},{16,24},{20,28},{24,16},{28,20},{1,9},{5... | collective-permute-start | bytes 393224 | tf_op jit(solution)/shard_map/ppermute | solution.py:32
  57.0 1.6 %copy-start.11 = (bf16[256,2048]{1,0:T(8,128)(2,1)}, bf16[256,2048]{1,0:T(8,128)(2,1)S(1)}, u32[]{:S(2)}) copy-start(bf16[256,2048]{1,0:T(8,128)(2,1)S(1)} %collective-permute-done.16.refs_0_) | copy-start | bytes 3145732
  57.0 12.5 %collective-permute-start.18 = (bf16[256,2048]{1,0:T(8,128)(2,1)S(1)}, bf16[256,2048]{1,0:T(8,128)(2,1)S(1)}, u32[]{:S(2)}, u32[]{:S(2)}) collective-permute-start(bf16[256,2048]{1,0:T(8,128)(2,1)S(1)} %collective-permute-done.16.refs_0_), channel_id=1, source_target_pairs={{0,1},{1,0},{2,3},{3,2},{4,5},{5,4},{6,7},{7,6},{8,9},{9,8},{10,11... | collective-permute-start | bytes 3145736 | tf_op jit(solution)/shard_map/ppermute | solution.py:32
  58.6 6.0 %collective-permute-start.15 = (bf16[256,256]{1,0:T(8,128)(2,1)S(1)}, bf16[256,256]{1,0:T(8,128)(2,1)S(1)}, u32[]{:S(2)}, u32[]{:S(2)}) collective-permute-start(bf16[256,256]{1,0:T(8,128)(2,1)S(1)} %shard_map.150.refs_0_), channel_id=1, source_target_pairs={{0,2},{1,3},{2,0},{3,1},{4,6},{5,7},{6,4},{7,5},{8,10},{9,11},{10,... | collective-permute-start | bytes 393224 | tf_op jit(solution)/shard_map/ppermute | solution.py:32
  60.1 6.9 %collective-permute-start.13 = (bf16[256,256]{1,0:T(8,128)(2,1)S(1)}, bf16[256,256]{1,0:T(8,128)(2,1)S(1)}, u32[]{:S(2)}, u32[]{:S(2)}) collective-permute-start(bf16[256,256]{1,0:T(8,128)(2,1)S(1)} %shard_map.150.refs_0_), channel_id=1, source_target_pairs={{0,1},{1,0},{2,3},{3,2},{4,5},{5,4},{6,7},{7,6},{8,9},{9,8},{10,11... | collective-permute-start | bytes 393224 | tf_op jit(solution)/shard_map/ppermute | solution.py:32
  64.6 4.9 %collective-permute-start.17 = (bf16[256,256]{1,0:T(8,128)(2,1)S(1)}, bf16[256,256]{1,0:T(8,128)(2,1)S(1)}, u32[]{:S(2)}, u32[]{:S(2)}) collective-permute-start(bf16[256,256]{1,0:T(8,128)(2,1)S(1)} %collective-permute-done.15.refs_1_), channel_id=1, source_target_pairs={{0,1},{1,0},{2,3},{3,2},{4,5},{5,4},{6,7},{7,6},{8,9},{9,8},{10,11... | collective-permute-start | bytes 393224 | tf_op jit(solution)/shard_map/ppermute | solution.py:32
  69.0 1.2 %copy-start.4 = (bf16[256,2048]{1,0:T(8,128)(2,1)S(1)}, bf16[256,2048]{1,0:T(8,128)(2,1)}, u32[]{:S(2)}) copy-start(bf16[256,2048]{1,0:T(8,128)(2,1)} %lat_ref.5) | copy-start | bytes 3145732
  69.0 1.2 %copy-start.6 = (f32[8,2048]{1,0:T(8,128)S(1)}, f32[8,2048]{1,0:T(8,128)}, u32[]{:S(2)}) copy-start(f32[8,2048]{1,0:T(8,128)} %copy-done.5) | copy-start | bytes 196612

commit v5 on v4

--- a/solution.py
+++ b/solution.py
@@ -482,7 +482,13 @@
     other_pairs = [(i, i + 1) for i in range(1, sp_count - 1, 2)]
     other_pairs += [(j, i) for i, j in other_pairs]
     other_kv = lax.ppermute(kv, "sp", other_pairs)
-    ctx_pieces = gather_pieces(ctx_kv, "sp", [code for code in sp_bits if code != raw_code])
+    rest = [code for code in sp_bits if code != raw_code]
+    ctx_pieces = [ctx_kv]
+    for code in (rest[0], rest[1], rest[0] | rest[1]):
+        ctx_pieces.append(swap(ctx_kv, "sp", code))
+    if rest[2:]:
+        whole = jnp.concatenate(ctx_pieces, axis=0)
+        ctx_pieces = gather_pieces(whole, "sp", rest[2:])
 
     def attend(lat, lat_kinds, ctx, prev, is_last):
         shape = (tokens, cols)

time: 72.4 us -> 66.1 us (0.913)
  starting transfers between devices: 24.4 us -> 20.6 us
  waiting for transfers between devices: 30.7 us -> 29.4 us
  Pallas kernels: 15.9 us -> 14.7 us
    ppermute x18, starting transfers between devices: 23.7 us -> 20 us  [swap(): lax.ppermute(x, axis, [(i, i ^ code) for i in range(lax.axis_size(axis))])]
    ppermute x18, waiting for transfers between devices: 30.7 us -> 29.4 us  [swap(): lax.ppermute(x, axis, [(i, i ^ code) for i in range(lax.axis_size(axis))])]
    pallas_call x11, Pallas kernels: 15.9 us -> 14.7 us  [run(): return pl.pallas_call(*args, **kwargs)(*operands)]
  transfers between devices with their start and end apart: 19 -> 19, of which waited for: 7 -> 6; matrix products, arithmetic and copies ran while one was open for 0% -> 0% of each run, Pallas kernels for 17% -> 17%
where the time goes in v5:
time: 66.1 us; the launch traced here: 65.9 us
  waiting for transfers between devices  29.4 us (44%)
  starting transfers between devices  20.6 us (31%)
  Pallas kernels  14.7 us (22%)
  local copies, waits for them, and re-layouts  0.81 us (1%)
    ppermute x18, waiting for transfers between devices, swap(): lax.ppermute(x, axis, [(i, i ^ code) for i in range(lax.axis_size(axis))])  29.4 us
    ppermute x18, starting transfers between devices, swap(): lax.ppermute(x, axis, [(i, i ^ code) for i in range(lax.axis_size(axis))])  20 us
    pallas_call x11, Pallas kernels, run(): return pl.pallas_call(*args, **kwargs)(*operands)  14.7 us
  transfers between devices with their start and end apart: 19, of which 6 were waited for; matrix products, arithmetic and copies ran while one was open for 0% of the time, Pallas kernels for 17%

profile of v5, /device:TPU:0, one launch (start us, length us, event | category | flops | bytes accessed | tf_op | source)
XLA Modules:
  0.0 65.9 jit_solution(12555388006808439616)
XLA Ops:
  0.0 1.6 %shard_map.145 = (f32[8,512]{1,0:T(8,128)S(1)}, bf16[64,1024]{1,0:T(8,128)(2,1)S(1)}, bf16[256,1024]{1,0:T(8,128)(2,1)S(1)}) custom-call(f32[1,256]{1,0:T(1,128)} %bitcast.10, f32[1,256]{1,0:T(1,128)} %bitcast.11, bf16[256,512]{1,0:T(8,128)(2,1)} %shift_ref.1, bf16[256,512]{1,0:T(8,128)(2,1)} %scale_ref.1, bf16[256,512]{1,0:T(8,128)(2,1)} %gate_ref.1, ...), custom_call_target="tpu_custom_call" | custom-call | flops 137438953472 | bytes 1048576 | tf_op jit(solution)/shard_map/pallas_call | solution.py:37
  1.7 3.1 %collective-permute-start.7 = (bf16[256,1024]{1,0:T(8,128)(2,1)S(1)}, bf16[256,1024]{1,0:T(8,128)(2,1)S(1)}, u32[]{:S(2)}, u32[]{:S(2)}) collective-permute-start(bf16[256,1024]{1,0:T(8,128)(2,1)S(1)} %get-tuple-element.20), channel_id=1, source_target_pairs={{0,4},{4,0},{8,12},{12,8},{16,20},{20,16},{24,28},{28,24},{1,5},{5... | collective-permute-start | bytes 1572872 | tf_op jit(solution)/shard_map/ppermute | solution.py:32
  4.7 1.5 %collective-permute-start.2 = (f32[8,512]{1,0:T(8,128)S(1)}, f32[8,512]{1,0:T(8,128)S(1)}, u32[]{:S(2)}, u32[]{:S(2)}) collective-permute-start(f32[8,512]{1,0:T(8,128)S(1)} %get-tuple-element.18), channel_id=1, source_target_pairs={{0,2},{1,3},{2,0},{3,1},{4,6},{5,7},{6,4},{7,5},{8,10},{9,11},{10,... | collective-permute-start | bytes 49160 | tf_op jit(solution)/shard_map/ppermute | solution.py:32
  6.2 2.6 %collective-permute-start = (bf16[64,1024]{1,0:T(8,128)(2,1)S(1)}, bf16[64,1024]{1,0:T(8,128)(2,1)S(1)}, u32[]{:S(2)}, u32[]{:S(2)}) collective-permute-start(bf16[64,1024]{1,0:T(8,128)(2,1)S(1)} %get-tuple-element.17), channel_id=1, source_target_pairs={{0,16},{4,20},{8,24},{12,28},{16,0},{20,4},{24,8},{28,12},{1,17},{... | collective-permute-start | bytes 393224 | tf_op jit(solution)/shard_map/ppermute | solution.py:32
  8.8 0.6 collective-permute-start.3
  9.4 5.2 %collective-permute-done.mine_ref = bf16[64,1024]{1,0:T(8,128)(2,1)S(1)} collective-permute-done((bf16[64,1024]{1,0:T(8,128)(2,1)S(1)}, bf16[64,1024]{1,0:T(8,128)(2,1)S(1)}, u32[]{:S(2)}, u32[]{:S(2)}) %collective-permute-start) | collective-permute-done | bytes 131104 | tf_op jit(solution)/shard_map/ppermute | solution.py:32
  14.6 2.7 %collective-permute-done.3 = f32[16,512]{1,0:T(8,128)S(1)} collective-permute-done((f32[16,512]{1,0:T(8,128)S(1)}, f32[16,512]{1,0:T(8,128)S(1)}, u32[]{:S(2)}, u32[]{:S(2)}) %collective-permute-start.3) | collective-permute-done | bytes 32800 | tf_op jit(solution)/shard_map/ppermute | solution.py:32
  17.4 1.8 %collective-permute-start.4 = (f32[16,512]{1,0:T(8,128)S(1)}, f32[16,512]{1,0:T(8,128)S(1)}, u32[]{:S(2)}, u32[]{:S(2)}) collective-permute-start(f32[16,512]{1,0:T(8,128)S(1)} %add.11), channel_id=1, source_target_pairs={{0,8},{4,12},{8,0},{12,4},{16,24},{20,28},{24,16},{28,20},{1,9},{5... | collective-permute-start | bytes 98312 | tf_op jit(solution)/shard_map/ppermute | solution.py:32
  19.2 2.1 %collective-permute-done.4 = f32[16,512]{1,0:T(8,128)S(1)} collective-permute-done((f32[16,512]{1,0:T(8,128)S(1)}, f32[16,512]{1,0:T(8,128)S(1)}, u32[]{:S(2)}, u32[]{:S(2)}) %collective-permute-start.4) | collective-permute-done | bytes 32800 | tf_op jit(solution)/shard_map/ppermute | solution.py:32
  21.3 2.8 %collective-permute-start.5 = (f32[16,512]{1,0:T(8,128)S(1)}, f32[16,512]{1,0:T(8,128)S(1)}, u32[]{:S(2)}, u32[]{:S(2)}) collective-permute-start(f32[16,512]{1,0:T(8,128)S(1)} %add.12), channel_id=1, source_target_pairs={{0,16},{4,20},{8,24},{12,28},{16,0},{20,4},{24,8},{28,12},{1,17},{... | collective-permute-start | bytes 98312 | tf_op jit(solution)/shard_map/ppermute | solution.py:32
  24.1 2.0 %collective-permute-done.5 = f32[16,512]{1,0:T(8,128)S(1)} collective-permute-done((f32[16,512]{1,0:T(8,128)S(1)}, f32[16,512]{1,0:T(8,128)S(1)}, u32[]{:S(2)}, u32[]{:S(2)}) %collective-permute-start.5) | collective-permute-done | bytes 32800 | tf_op jit(solution)/shard_map/ppermute | solution.py:32
  26.1 1.8 %collective-permute-start.16 = (bf16[256,2048]{1,0:T(8,128)(2,1)}, bf16[256,2048]{1,0:T(8,128)(2,1)}, u32[]{:S(2)}, u32[]{:S(2)}) collective-permute-start(bf16[256,2048]{1,0:T(8,128)(2,1)} %refs_0_.1), channel_id=1, source_target_pairs={{0,2},{1,3},{2,0},{3,1},{4,6},{5,7},{6,4},{7,5},{8,10},{9,11},{10,... | collective-permute-start | bytes 3145736 | tf_op jit(solution)/shard_map/ppermute | solution.py:32
  27.9 1.0 %shard_map.148.refs_3_.refs_4_ = f32[4,14,64,128]{3,2,1,0:T(8,128)S(1)} custom-call(f32[4,15,128]{2,1,0:T(8,128)S(1)} %pad.4.bias_ref), custom_call_target="tpu_custom_call" | custom-call | tf_op jit(solution)/shard_map/pallas_call | solution.py:37
  28.9 0.2 collective-permute-start.8
  29.2 2.0 %shard_map.146 = (bf16[256,512]{1,0:T(8,128)(2,1)S(1)}, bf16[128,512]{1,0:T(8,128)(2,1)S(1)}, bf16[256,2048]{1,0:T(8,128)(2,1)S(1)}, f32[8,2048]{1,0:T(8,128)S(1)}) custom-call(bf16[256,2048]{1,0:T(8,128)(2,1)S(1)} %copy-done.3, bf16[64,2048]{1,0:T(8,128)(2,1)S(1)} %copy-done.10, bf16[64,1024]{1,0:T(8,128)(2,1)S(1)} %collective-permute-done.mine_ref, ...), custom_call_target="tpu_custom_call" | custom-call | flops 137438953472 | bytes 1048576 | tf_op jit(solution)/shard_map/pallas_call | solution.py:37
  31.2 1.6 %collective-permute-start.10 = (bf16[128,512]{1,0:T(8,128)(2,1)S(1)}, bf16[128,512]{1,0:T(8,128)(2,1)S(1)}, u32[]{:S(2)}, u32[]{:S(2)}) collective-permute-start(bf16[128,512]{1,0:T(8,128)(2,1)S(1)} %get-tuple-element.24.refs_2_), channel_id=1, source_target_pairs={{0,4},{4,0},{8,12},{12,8},{16,20},{20,16},{24,28},{28,24},{1,5},{5... | collective-permute-start | bytes 393224 | tf_op jit(solution)/shard_map/ppermute | solution.py:32
  32.8 1.6 %collective-permute-start.11 = (bf16[128,512]{1,0:T(8,128)(2,1)S(1)}, bf16[128,512]{1,0:T(8,128)(2,1)S(1)}, u32[]{:S(2)}, u32[]{:S(2)}) collective-permute-start(bf16[128,512]{1,0:T(8,128)(2,1)S(1)} %get-tuple-element.24.refs_2_), channel_id=1, source_target_pairs={{0,8},{4,12},{8,0},{12,4},{16,24},{20,28},{24,16},{28,20},{1,9},{5... | collective-permute-start | bytes 393224 | tf_op jit(solution)/shard_map/ppermute | solution.py:32
  34.4 0.4 collective-permute-start.12
  34.8 0.7 %collective-permute-start.9 = (bf16[256,512]{1,0:T(8,128)(2,1)S(1)}, bf16[256,512]{1,0:T(8,128)(2,1)S(1)}, u32[]{:S(2)}, u32[]{:S(2)}) collective-permute-start(bf16[256,512]{1,0:T(8,128)(2,1)S(1)} %get-tuple-element.23.refs_0_), channel_id=1, source_target_pairs={{4,8},{12,16},{20,24},{8,4},{16,12},{24,20},{5,9},{13,17},{21,25},... | collective-permute-start | bytes 786440 | tf_op jit(solution)/shard_map/ppermute | solution.py:484
  35.5 1.8 %shard_map.147 = (bf16[256,512]{1,0:T(8,128)(2,1)S(1)}, bf16[256,256]{1,0:T(8,128)(2,1)S(1)}) custom-call(bf16[256,1024]{1,0:T(8,128)(2,1)S(1)} %collective-permute-done.7.mine_ref, bf16[256,1024]{1,0:T(8,128)(2,1)S(1)} %collective-permute-done.8.passed_ref, f32[8,2048]{1,0:T(8,128)S(1)} %get-tuple-element.19.vec_ref.gate_ref, f32[1,2048]{1,0:T(1,128)S(1)} %bitcast.6, ...), custom_call_target="tpu_custom_call" | custom-call | tf_op jit(solution)/shard_map/pallas_call | solution.py:37
  37.3 1.3 %shard_map.149 = (f32[256,256]{1,0:T(8,128)S(1)}, f32[256,256]{1,0:T(8,128)S(1)}, f32[256,256]{1,0:T(8,128)S(1)}) custom-call(bf16[256,256]{1,0:T(8,128)(2,1)S(1)} %get-tuple-element.22.q_ref, bf16[256,512]{1,0:T(8,128)(2,1)S(1)} %get-tuple-element.23.refs_0_, bf16[256,512]{1,0:T(8,128)(2,1)S(1)} %get-tuple-element.25.refs_1_, ...), custom_call_target="tpu_custom_call" | custom-call | flops 137438953472 | bytes 1048576 | tf_op jit(solution)/shard_map/pallas_call | solution.py:37
  38.7 13.3 %collective-permute-done.16.refs_0_ = bf16[256,2048]{1,0:T(8,128)(2,1)} collective-permute-done((bf16[256,2048]{1,0:T(8,128)(2,1)}, bf16[256,2048]{1,0:T(8,128)(2,1)}, u32[]{:S(2)}, u32[]{:S(2)}) %collective-permute-start.16) | collective-permute-done | bytes 1048608 | tf_op jit(solution)/shard_map/ppermute | solution.py:32
  52.0 1.5 %shard_map.150.refs_0_ = bf16[256,256]{1,0:T(8,128)(2,1)S(1)} custom-call(bf16[256,256]{1,0:T(8,128)(2,1)S(1)} %get-tuple-element.22.q_ref, bf16[256,512]{1,0:T(8,128)(2,1)S(1)} %collective-permute-done.9.refs_0_, bf16[128,512]{1,0:T(8,128)(2,1)S(1)} %collective-permute-done.10.refs_1_, bf16[128,512]{1,0:T(8,128)(2,1)S(1)} %collective-permute-done.11.refs_2_, ...), custom_call_target="tpu_custom_call" | custom-call | flops 137438953472 | bytes 1048576 | tf_op jit(solution)/shard_map/pallas_call | solution.py:37
  53.6 1.8 %collective-permute-start.15 = (bf16[256,256]{1,0:T(8,128)(2,1)S(1)}, bf16[256,256]{1,0:T(8,128)(2,1)S(1)}, u32[]{:S(2)}, u32[]{:S(2)}) collective-permute-start(bf16[256,256]{1,0:T(8,128)(2,1)S(1)} %shard_map.150.refs_0_), channel_id=1, source_target_pairs={{0,2},{1,3},{2,0},{3,1},{4,6},{5,7},{6,4},{7,5},{8,10},{9,11},{10,... | collective-permute-start | bytes 393224 | tf_op jit(solution)/shard_map/ppermute | solution.py:32
  55.3 0.2 collective-permute-start.13
  55.6 4.0 %collective-permute-done.15.refs_1_ = bf16[256,256]{1,0:T(8,128)(2,1)S(1)} collective-permute-done((bf16[256,256]{1,0:T(8,128)(2,1)S(1)}, bf16[256,256]{1,0:T(8,128)(2,1)S(1)}, u32[]{:S(2)}, u32[]{:S(2)}) %collective-permute-start.15) | collective-permute-done | bytes 131104 | tf_op jit(solution)/shard_map/ppermute | solution.py:32
  59.5 1.2 %shard_map.151.refs_2_ = bf16[256,2048]{1,0:T(8,128)(2,1)S(1)} custom-call(bf16[256,2048]{1,0:T(8,128)(2,1)} %refs_0_.1), custom_call_target="tpu_custom_call" | custom-call | tf_op jit(solution)/shard_map/pallas_call | solution.py:37
  60.8 1.2 %shard_map.153.refs_2_ = bf16[256,2048]{1,0:T(8,128)(2,1)S(1)} custom-call(bf16[256,2048]{1,0:T(8,128)(2,1)} %collective-permute-done.16.refs_0_), custom_call_target="tpu_custom_call" | custom-call | tf_op jit(solution)/shard_map/pallas_call | solution.py:37
  62.0 0.7 %shard_map.152.refs_0_ = f32[256,2048]{1,0:T(8,128)S(1)} custom-call(bf16[256,256]{1,0:T(8,128)(2,1)S(1)} %shard_map.150.refs_0_, bf16[256,256]{1,0:T(8,128)(2,1)S(1)} %collective-permute-done.13.refs_1_, bf16[256,2048]{1,0:T(8,128)(2,1)S(1)} %shard_map.151.refs_2_, bf16[256,2048]{1,0:T(8,128)(2,1)S(1)} %collective-permute-done.14.refs_3_), custom_call_target="tpu_custom_call" | custom-call | tf_op jit(solution)/shard_map/pallas_call | solution.py:37
  62.8 0.4 shard_map.154.sum_ref
  63.3 0.7 %copy-done.4 = bf16[256,2048]{1,0:T(8,128)(2,1)S(1)} copy-done((bf16[256,2048]{1,0:T(8,128)(2,1)S(1)}, bf16[256,2048]{1,0:T(8,128)(2,1)}, u32[]{:S(2)}) %copy-start.4) | copy-done | bytes 1048600
  64.0 1.9 %shard_map.155 = bf16[256,2048]{1,0:T(8,128)(2,1)} custom-call(bf16[256,2048]{1,0:T(8,128)(2,1)S(1)} %copy-done.4, f32[8,2048]{1,0:T(8,128)S(1)} %copy-done.6, f32[256,2048]{1,0:T(8,128)S(1)} %shard_map.154.sum_ref, bf16[256,256]{1,0:T(8,128)(2,1)S(1)} %collective-permute-done.17.refs_0_, bf16[256,2048]{1,0:T(8,128)(2,1)S(1)} %collective-permute-done.18.refs_1_), custom_call_target="tpu_custom_call" | custom-call | tf_op jit(solution)/shard_map/pallas_call | solution.py:37
  (48 shorter events, 0.2 us)
Async XLA Ops:
  0.0 27.9 %copy-start.11 = (f32[4,15,31]{2,0,1:T(4,128)S(1)}, f32[4,15,31]{2,0,1:T(4,128)}, u32[]{:S(2)}) copy-start(f32[4,15,31]{2,0,1:T(4,128)} %param.28) | copy-start | bytes 22324
  0.0 29.2 %copy-start.3 = (bf16[256,2048]{1,0:T(8,128)(2,1)S(1)}, bf16[256,2048]{1,0:T(8,128)(2,1)}, u32[]{:S(2)}) copy-start(bf16[256,2048]{1,0:T(8,128)(2,1)} %lat_ref.5) | copy-start | bytes 3145732
  0.0 29.2 %copy-start.10 = (bf16[64,2048]{1,0:T(8,128)(2,1)S(1)}, bf16[64,2048]{1,0:T(8,128)(2,1)}, u32[]{:S(2)}) copy-start(bf16[64,2048]{1,0:T(8,128)(2,1)} %ctx_ref.3) | copy-start | bytes 786436
  1.6 27.6 %copy-start = (bf16[2048,256]{1,0:T(8,128)(2,1)S(1)}, bf16[2048,256]{1,0:T(8,128)(2,1)}, u32[]{:S(2)}) copy-start(bf16[2048,256]{1,0:T(8,128)(2,1)} %wk.1) | copy-start | bytes 3145732
  1.6 27.6 %copy-start.1 = (bf16[2048,256]{1,0:T(8,128)(2,1)S(1)}, bf16[2048,256]{1,0:T(8,128)(2,1)}, u32[]{:S(2)}) copy-start(bf16[2048,256]{1,0:T(8,128)(2,1)} %wv.1) | copy-start | bytes 3145732
  1.6 27.6 %copy-start.7 = (f32[2048]{0:T(1024)S(1)}, f32[2048]{0:T(1024)}, u32[]{:S(2)}) copy-start(f32[2048]{0:T(1024)} %param.22) | copy-start | bytes 24580
  1.7 27.6 %copy-start.8 = (f32[64]{0:T(128)S(1)}, f32[64]{0:T(128)}, u32[]{:S(2)}) copy-start(f32[64]{0:T(128)} %param.27) | copy-start | bytes 772
  1.7 27.3 %collective-permute-start.7 = (bf16[256,1024]{1,0:T(8,128)(2,1)S(1)}, bf16[256,1024]{1,0:T(8,128)(2,1)S(1)}, u32[]{:S(2)}, u32[]{:S(2)}) collective-permute-start(bf16[256,1024]{1,0:T(8,128)(2,1)S(1)} %get-tuple-element.20), channel_id=1, source_target_pairs={{0,4},{4,0},{8,12},{12,8},{16,20},{20,16},{24,28},{28,24},{1,5},{5... | collective-permute-start | bytes 1572872 | tf_op jit(solution)/shard_map/ppermute | solution.py:32
  4.7 4.1 %collective-permute-start.2 = (f32[8,512]{1,0:T(8,128)S(1)}, f32[8,512]{1,0:T(8,128)S(1)}, u32[]{:S(2)}, u32[]{:S(2)}) collective-permute-start(f32[8,512]{1,0:T(8,128)S(1)} %get-tuple-element.18), channel_id=1, source_target_pairs={{0,2},{1,3},{2,0},{3,1},{4,6},{5,7},{6,4},{7,5},{8,10},{9,11},{10,... | collective-permute-start | bytes 49160 | tf_op jit(solution)/shard_map/ppermute | solution.py:32
  6.2 8.4 %collective-permute-start = (bf16[64,1024]{1,0:T(8,128)(2,1)S(1)}, bf16[64,1024]{1,0:T(8,128)(2,1)S(1)}, u32[]{:S(2)}, u32[]{:S(2)}) collective-permute-start(bf16[64,1024]{1,0:T(8,128)(2,1)S(1)} %get-tuple-element.17), channel_id=1, source_target_pairs={{0,16},{4,20},{8,24},{12,28},{16,0},{20,4},{24,8},{28,12},{1,17},{... | collective-permute-start | bytes 393224 | tf_op jit(solution)/shard_map/ppermute | solution.py:32
  8.8 8.5 %collective-permute-start.3 = (f32[16,512]{1,0:T(8,128)S(1)}, f32[16,512]{1,0:T(8,128)S(1)}, u32[]{:S(2)}, u32[]{:S(2)}) collective-permute-start(f32[16,512]{1,0:T(8,128)S(1)} %constant_dynamic-update-slice_fusion), channel_id=1, source_target_pairs={{0,4},{4,0},{8,12},{12,8},{16,20},{20,16},{24,28},{28,24},{1,5},{5... | collective-permute-start | bytes 98312 | tf_op jit(solution)/shard_map/ppermute | solution.py:32
  14.6 14.6 %collective-permute-start.1 = (bf16[64,1024]{1,0:T(8,128)(2,1)S(1)}, bf16[64,1024]{1,0:T(8,128)(2,1)S(1)}, u32[]{:S(2)}, u32[]{:S(2)}) collective-permute-start(bf16[64,1024]{1,0:T(8,128)(2,1)S(1)} %collective-permute-done.mine_ref), channel_id=1, source_target_pairs={{0,1},{1,0},{2,3},{3,2},{4,5},{5,4},{6,7},{7,6},{8,9},{9,8},{10,11... | collective-permute-start | bytes 393224 | tf_op jit(solution)/shard_map/ppermute | solution.py:32
  17.4 3.9 %collective-permute-start.4 = (f32[16,512]{1,0:T(8,128)S(1)}, f32[16,512]{1,0:T(8,128)S(1)}, u32[]{:S(2)}, u32[]{:S(2)}) collective-permute-start(f32[16,512]{1,0:T(8,128)S(1)} %add.11), channel_id=1, source_target_pairs={{0,8},{4,12},{8,0},{12,4},{16,24},{20,28},{24,16},{28,20},{1,9},{5... | collective-permute-start | bytes 98312 | tf_op jit(solution)/shard_map/ppermute | solution.py:32
  21.3 4.8 %collective-permute-start.5 = (f32[16,512]{1,0:T(8,128)S(1)}, f32[16,512]{1,0:T(8,128)S(1)}, u32[]{:S(2)}, u32[]{:S(2)}) collective-permute-start(f32[16,512]{1,0:T(8,128)S(1)} %add.12), channel_id=1, source_target_pairs={{0,16},{4,20},{8,24},{12,28},{16,0},{20,4},{24,8},{28,12},{1,17},{... | collective-permute-start | bytes 98312 | tf_op jit(solution)/shard_map/ppermute | solution.py:32
  26.1 3.0 %collective-permute-start.6 = (f32[16,512]{1,0:T(8,128)S(1)}, f32[16,512]{1,0:T(8,128)S(1)}, u32[]{:S(2)}, u32[]{:S(2)}) collective-permute-start(f32[16,512]{1,0:T(8,128)S(1)} %add.13.part_ref), channel_id=1, source_target_pairs={{0,1},{1,0},{2,3},{3,2},{4,5},{5,4},{6,7},{7,6},{8,9},{9,8},{10,11... | collective-permute-start | bytes 98312 | tf_op jit(solution)/shard_map/ppermute | solution.py:32
  26.1 25.9 %collective-permute-start.16 = (bf16[256,2048]{1,0:T(8,128)(2,1)}, bf16[256,2048]{1,0:T(8,128)(2,1)}, u32[]{:S(2)}, u32[]{:S(2)}) collective-permute-start(bf16[256,2048]{1,0:T(8,128)(2,1)} %refs_0_.1), channel_id=1, source_target_pairs={{0,2},{1,3},{2,0},{3,1},{4,6},{5,7},{6,4},{7,5},{8,10},{9,11},{10,... | collective-permute-start | bytes 3145736 | tf_op jit(solution)/shard_map/ppermute | solution.py:32
  28.9 5.9 %collective-permute-start.8 = (bf16[256,1024]{1,0:T(8,128)(2,1)S(1)}, bf16[256,1024]{1,0:T(8,128)(2,1)S(1)}, u32[]{:S(2)}, u32[]{:S(2)}) collective-permute-start(bf16[256,1024]{1,0:T(8,128)(2,1)S(1)} %collective-permute-done.7.mine_ref), channel_id=1, source_target_pairs={{0,1},{1,0},{2,3},{3,2},{4,5},{5,4},{6,7},{7,6},{8,9},{9,8},{10,11... | collective-permute-start | bytes 1572872 | tf_op jit(solution)/shard_map/ppermute | solution.py:32
  29.2 6.2 %copy-start.2 = (bf16[2048,256]{1,0:T(8,128)(2,1)S(1)}, bf16[2048,256]{1,0:T(8,128)(2,1)}, u32[]{:S(2)}) copy-start(bf16[2048,256]{1,0:T(8,128)(2,1)} %wq.1) | copy-start | bytes 3145732
  29.2 6.2 %copy-start.9 = (f32[64]{0:T(128)S(1)}, f32[64]{0:T(128)}, u32[]{:S(2)}) copy-start(f32[64]{0:T(128)} %param.26) | copy-start | bytes 772
  31.2 6.1 %copy-start.5 = (f32[8,2048]{1,0:T(8,128)}, f32[8,2048]{1,0:T(8,128)S(1)}, u32[]{:S(2)}) copy-start(f32[8,2048]{1,0:T(8,128)S(1)} %get-tuple-element.19.vec_ref.gate_ref) | copy-start | bytes 196612
  31.2 7.4 %collective-permute-start.10 = (bf16[128,512]{1,0:T(8,128)(2,1)S(1)}, bf16[128,512]{1,0:T(8,128)(2,1)S(1)}, u32[]{:S(2)}, u32[]{:S(2)}) collective-permute-start(bf16[128,512]{1,0:T(8,128)(2,1)S(1)} %get-tuple-element.24.refs_2_), channel_id=1, source_target_pairs={{0,4},{4,0},{8,12},{12,8},{16,20},{20,16},{24,28},{28,24},{1,5},{5... | collective-permute-start | bytes 393224 | tf_op jit(solution)/shard_map/ppermute | solution.py:32
  32.8 19.2 %collective-permute-start.11 = (bf16[128,512]{1,0:T(8,128)(2,1)S(1)}, bf16[128,512]{1,0:T(8,128)(2,1)S(1)}, u32[]{:S(2)}, u32[]{:S(2)}) collective-permute-start(bf16[128,512]{1,0:T(8,128)(2,1)S(1)} %get-tuple-element.24.refs_2_), channel_id=1, source_target_pairs={{0,8},{4,12},{8,0},{12,4},{16,24},{20,28},{24,16},{28,20},{1,9},{5... | collective-permute-start | bytes 393224 | tf_op jit(solution)/shard_map/ppermute | solution.py:32
  34.4 17.6 %collective-permute-start.12 = (bf16[128,512]{1,0:T(8,128)(2,1)S(1)}, bf16[128,512]{1,0:T(8,128)(2,1)S(1)}, u32[]{:S(2)}, u32[]{:S(2)}) collective-permute-start(bf16[128,512]{1,0:T(8,128)(2,1)S(1)} %get-tuple-element.24.refs_2_), channel_id=1, source_target_pairs={{0,12},{4,8},{8,4},{12,0},{16,28},{20,24},{24,20},{28,16},{1,13},{... | collective-permute-start | bytes 393224 | tf_op jit(solution)/shard_map/ppermute | solution.py:32
  34.8 17.2 %collective-permute-start.9 = (bf16[256,512]{1,0:T(8,128)(2,1)S(1)}, bf16[256,512]{1,0:T(8,128)(2,1)S(1)}, u32[]{:S(2)}, u32[]{:S(2)}) collective-permute-start(bf16[256,512]{1,0:T(8,128)(2,1)S(1)} %get-tuple-element.23.refs_0_), channel_id=1, source_target_pairs={{4,8},{12,16},{20,24},{8,4},{16,12},{24,20},{5,9},{13,17},{21,25},... | collective-permute-start | bytes 786440 | tf_op jit(solution)/shard_map/ppermute | solution.py:484
  38.6 23.4 %collective-permute-start.14 = (bf16[256,2048]{1,0:T(8,128)(2,1)}, bf16[256,2048]{1,0:T(8,128)(2,1)S(1)}, u32[]{:S(2)}, u32[]{:S(2)}) collective-permute-start(bf16[256,2048]{1,0:T(8,128)(2,1)} %refs_0_.1), channel_id=1, source_target_pairs={{0,1},{1,0},{2,3},{3,2},{4,5},{5,4},{6,7},{7,6},{8,9},{9,8},{10,11... | collective-permute-start | bytes 3145736 | tf_op jit(solution)/shard_map/ppermute | solution.py:32
  52.0 11.3 %collective-permute-start.18 = (bf16[256,2048]{1,0:T(8,128)(2,1)}, bf16[256,2048]{1,0:T(8,128)(2,1)S(1)}, u32[]{:S(2)}, u32[]{:S(2)}) collective-permute-start(bf16[256,2048]{1,0:T(8,128)(2,1)} %collective-permute-done.16.refs_0_), channel_id=1, source_target_pairs={{0,1},{1,0},{2,3},{3,2},{4,5},{5,4},{6,7},{7,6},{8,9},{9,8},{10,11... | collective-permute-start | bytes 3145736 | tf_op jit(solution)/shard_map/ppermute | solution.py:32
  53.6 6.0 %collective-permute-start.15 = (bf16[256,256]{1,0:T(8,128)(2,1)S(1)}, bf16[256,256]{1,0:T(8,128)(2,1)S(1)}, u32[]{:S(2)}, u32[]{:S(2)}) collective-permute-start(bf16[256,256]{1,0:T(8,128)(2,1)S(1)} %shard_map.150.refs_0_), channel_id=1, source_target_pairs={{0,2},{1,3},{2,0},{3,1},{4,6},{5,7},{6,4},{7,5},{8,10},{9,11},{10,... | collective-permute-start | bytes 393224 | tf_op jit(solution)/shard_map/ppermute | solution.py:32
  55.3 6.7 %collective-permute-start.13 = (bf16[256,256]{1,0:T(8,128)(2,1)S(1)}, bf16[256,256]{1,0:T(8,128)(2,1)S(1)}, u32[]{:S(2)}, u32[]{:S(2)}) collective-permute-start(bf16[256,256]{1,0:T(8,128)(2,1)S(1)} %shard_map.150.refs_0_), channel_id=1, source_target_pairs={{0,1},{1,0},{2,3},{3,2},{4,5},{5,4},{6,7},{7,6},{8,9},{9,8},{10,11... | collective-permute-start | bytes 393224 | tf_op jit(solution)/shard_map/ppermute | solution.py:32
  59.5 3.7 %collective-permute-start.17 = (bf16[256,256]{1,0:T(8,128)(2,1)S(1)}, bf16[256,256]{1,0:T(8,128)(2,1)S(1)}, u32[]{:S(2)}, u32[]{:S(2)}) collective-permute-start(bf16[256,256]{1,0:T(8,128)(2,1)S(1)} %collective-permute-done.15.refs_1_), channel_id=1, source_target_pairs={{0,1},{1,0},{2,3},{3,2},{4,5},{5,4},{6,7},{7,6},{8,9},{9,8},{10,11... | collective-permute-start | bytes 393224 | tf_op jit(solution)/shard_map/ppermute | solution.py:32
  62.8 1.2 %copy-start.4 = (bf16[256,2048]{1,0:T(8,128)(2,1)S(1)}, bf16[256,2048]{1,0:T(8,128)(2,1)}, u32[]{:S(2)}) copy-start(bf16[256,2048]{1,0:T(8,128)(2,1)} %lat_ref.5) | copy-start | bytes 3145732
  62.8 1.2 %copy-start.6 = (f32[8,2048]{1,0:T(8,128)S(1)}, f32[8,2048]{1,0:T(8,128)}, u32[]{:S(2)}) copy-start(f32[8,2048]{1,0:T(8,128)} %copy-done.5) | copy-start | bytes 196612
